TPU v7x, 512 devices: a whole 4x4x16 slice. The times are simulated.
512 devices in a mesh: sp: 32 (over z, core), tp: 16 (over y, x).
Axes of the slice: x: 4, y: 4, z: 16, core: 2. Of those that a mesh axis runs over, the one named last changes fastest.
Arguments:
- queries: bfloat16 [8192, 2048], P('sp', 'tp'), may hold values from -6 to 6
- keys: bfloat16 [8192, 256], P('sp'), may hold values from -6 to 6
- values: bfloat16 [8192, 256], P('sp'), may hold values from -6 to 6
- query_gain: float32 [128], replicated, may hold values from 0.1 to 5.5
- key_gain: float32 [128], replicated, may hold values from 0.1 to 5.5
- out_proj: bfloat16 [2048, 2048], P(None, 'tp'), may hold values from -0.125 to 0.125
- expert_norm_scale: float32 [2048], replicated, may hold values from 0.1 to 1.9
- residual: bfloat16 [8192, 2048], P(('sp', 'tp')), may hold values from -6 to 6
- routes: int32 [8192, 2], P(('sp', 'tp')), may hold values from 0 to 31, all different within a row; in each aligned block of 16 rows (0 to 15, 16 to 31, ...) at most 2 rows name the same one
- route_weights: float32 [8192, 2], P(('sp', 'tp')), may hold values from 0.1 to 0.9
- w_gate: bfloat16 [32, 2048, 4096], P('sp', None, 'tp'), may hold values from -0.125 to 0.125
- w_up: bfloat16 [32, 2048, 4096], P('sp', None, 'tp'), may hold values from -0.125 to 0.125
- w_down: bfloat16 [32, 4096, 2048], P('sp', 'tp'), may hold values from -0.09375 to 0.09375
Outputs:
- layer_out: bfloat16 [8192, 2048], P(('sp', 'tp'))
Inputs may be any that keep to these rules, and one draw needn't show every extreme that they name: `routes`: in the rows of one device no expert is named by more than 2 rows, a bound that some block reaches; a row names 2 different experts.
All inputs are finite; a program needn't handle non-finite values.
Results may differ from a plain program's by a relative error of at most 0.0095.
The roundings to bfloat16 on the way count: a program that leaves them out, or rounds other values in their place, can miss the bound.
Values may be sent and summed in bfloat16 or wider, within the bound.
No kernel may reach another device: no remote copies, remote signals or barrier semaphores. Data moves between devices by JAX's collectives and lax.ppermute only.
A program may use at most 64 MiB of HBM per device.

v0:
```python
import math

import jax
import jax.numpy as jnp
from jax import lax
from jax.experimental import pallas as pl
from jax.experimental.pallas import tpu as pltpu
from jax.sharding import Mesh, PartitionSpec as P


GRID_W = 64
EPS = 1e-06
ROPE_BASE = 10000.0
LOG2E = 1.4426950408889634
BF = jnp.bfloat16
F32 = jnp.float32

NZ, NC, NYH, NYL, NX = 16, 2, 2, 2, 4
NY = NYH * NYL
NT = NY * NX
NG = NYL * NX
TP = ("yh", "yl", "x")
GROUP = ("yl", "x")
STAT_ROWS = 16
COLOURS = tuple((i % NX + i // NX) % 4 for i in range(NT))


def exchange(blocks, axis):
    return lax.all_to_all(blocks, axis, split_axis=0, concat_axis=0, tiled=True)


def swap_cores(value):
    return lax.ppermute(value, "c", [(0, 1), (1, 0)])


def ring(value, axis, step):
    return lax.ppermute(value, axis, [(i, (i + step) % 4) for i in range(4)])


def turned(field, gain, start):
    count, width = field.shape
    quarter = width // 4
    f = field.astype(F32)
    f = f * lax.rsqrt(jnp.mean(f * f, axis=-1, keepdims=True) + EPS) * gain
    lane = lax.broadcasted_iota(jnp.int32, (count, width), 1)
    position = start + lax.broadcasted_iota(jnp.int32, (count, width), 0)
    coord = jnp.where(lane < 2 * quarter, position // GRID_W, position % GRID_W)
    step = (lane % quarter).astype(F32) / quarter
    angle = coord.astype(F32) * jnp.exp(step * (-math.log(ROPE_BASE)))
    first = lane % (2 * quarter) < quarter
    ahead = pltpu.roll(f, width - quarter, 1)
    behind = pltpu.roll(f, quarter, 1)
    other = jnp.where(first, -ahead, behind)
    return (f * jnp.cos(angle) + other * jnp.sin(angle)).astype(BF)


def prepare_kernel(at_ref, q_ref, k_ref, v_ref, q_gain_ref, k_gain_ref, q8_ref, kv_ref):
    q_rot = turned(q_ref[...], q_gain_ref[...], at_ref[2])
    for i in range(q8_ref.shape[0]):
        q8_ref[i] = q_rot
    k_rot = turned(k_ref[...], k_gain_ref[...], at_ref[3])
    both = jnp.concatenate([k_rot, v_ref[...]], axis=1)
    for i in range(kv_ref.shape[0]):
        kv_ref[i] = both


def prepare(queries, keys, values, query_gain, key_gain, block, head, start):
    tokens, width = queries.shape
    size = tokens // NG
    at = jnp.stack([block, head, start, start + block * size]).astype(jnp.int32)
    whole = lambda shape: pl.BlockSpec(shape, lambda i, at: (0,) * len(shape))
    part = pl.BlockSpec((size, width), lambda i, at: (at[0], at[1]))
    outs = ((NG, tokens, width), (NZ, size, 2 * width))
    return pl.pallas_call(
        prepare_kernel,
        grid_spec=pltpu.PrefetchScalarGridSpec(
            num_scalar_prefetch=1,
            grid=(1,),
            in_specs=[whole((tokens, width)), part, part, whole((1, width)), whole((1, width))],
            out_specs=[whole(shape) for shape in outs],
        ),
        out_shape=[jax.ShapeDtypeStruct(shape, BF) for shape in outs],
        name="prepare",
    )(at, queries, keys, values, query_gain[None, :], key_gain[None, :])


def split3(x):
    hi = x.astype(BF)
    rest = x - hi.astype(F32)
    mid = rest.astype(BF)
    lo = (rest - mid.astype(F32)).astype(BF)
    return hi, mid, lo


def attend_kernel(q_ref, own_ref, other_ref, out_ref):
    width = q_ref.shape[2]
    factor = width ** (-0.5) * LOG2E
    keys = jnp.concatenate([own_ref[:, :width], other_ref[:, :width]], axis=0)
    values = jnp.concatenate([own_ref[:, width:], other_ref[:, width:]], axis=0)
    scores = lax.dot_general(
        keys, q_ref[0], (((1,), (1,)), ((), ())), preferred_element_type=F32
    )
    top = jnp.max(scores, axis=0, keepdims=True)
    weights = jnp.exp2((scores - top) * factor).astype(BF)
    total = jnp.sum(weights.astype(F32), axis=0, keepdims=True)
    summed = lax.dot_general(
        values, weights, (((0,), (0,)), ((), ())), preferred_element_type=F32
    )
    out_ref[0, :width, :] = (summed / total).astype(BF)
    cols = summed.shape[1]
    row = lax.broadcasted_iota(jnp.int32, (STAT_ROWS, cols), 0)
    stats = jnp.zeros((STAT_ROWS, cols), F32)
    for i, part in enumerate(split3(top * factor) + split3(total)):
        stats = jnp.where(row == i, part.astype(F32), stats)
    out_ref[0, width:, :] = stats.astype(BF)


def attend(q8, own, other):
    heads, rows, width = q8.shape
    return pl.pallas_call(
        attend_kernel,
        grid=(heads,),
        in_specs=[
            pl.BlockSpec((1, rows, width), lambda h: (h, 0, 0)),
            pl.BlockSpec(own.shape, lambda h: (0, 0)),
            pl.BlockSpec(other.shape, lambda h: (0, 0)),
        ],
        out_specs=pl.BlockSpec((1, width + STAT_ROWS, rows), lambda h: (h, 0, 0)),
        out_shape=jax.ShapeDtypeStruct((heads, width + STAT_ROWS, rows), BF),
        name="attend",
    )(q8, own, other)


def combine_kernel(parts_ref, out_ref):
    count = parts_ref.shape[0]
    width = out_ref.shape[1]
    tops, totals = [], []
    for j in range(count):
        s = parts_ref[j, width:, :].astype(F32)
        tops.append(s[0:1] + s[1:2] + s[2:3])
        totals.append(s[3:4] + s[4:5] + s[5:6])
    top = tops[0]
    for j in range(1, count):
        top = jnp.maximum(top, tops[j])
    shares = [totals[j] * jnp.exp2(tops[j] - top) for j in range(count)]
    whole = sum(shares[1:], shares[0])
    acc = jnp.zeros(out_ref.shape[1:], F32)
    for j in range(count):
        acc = acc + parts_ref[j, :width, :].astype(F32) * (shares[j] / whole)
    done = acc.astype(BF)
    for i in range(out_ref.shape[0]):
        out_ref[i] = done


def combine(parts):
    width = parts.shape[1] - STAT_ROWS
    return pl.pallas_call(
        combine_kernel,
        out_shape=jax.ShapeDtypeStruct((NT, width, parts.shape[2]), BF),
        name="combine",
    )(parts)


def deal_kernel(classes_ref, out_ref):
    for i, k in enumerate(COLOURS):
        out_ref[i] = classes_ref[k]


def deal(classes):
    return pl.pallas_call(
        deal_kernel,
        out_shape=jax.ShapeDtypeStruct((NT, *classes.shape[1:]), BF),
        name="deal",
    )(classes)


def experts_kernel(rows_ref, *refs):
    pieces, out_ref, held, acc, sems = refs[:-4], refs[-4], refs[-3], refs[-2], refs[-1]
    count, depth, _ = held.shape
    waits = [[] for _ in range(count)]
    chunk, at = 0, 0
    for i, piece in enumerate(pieces):
        size = piece.shape[0]
        copy = pltpu.make_async_copy(piece, held.at[chunk, pl.ds(at, size), :], sems.at[i])
        copy.start()
        waits[chunk].append(copy)
        at += size
        if at == depth:
            chunk, at = chunk + 1, 0
    units = held.shape[2] // 3
    for pair in range(count // 2):
        hidden, down = [], []
        for k in (2 * pair, 2 * pair + 1):
            for copy in waits[k]:
                copy.wait()
            both = jnp.dot(
                rows_ref[...], held[k, :, : 2 * units], preferred_element_type=F32
            )
            gate, upper = both[:, :units], both[:, units:]
            hidden.append((gate / (1.0 + jnp.exp(-gate)) * upper).astype(BF))
            down.append(held[k, :, 2 * units :])
        part = lax.dot_general(
            jnp.concatenate(hidden, axis=1),
            jnp.concatenate(down, axis=1),
            (((1,), (1,)), ((), ())),
            preferred_element_type=F32,
        )
        if pair == 0:
            acc[...] = part
        elif pair < count // 2 - 1:
            acc[...] += part
        else:
            out_ref[...] = (acc[...] + part).astype(BF)


def experts(rows, pieces):
    depth = sum(p.shape[0] for p in pieces) // 8
    width = pieces[0].shape[1]
    return pl.pallas_call(
        experts_kernel,
        in_specs=[pl.BlockSpec(memory_space=pltpu.VMEM)]
        + [pl.BlockSpec(memory_space=pl.ANY)] * len(pieces),
        out_specs=pl.BlockSpec(memory_space=pltpu.VMEM),
        out_shape=jax.ShapeDtypeStruct(rows.shape, BF),
        scratch_shapes=[
            pltpu.VMEM((8, depth, width), BF),
            pltpu.VMEM(rows.shape, F32),
            pltpu.SemaphoreType.DMA((len(pieces),)),
        ],
        compiler_params=pltpu.CompilerParams(vmem_limit_bytes=40 * 1024 * 1024),
        name="experts",
    )(rows, *pieces)


def local(
    queries,
    keys,
    values,
    query_gain,
    key_gain,
    out_proj,
    expert_norm_scale,
    residual,
    routes,
    route_weights,
    w_gate,
    w_up,
    w_down,
):
    width = query_gain.shape[0]
    tok_sp = queries.shape[0]
    tok_dev, depth = residual.shape
    top = routes.shape[1]
    z, c = lax.axis_index("z"), lax.axis_index("c")
    yh, yl, x = lax.axis_index("yh"), lax.axis_index("yl"), lax.axis_index("x")
    start = (z * NC + c) * tok_sp

    q8, kv = prepare(
        queries, keys, values, query_gain, key_gain, yl * NX + x, yh, start
    )
    q8 = exchange(q8, GROUP)
    q8, kv = lax.optimization_barrier((q8, kv))
    kv_mine = exchange(kv, "z").reshape(-1, 2 * width)
    kv_other = swap_cores(kv_mine)

    units = w_gate.shape[2] // 2
    pieces = []
    for s, axis in ((slice(0, units), "x"), (slice(units, 2 * units), ("yh", "yl"))):
        pack = jnp.concatenate([w_gate[0][:, s], w_up[0][:, s], w_down[0][s, :].T], axis=1)
        left, right = ring(pack, axis, 1), ring(pack, axis, -1)
        far = ring(left, axis, 1)
        pieces += [pack, left, right, far]

    parts = attend(q8, kv_mine, kv_other)
    parts = exchange(parts, GROUP)
    attn_all = exchange(combine(parts), TP).reshape(NT * width, tok_sp)
    columns = lax.dot_general(
        attn_all, out_proj, (((0,), (0,)), ((), ())), preferred_element_type=F32
    ).astype(BF)
    projected = lax.all_to_all(columns, TP, split_axis=0, concat_axis=1, tiled=True)
    mixed = (residual.astype(F32) + projected.astype(F32)).astype(BF)
    mixed_f = mixed.astype(F32)
    normed = (
        mixed_f
        * lax.rsqrt(jnp.mean(mixed_f * mixed_f, axis=-1, keepdims=True) + EPS)
        * expert_norm_scale
    ).astype(BF)

    cap = max(2, 2 * tok_dev * top // (NZ * NC))
    tok = jnp.arange(tok_dev, dtype=jnp.int32)
    before = tok[None, :] < tok[:, None]
    place = jnp.arange(NZ * NC * cap, dtype=jnp.int32)
    rel, zc_slot = place // (NZ * cap), place % (NZ * cap)
    expert_of = (zc_slot // cap) * NC + (c + rel) % NC
    slot_of = zc_slot % cap
    hits = []
    for k in range(top):
        mine = routes[:, k]
        slot = sum(
            jnp.sum(
                ((mine[:, None] == routes[:, j][None, :]) & before).astype(jnp.int32), axis=1
            )
            for j in range(top)
        )
        hits.append(
            (mine[:, None] == expert_of[None, :]) & (slot[:, None] == slot_of[None, :])
        )
    selector = sum(h.astype(BF) for h in hits)
    sent = lax.dot_general(
        selector, normed, (((0,), (0,)), ((), ())), preferred_element_type=F32
    ).astype(BF)
    half = NZ * cap
    from_other = swap_cores(sent[half:])
    outgoing = jnp.concatenate(
        [sent[:half].reshape(NZ, cap, depth), from_other.reshape(NZ, cap, depth)], axis=1
    )
    arrived = exchange(outgoing, "z")

    rows = exchange(deal(arrived.reshape(4, NZ * NC * cap // 4, depth)), TP)
    partial = experts(rows.reshape(-1, depth), pieces).reshape(rows.shape)
    back = exchange(partial, TP)
    expert_out = jnp.stack(
        [
            sum(back[i].astype(F32) for i in range(NT) if COLOURS[i] == k).astype(BF)
            for k in range(4)
        ]
    ).reshape(NZ, NC * cap, depth)
    returned = exchange(expert_out, "z")
    for_other = swap_cores(returned[:, cap:].reshape(half, depth))
    picked_from = jnp.concatenate([returned[:, :cap].reshape(half, depth), for_other], axis=0)
    moe = sum(
        jnp.dot(hits[k].astype(BF), picked_from, preferred_element_type=F32)
        * route_weights[:, k][:, None]
        for k in range(top)
    )
    return (mixed_f + moe).astype(BF)


def solution(mesh):
    fine = Mesh(
        mesh.devices.reshape(NZ, NC, NYH, NYL, NX), ("z", "c", "yh", "yl", "x")
    )
    sp, both = ("z", "c"), ("z", "c", "yh", "yl", "x")
    placed = (
        P(sp, TP),
        P(sp, None),
        P(sp, None),
        P(),
        P(),
        P(None, TP),
        P(),
        P(both, None),
        P(both, None),
        P(both, None),
        P(sp, None, TP),
        P(sp, None, TP),
        P(sp, TP, None),
    )
    return jax.shard_map(
        local, mesh=fine, in_specs=placed, out_specs=P(both, None), check_vma=False
    )
```

profile of v0, /device:TPU:1, one launch (start us, length us, event | category | flops | bytes accessed | tf_op | source)
XLA Modules:
  0.0 272.6 jit_solution(45921941527996304)
XLA Ops:
  0.7 3.1 %prepare.1 = (bf16[8,256,128]{2,1,0:T(8,128)(2,1)}, bf16[16,32,256]{2,1,0:T(8,128)(2,1)}) custom-call(s32[4]{0:T(128)} %pad_add_fusion.at_ref, bf16[256,128]{1,0:T(8,128)(2,1)} %q_ref.1, bf16[256,256]{1,0:T(8,128)(2,1)} %k_ref.1, bf16[256,256]{1,0:T(8,128)(2,1)} %v_ref.1, f32[1,128]{1,0:T(1,128)} %bitcast.49, f32[1,128]{1,0:T(1,128)} %bitcast.50), custom_call_target="tpu_custom_call" | custom-call | tf_op jit(solution)/shard_map/prepare/pallas_call | solution.py:74
  3.8 13.5 %all_to_all.53.q_ref = bf16[8,256,128]{2,1,0:T(8,128)(2,1)} all-to-all(bf16[8,256,128]{2,1,0:T(8,128)(2,1)} %get-tuple-element.9), channel_id=1, replica_groups=mesh['z'=16,'c'=2,'yh'=2,'yl'=2,'x'=4] {'yl','x'}, dimensions={0} | all-to-all | bytes 1048576 | tf_op jit(solution)/shard_map/all_to_all | solution.py:29
  17.2 29.5 %all_to_all.54 = bf16[16,32,256]{2,1,0:T(8,128)(2,1)S(1)} all-to-all(bf16[16,32,256]{2,1,0:T(8,128)(2,1)} %get-tuple-element.12), channel_id=1, replica_groups=mesh['z'=16,'c'=2,'yh'=2,'yl'=2,'x'=4] {'z'}, dimensions={0} | all-to-all | bytes 524288 | tf_op jit(solution)/shard_map/all_to_all | solution.py:29
  46.7 8.7 %collective-permute-start = (bf16[512,256]{1,0:T(8,128)(2,1)S(1)}, bf16[512,256]{1,0:T(8,128)(2,1)S(1)}, u32[]{:S(2)}, u32[]{:S(2)}) collective-permute-start(bf16[512,256]{1,0:T(8,128)(2,1)S(1)} %bitcast.45), channel_id=1, source_target_pairs={{0,16},{16,0},{1,17},{17,1},{2,18},{18,2},{3,19},{19,3},{4,20},{20... | collective-permute-start | bytes 786440 | tf_op jit(solution)/shard_map/ppermute | solution.py:33
  55.4 1.1 collective-permute-done.other_ref
  56.5 0.7 copy-done.5
  57.2 8.4 %attend.1 = bf16[8,144,256]{2,1,0:T(8,128)(2,1)} custom-call(bf16[8,256,128]{2,1,0:T(8,128)(2,1)} %all_to_all.53.q_ref, bf16[512,256]{1,0:T(8,128)(2,1)} %bitcast.46, bf16[512,256]{1,0:T(8,128)(2,1)} %copy-done.5), custom_call_target="tpu_custom_call" | custom-call | tf_op jit(solution)/shard_map/attend/pallas_call | solution.py:120
  65.7 3.5 %all-to-all-start.2 = ((bf16[8,144,256]{2,1,0:T(8,128)(2,1)}), bf16[8,144,256]{2,1,0:T(8,128)(2,1)S(1)}, u32[]{:S(2)}, u32[]{:S(2)}) async-start(bf16[8,144,256]{2,1,0:T(8,128)(2,1)} %attend.1), calls=%async_computation.2 | async-start | bytes 1179648 | tf_op jit(solution)/shard_map/all_to_all | solution.py:29
  69.2 1.5 fusion.37
  70.7 9.3 %all-to-all-done.2.parts_ref = bf16[8,144,256]{2,1,0:T(8,128)(2,1)S(1)} async-done(((bf16[8,144,256]{2,1,0:T(8,128)(2,1)}), bf16[8,144,256]{2,1,0:T(8,128)(2,1)S(1)}, u32[]{:S(2)}, u32[]{:S(2)}) %all-to-all-start.2) | async-done | bytes 589856 | tf_op jit(solution)/shard_map/all_to_all | solution.py:29
  80.1 0.8 copy-done.1
  80.9 2.2 combine.1
  83.2 4.6 %all-to-all-start.3 = ((bf16[16,128,256]{2,1,0:T(8,128)(2,1)}), bf16[16,128,256]{2,1,0:T(8,128)(2,1)S(1)}, u32[]{:S(2)}, u32[]{:S(2)}) async-start(bf16[16,128,256]{2,1,0:T(8,128)(2,1)} %combine.1), calls=%async_computation.3 | async-start | bytes 2097152 | tf_op jit(solution)/shard_map/all_to_all | solution.py:29
  87.8 2.1 fusion.39
  89.9 1.0 copy.20
  90.9 1.6 pad_maximum_fusion.refs_0_
  92.5 3.3 %collective-permute-start.2 = (bf16[2048,384]{1,0:T(8,128)(2,1)S(1)}, bf16[2048,384]{1,0:T(8,128)(2,1)}, u32[]{:S(2)}, u32[]{:S(2)}) collective-permute-start(bf16[2048,384]{1,0:T(8,128)(2,1)S(1)} %pad_maximum_fusion.refs_0_), channel_id=1, source_target_pairs={{0,1},{1,2},{2,3},{3,0},{4,5},{5,6},{6,7},{7,4},{8,9},{9,10},{10,1... | collective-permute-start | bytes 4718600 | tf_op jit(solution)/shard_map/ppermute | solution.py:37
  95.8 2.0 copy.21
  97.8 2.7 %pad_maximum_fusion.1.refs_4_ = bf16[2048,384]{1,0:T(8,128)(2,1)} fusion(bf16[2048,128]{1,0:T(8,128)(2,1)} %bitcast.43, bf16[2048,128]{1,0:T(8,128)(2,1)} %get-tuple-element.40, bf16[2048,128]{1,0:T(8,128)(2,1)} %get-tuple-element.23), kind=kLoop, calls=%fused_computation.7 | loop fusion | flops 4718592 | bytes 3145728 | tf_op jit(solution)/shard_map/concatenate | solution.py:269
  100.5 3.2 %collective-permute-start.5 = (bf16[2048,384]{1,0:T(8,128)(2,1)}, bf16[2048,384]{1,0:T(8,128)(2,1)}, u32[]{:S(2)}, u32[]{:S(2)}) collective-permute-start(bf16[2048,384]{1,0:T(8,128)(2,1)} %pad_maximum_fusion.1.refs_4_), channel_id=1, source_target_pairs={{0,4},{4,8},{8,12},{12,0},{1,5},{5,9},{9,13},{13,1},{2,6},{6,10},{... | collective-permute-start | bytes 4718600 | tf_op jit(solution)/shard_map/ppermute | solution.py:37
  104.1 1.1 convolution_convert_fusion.1
  105.2 5.9 %all-to-all-start.4 = ((bf16[16,16,128]{2,1,0:T(8,128)(2,1)}), bf16[16,16,128]{2,1,0:T(8,128)(2,1)S(1)}, u32[]{:S(2)}, u32[]{:S(2)}) async-start(bf16[16,16,128]{2,1,0:T(8,128)(2,1)} %bitcast.8), calls=%async_computation.4 | async-start | bytes 131072 | tf_op jit(solution)/shard_map/all_to_all | solution.py:280
  111.1 28.9 %all-to-all-done.4 = bf16[16,16,128]{2,1,0:T(8,128)(2,1)S(1)} async-done(((bf16[16,16,128]{2,1,0:T(8,128)(2,1)}), bf16[16,16,128]{2,1,0:T(8,128)(2,1)S(1)}, u32[]{:S(2)}, u32[]{:S(2)}) %all-to-all-start.4) | async-done | bytes 65568 | tf_op jit(solution)/shard_map/all_to_all | solution.py:280
  140.5 4.4 %collective-permute-start.1 = (bf16[32,2048]{1,0:T(8,128)(2,1)S(1)}, bf16[32,2048]{1,0:T(8,128)(2,1)S(1)}, u32[]{:S(2)}, u32[]{:S(2)}) collective-permute-start(bf16[32,2048]{1,0:T(8,128)(2,1)S(1)} %get-tuple-element.32), channel_id=1, source_target_pairs={{0,16},{16,0},{1,17},{17,1},{2,18},{18,2},{3,19},{19,3},{4,20},{20... | collective-permute-start | bytes 393224 | tf_op jit(solution)/shard_map/ppermute | solution.py:33
  144.9 0.9 collective-permute-done.1
  145.9 1.0 pad_maximum_fusion.2
  146.9 5.3 %all-to-all-start.5 = ((bf16[16,4,2048]{2,1,0:T(4,128)(2,1)}), bf16[16,4,2048]{2,1,0:T(4,128)(2,1)S(1)}, u32[]{:S(2)}, u32[]{:S(2)}) async-start(bf16[16,4,2048]{2,1,0:T(4,128)(2,1)} %pad_maximum_fusion.2), calls=%async_computation.5 | async-start | bytes 524288 | tf_op jit(solution)/shard_map/all_to_all | solution.py:29
  152.2 3.4 %collective-permute-start.3 = (bf16[2048,384]{1,0:T(8,128)(2,1)S(1)}, bf16[2048,384]{1,0:T(8,128)(2,1)}, u32[]{:S(2)}, u32[]{:S(2)}) collective-permute-start(bf16[2048,384]{1,0:T(8,128)(2,1)S(1)} %pad_maximum_fusion.refs_0_), channel_id=1, source_target_pairs={{0,3},{1,0},{2,1},{3,2},{4,7},{5,4},{6,5},{7,6},{8,11},{9,8},{10,9... | collective-permute-start | bytes 4718600 | tf_op jit(solution)/shard_map/ppermute | solution.py:37
  155.6 2.2 collective-permute-start.6
  157.9 1.9 collective-permute-start.4
  159.8 3.1 %collective-permute-start.7 = (bf16[2048,384]{1,0:T(8,128)(2,1)}, bf16[2048,384]{1,0:T(8,128)(2,1)}, u32[]{:S(2)}, u32[]{:S(2)}) collective-permute-start(bf16[2048,384]{1,0:T(8,128)(2,1)} %collective-permute-done.5.refs_5_), channel_id=1, source_target_pairs={{0,4},{4,8},{8,12},{12,0},{1,5},{5,9},{9,13},{13,1},{2,6},{6,10},{... | collective-permute-start | bytes 4718600 | tf_op jit(solution)/shard_map/ppermute | solution.py:37
  162.9 3.4 %all-to-all-done.5 = bf16[16,4,2048]{2,1,0:T(4,128)(2,1)S(1)} async-done(((bf16[16,4,2048]{2,1,0:T(4,128)(2,1)}), bf16[16,4,2048]{2,1,0:T(4,128)(2,1)S(1)}, u32[]{:S(2)}, u32[]{:S(2)}) %all-to-all-start.5) | async-done | bytes 262176 | tf_op jit(solution)/shard_map/all_to_all | solution.py:29
  166.3 0.8 reshape.124.classes_ref
  167.0 2.0 deal.1
  169.0 4.1 %all-to-all-start.6 = ((bf16[16,16,2048]{2,1,0:T(8,128)(2,1)}), bf16[16,16,2048]{2,1,0:T(8,128)(2,1)S(1)}, u32[]{:S(2)}, u32[]{:S(2)}) async-start(bf16[16,16,2048]{2,1,0:T(8,128)(2,1)} %deal.1), calls=%async_computation.6 | async-start | bytes 2097152 | tf_op jit(solution)/shard_map/all_to_all | solution.py:29
  173.1 16.4 %collective-permute-done.3.refs_2_ = bf16[2048,384]{1,0:T(8,128)(2,1)} collective-permute-done((bf16[2048,384]{1,0:T(8,128)(2,1)S(1)}, bf16[2048,384]{1,0:T(8,128)(2,1)}, u32[]{:S(2)}, u32[]{:S(2)}) %collective-permute-start.3) | collective-permute-done | bytes 1572896 | tf_op jit(solution)/shard_map/ppermute | solution.py:37
  189.5 3.3 %collective-permute-done.6.refs_6_ = bf16[2048,384]{1,0:T(8,128)(2,1)} collective-permute-done((bf16[2048,384]{1,0:T(8,128)(2,1)}, bf16[2048,384]{1,0:T(8,128)(2,1)}, u32[]{:S(2)}, u32[]{:S(2)}) %collective-permute-start.6) | collective-permute-done | bytes 1572896 | tf_op jit(solution)/shard_map/ppermute | solution.py:37
  192.9 3.5 %collective-permute-done.4.refs_3_ = bf16[2048,384]{1,0:T(8,128)(2,1)} collective-permute-done((bf16[2048,384]{1,0:T(8,128)(2,1)}, bf16[2048,384]{1,0:T(8,128)(2,1)}, u32[]{:S(2)}, u32[]{:S(2)}) %collective-permute-start.4) | collective-permute-done | bytes 1572896 | tf_op jit(solution)/shard_map/ppermute | solution.py:37
  196.3 7.0 %collective-permute-done.7.refs_7_ = bf16[2048,384]{1,0:T(8,128)(2,1)} collective-permute-done((bf16[2048,384]{1,0:T(8,128)(2,1)}, bf16[2048,384]{1,0:T(8,128)(2,1)}, u32[]{:S(2)}, u32[]{:S(2)}) %collective-permute-start.7) | collective-permute-done | bytes 1572896 | tf_op jit(solution)/shard_map/ppermute | solution.py:37
  203.4 4.2 %all-to-all-done.6 = bf16[16,16,2048]{2,1,0:T(8,128)(2,1)S(1)} async-done(((bf16[16,16,2048]{2,1,0:T(8,128)(2,1)}), bf16[16,16,2048]{2,1,0:T(8,128)(2,1)S(1)}, u32[]{:S(2)}, u32[]{:S(2)}) %all-to-all-start.6) | async-done | bytes 1048608 | tf_op jit(solution)/shard_map/all_to_all | solution.py:29
  207.6 8.0 %experts.1 = bf16[256,2048]{1,0:T(8,128)(2,1)S(1)} custom-call(bf16[256,2048]{1,0:T(8,128)(2,1)S(1)} %bitcast.40, bf16[2048,384]{1,0:T(8,128)(2,1)S(1)} %pad_maximum_fusion.refs_0_, bf16[2048,384]{1,0:T(8,128)(2,1)} %collective-permute-done.2.refs_1_, bf16[2048,384]{1,0:T(8,128)(2,1)} %collective-permute-done.3.refs_2_, ...), custom_call_target="tpu_custom_call" | custom-call | tf_op jit(solution)/shard_map/experts/pallas_call | solution.py:219
  215.6 20.1 %all_to_all.55 = bf16[16,16,2048]{2,1,0:T(8,128)(2,1)S(1)} all-to-all(bf16[16,16,2048]{2,1,0:T(8,128)(2,1)S(1)} %bitcast.41), channel_id=1, replica_groups=mesh['z'=16,'c'=2,'yh'=2,'yl'=2,'x'=4] {'yh','yl','x'}, dimensions={0} | all-to-all | bytes 2097152 | tf_op jit(solution)/shard_map/all_to_all | solution.py:29
  235.9 0.8 reshape.127
  236.7 10.9 %all-to-all-start.8 = ((bf16[16,4,2048]{2,1,0:T(4,128)(2,1)}), bf16[16,4,2048]{2,1,0:T(4,128)(2,1)S(1)}, u32[]{:S(2)}, u32[]{:S(2)}) async-start(bf16[16,4,2048]{2,1,0:T(4,128)(2,1)} %reshape.127), calls=%async_computation.8 | async-start | bytes 524288 | tf_op jit(solution)/shard_map/all_to_all | solution.py:29
  247.6 12.7 %all-to-all-done.8 = bf16[16,4,2048]{2,1,0:T(4,128)(2,1)S(1)} async-done(((bf16[16,4,2048]{2,1,0:T(4,128)(2,1)}), bf16[16,4,2048]{2,1,0:T(4,128)(2,1)S(1)}, u32[]{:S(2)}, u32[]{:S(2)}) %all-to-all-start.8) | async-done | bytes 262176 | tf_op jit(solution)/shard_map/all_to_all | solution.py:29
  260.6 9.9 %collective-permute-start.8 = (bf16[32,2048]{1,0:T(8,128)(2,1)S(1)}, bf16[32,2048]{1,0:T(8,128)(2,1)S(1)}, u32[]{:S(2)}, u32[]{:S(2)}) collective-permute-start(bf16[32,2048]{1,0:T(8,128)(2,1)S(1)} %reshape.129), channel_id=1, source_target_pairs={{0,16},{16,0},{1,17},{17,1},{2,18},{18,2},{3,19},{19,3},{4,20},{20... | collective-permute-start | bytes 393224 | tf_op jit(solution)/shard_map/ppermute | solution.py:33
  270.6 0.9 collective-permute-done.8
  271.8 0.9 fusion.2
  (42 shorter events, 2.3 us)
Async XLA Ops:
  0.0 104.0 %copy-start = (bf16[2048,128]{1,0:T(8,128)(2,1)S(1)}, bf16[2048,128]{1,0:T(8,128)(2,1)}, u32[]{:S(2)}) copy-start(bf16[2048,128]{1,0:T(8,128)(2,1)} %param.18) | copy-start | bytes 1572868
  17.2 52.0 %copy-start.3 = (bf16[1,2048,256]{2,1,0:T(8,128)(2,1)S(1)}, bf16[1,2048,256]{2,1,0:T(8,128)(2,1)}, u32[]{:S(2)}) copy-start(bf16[1,2048,256]{2,1,0:T(8,128)(2,1)} %param.23) | copy-start | bytes 3145732
  17.2 52.0 %copy-start.4 = (bf16[1,2048,256]{2,1,0:T(8,128)(2,1)S(1)}, bf16[1,2048,256]{2,1,0:T(8,128)(2,1)}, u32[]{:S(2)}) copy-start(bf16[1,2048,256]{2,1,0:T(8,128)(2,1)} %param.24) | copy-start | bytes 3145732
  46.7 9.8 %copy-start.2 = (bf16[16,32,256]{2,1,0:T(8,128)(2,1)}, bf16[16,32,256]{2,1,0:T(8,128)(2,1)S(1)}, u32[]{:S(2)}) copy-start(bf16[16,32,256]{2,1,0:T(8,128)(2,1)S(1)} %all_to_all.54) | copy-start | bytes 786436
  46.7 9.8 %collective-permute-start = (bf16[512,256]{1,0:T(8,128)(2,1)S(1)}, bf16[512,256]{1,0:T(8,128)(2,1)S(1)}, u32[]{:S(2)}, u32[]{:S(2)}) collective-permute-start(bf16[512,256]{1,0:T(8,128)(2,1)S(1)} %bitcast.45), channel_id=1, source_target_pairs={{0,16},{16,0},{1,17},{17,1},{2,18},{18,2},{3,19},{19,3},{4,20},{20... | collective-permute-start | bytes 786440 | tf_op jit(solution)/shard_map/ppermute | solution.py:33
  56.5 0.7 copy-start.5
  65.7 14.4 %all-to-all-start.2 = ((bf16[8,144,256]{2,1,0:T(8,128)(2,1)}), bf16[8,144,256]{2,1,0:T(8,128)(2,1)S(1)}, u32[]{:S(2)}, u32[]{:S(2)}) async-start(bf16[8,144,256]{2,1,0:T(8,128)(2,1)} %attend.1), calls=%async_computation.2 | async-start | bytes 1179648 | tf_op jit(solution)/shard_map/all_to_all | solution.py:29
  80.1 0.8 copy-start.1
  83.2 20.9 %all-to-all-start.3 = ((bf16[16,128,256]{2,1,0:T(8,128)(2,1)}), bf16[16,128,256]{2,1,0:T(8,128)(2,1)S(1)}, u32[]{:S(2)}, u32[]{:S(2)}) async-start(bf16[16,128,256]{2,1,0:T(8,128)(2,1)} %combine.1), calls=%async_computation.3 | async-start | bytes 2097152 | tf_op jit(solution)/shard_map/all_to_all | solution.py:29
  92.5 65.4 %collective-permute-start.2 = (bf16[2048,384]{1,0:T(8,128)(2,1)S(1)}, bf16[2048,384]{1,0:T(8,128)(2,1)}, u32[]{:S(2)}, u32[]{:S(2)}) collective-permute-start(bf16[2048,384]{1,0:T(8,128)(2,1)S(1)} %pad_maximum_fusion.refs_0_), channel_id=1, source_target_pairs={{0,1},{1,2},{2,3},{3,0},{4,5},{5,6},{6,7},{7,4},{8,9},{9,10},{10,1... | collective-permute-start | bytes 4718600 | tf_op jit(solution)/shard_map/ppermute | solution.py:37
  97.8 6.0 %copy-start.8 = (s32[16,2]{0,1:T(2,128)S(1)}, s32[16,2]{0,1:T(2,128)}, u32[]{:S(2)}) copy-start(s32[16,2]{0,1:T(2,128)} %param.21) | copy-start | bytes 388
  100.5 39.4 %copy-start.6 = (bf16[16,2048]{1,0:T(8,128)(2,1)S(1)}, bf16[16,2048]{1,0:T(8,128)(2,1)}, u32[]{:S(2)}) copy-start(bf16[16,2048]{1,0:T(8,128)(2,1)} %param.20) | copy-start | bytes 196612
  100.5 39.5 %copy-start.7 = (f32[2048]{0:T(1024)S(1)}, f32[2048]{0:T(1024)}, u32[]{:S(2)}) copy-start(f32[2048]{0:T(1024)} %param.19) | copy-start | bytes 24580
  100.5 59.3 %collective-permute-start.5 = (bf16[2048,384]{1,0:T(8,128)(2,1)}, bf16[2048,384]{1,0:T(8,128)(2,1)}, u32[]{:S(2)}, u32[]{:S(2)}) collective-permute-start(bf16[2048,384]{1,0:T(8,128)(2,1)} %pad_maximum_fusion.1.refs_4_), channel_id=1, source_target_pairs={{0,4},{4,8},{8,12},{12,0},{1,5},{5,9},{9,13},{13,1},{2,6},{6,10},{... | collective-permute-start | bytes 4718600 | tf_op jit(solution)/shard_map/ppermute | solution.py:37
  105.2 34.8 %all-to-all-start.4 = ((bf16[16,16,128]{2,1,0:T(8,128)(2,1)}), bf16[16,16,128]{2,1,0:T(8,128)(2,1)S(1)}, u32[]{:S(2)}, u32[]{:S(2)}) async-start(bf16[16,16,128]{2,1,0:T(8,128)(2,1)} %bitcast.8), calls=%async_computation.4 | async-start | bytes 131072 | tf_op jit(solution)/shard_map/all_to_all | solution.py:280
  140.5 5.3 %collective-permute-start.1 = (bf16[32,2048]{1,0:T(8,128)(2,1)S(1)}, bf16[32,2048]{1,0:T(8,128)(2,1)S(1)}, u32[]{:S(2)}, u32[]{:S(2)}) collective-permute-start(bf16[32,2048]{1,0:T(8,128)(2,1)S(1)} %get-tuple-element.32), channel_id=1, source_target_pairs={{0,16},{16,0},{1,17},{17,1},{2,18},{18,2},{3,19},{19,3},{4,20},{20... | collective-permute-start | bytes 393224 | tf_op jit(solution)/shard_map/ppermute | solution.py:33
  146.9 19.4 %all-to-all-start.5 = ((bf16[16,4,2048]{2,1,0:T(4,128)(2,1)}), bf16[16,4,2048]{2,1,0:T(4,128)(2,1)S(1)}, u32[]{:S(2)}, u32[]{:S(2)}) async-start(bf16[16,4,2048]{2,1,0:T(4,128)(2,1)} %pad_maximum_fusion.2), calls=%async_computation.5 | async-start | bytes 524288 | tf_op jit(solution)/shard_map/all_to_all | solution.py:29
  152.2 37.3 %collective-permute-start.3 = (bf16[2048,384]{1,0:T(8,128)(2,1)S(1)}, bf16[2048,384]{1,0:T(8,128)(2,1)}, u32[]{:S(2)}, u32[]{:S(2)}) collective-permute-start(bf16[2048,384]{1,0:T(8,128)(2,1)S(1)} %pad_maximum_fusion.refs_0_), channel_id=1, source_target_pairs={{0,3},{1,0},{2,1},{3,2},{4,7},{5,4},{6,5},{7,6},{8,11},{9,8},{10,9... | collective-permute-start | bytes 4718600 | tf_op jit(solution)/shard_map/ppermute | solution.py:37
  155.6 37.2 %collective-permute-start.6 = (bf16[2048,384]{1,0:T(8,128)(2,1)}, bf16[2048,384]{1,0:T(8,128)(2,1)}, u32[]{:S(2)}, u32[]{:S(2)}) collective-permute-start(bf16[2048,384]{1,0:T(8,128)(2,1)} %pad_maximum_fusion.1.refs_4_), channel_id=1, source_target_pairs={{0,12},{4,0},{8,4},{12,8},{1,13},{5,1},{9,5},{13,9},{2,14},{6,2},{... | collective-permute-start | bytes 4718600 | tf_op jit(solution)/shard_map/ppermute | solution.py:37
  157.9 38.5 %collective-permute-start.4 = (bf16[2048,384]{1,0:T(8,128)(2,1)}, bf16[2048,384]{1,0:T(8,128)(2,1)}, u32[]{:S(2)}, u32[]{:S(2)}) collective-permute-start(bf16[2048,384]{1,0:T(8,128)(2,1)} %collective-permute-done.2.refs_1_), channel_id=1, source_target_pairs={{0,1},{1,2},{2,3},{3,0},{4,5},{5,6},{6,7},{7,4},{8,9},{9,10},{10,1... | collective-permute-start | bytes 4718600 | tf_op jit(solution)/shard_map/ppermute | solution.py:37
  159.8 43.5 %collective-permute-start.7 = (bf16[2048,384]{1,0:T(8,128)(2,1)}, bf16[2048,384]{1,0:T(8,128)(2,1)}, u32[]{:S(2)}, u32[]{:S(2)}) collective-permute-start(bf16[2048,384]{1,0:T(8,128)(2,1)} %collective-permute-done.5.refs_5_), channel_id=1, source_target_pairs={{0,4},{4,8},{8,12},{12,0},{1,5},{5,9},{9,13},{13,1},{2,6},{6,10},{... | collective-permute-start | bytes 4718600 | tf_op jit(solution)/shard_map/ppermute | solution.py:37
  169.0 38.6 %all-to-all-start.6 = ((bf16[16,16,2048]{2,1,0:T(8,128)(2,1)}), bf16[16,16,2048]{2,1,0:T(8,128)(2,1)S(1)}, u32[]{:S(2)}, u32[]{:S(2)}) async-start(bf16[16,16,2048]{2,1,0:T(8,128)(2,1)} %deal.1), calls=%async_computation.6 | async-start | bytes 2097152 | tf_op jit(solution)/shard_map/all_to_all | solution.py:29
  235.7 11.9 %copy-start.9 = (f32[16,2]{0,1:T(2,128)S(1)}, f32[16,2]{0,1:T(2,128)}, u32[]{:S(2)}) copy-start(f32[16,2]{0,1:T(2,128)} %param.22) | copy-start | bytes 388
  236.7 23.7 %all-to-all-start.8 = ((bf16[16,4,2048]{2,1,0:T(4,128)(2,1)}), bf16[16,4,2048]{2,1,0:T(4,128)(2,1)S(1)}, u32[]{:S(2)}, u32[]{:S(2)}) async-start(bf16[16,4,2048]{2,1,0:T(4,128)(2,1)} %reshape.127), calls=%async_computation.8 | async-start | bytes 524288 | tf_op jit(solution)/shard_map/all_to_all | solution.py:29
  260.6 10.9 %collective-permute-start.8 = (bf16[32,2048]{1,0:T(8,128)(2,1)S(1)}, bf16[32,2048]{1,0:T(8,128)(2,1)S(1)}, u32[]{:S(2)}, u32[]{:S(2)}) collective-permute-start(bf16[32,2048]{1,0:T(8,128)(2,1)S(1)} %reshape.129), channel_id=1, source_target_pairs={{0,16},{16,0},{1,17},{17,1},{2,18},{18,2},{3,19},{19,3},{4,20},{20... | collective-permute-start | bytes 393224 | tf_op jit(solution)/shard_map/ppermute | solution.py:33
where the time goes:
time: 274 us; the launch traced here: 273 us
  waiting for transfers between devices  91.7 us (33%)
  starting transfers between devices  74.5 us (27%)
  blocking collectives  63.1 us (23%)
  Pallas kernels  23.7 us (9%)
  local copies, waits for them, and re-layouts  10.4 us (4%)
  other arithmetic  6.47 us (2%)
    all_to_all x3, blocking collectives, exchange(): return lax.all_to_all(blocks, axis, split_axis=0, concat_axis=0, tiled=True)  63.1 us
    ppermute x6, waiting for transfers between devices, ring(): return lax.ppermute(value, axis, [(i, (i + step) % 4) for i in range(4)])  30.3 us
    all_to_all x5, waiting for transfers between devices, exchange(): return lax.all_to_all(blocks, axis, split_axis=0, concat_axis=0, tiled=True)  29.6 us
    all_to_all x1, waiting for transfers between devices, local(): lax.all_to_all(columns, TP, split_axis=0, concat_axis=1, tiled=True)  28.9 us
    all_to_all x5, starting transfers between devices, exchange(): return lax.all_to_all(blocks, axis, split_axis=0, concat_axis=0, tiled=True)  28.5 us
    ppermute x3, starting transfers between devices, swap_cores(): return lax.ppermute(value, 'c', [(0, 1), (1, 0)])  23 us
    ppermute x6, starting transfers between devices, ring(): return lax.ppermute(value, axis, [(i, (i + step) % 4) for i in range(4)])  17.1 us
    pallas_call x1, Pallas kernels, attend(): pl.pallas_call(attend_kernel, grid=(heads,), in_specs=[pl.BlockSpec((1, r...  8.42 us
  transfers between devices with their start and end apart: 15, of which 12 were waited for; matrix products, arithmetic and copies ran while one was open for 5% of the time, Pallas kernels for 1%

commit v1 on v0

--- a/solution.py
+++ b/solution.py
@@ -22,7 +22,12 @@
 TP = ("yh", "yl", "x")
 GROUP = ("yl", "x")
 STAT_ROWS = 16
-COLOURS = tuple((i % NX + i // NX) % 4 for i in range(NT))
+SHARE = 64
+COLOURS = tuple((i % NX + i // NX) % 2 for i in range(NT))
+
+
+IN_VMEM = pl.BlockSpec(memory_space=pltpu.VMEM)
+IN_HBM = pl.BlockSpec(memory_space=pltpu.HBM)
 
 
 def exchange(blocks, axis):
@@ -93,39 +98,35 @@
 
 
 def attend_kernel(q_ref, own_ref, other_ref, out_ref):
-    width = q_ref.shape[2]
+    heads, rows, width = q_ref.shape
     factor = width ** (-0.5) * LOG2E
     keys = jnp.concatenate([own_ref[:, :width], other_ref[:, :width]], axis=0)
     values = jnp.concatenate([own_ref[:, width:], other_ref[:, width:]], axis=0)
-    scores = lax.dot_general(
-        keys, q_ref[0], (((1,), (1,)), ((), ())), preferred_element_type=F32
-    )
-    top = jnp.max(scores, axis=0, keepdims=True)
-    weights = jnp.exp2((scores - top) * factor).astype(BF)
-    total = jnp.sum(weights.astype(F32), axis=0, keepdims=True)
-    summed = lax.dot_general(
-        values, weights, (((0,), (0,)), ((), ())), preferred_element_type=F32
-    )
-    out_ref[0, :width, :] = (summed / total).astype(BF)
-    cols = summed.shape[1]
-    row = lax.broadcasted_iota(jnp.int32, (STAT_ROWS, cols), 0)
-    stats = jnp.zeros((STAT_ROWS, cols), F32)
-    for i, part in enumerate(split3(top * factor) + split3(total)):
-        stats = jnp.where(row == i, part.astype(F32), stats)
-    out_ref[0, width:, :] = stats.astype(BF)
+    values = jnp.concatenate(
+        [values.T, jnp.ones((STAT_ROWS, values.shape[0]), BF)], axis=0
+    )
+    row = lax.broadcasted_iota(jnp.int32, (STAT_ROWS, rows), 0)
+    for head in range(heads):
+        scores = lax.dot_general(
+            keys, q_ref[head], (((1,), (1,)), ((), ())), preferred_element_type=F32
+        )
+        top = jnp.max(scores, axis=0, keepdims=True)
+        weights = jnp.exp2((scores - top) * factor).astype(BF)
+        summed = jnp.dot(values, weights, preferred_element_type=F32)
+        total = summed[width : width + 1]
+        out_ref[head, :width, :] = (summed[:width] * (1.0 / total)).astype(BF)
+        stats = jnp.zeros((STAT_ROWS, rows), F32)
+        for i, part in enumerate(split3(top * factor) + split3(total)):
+            stats = jnp.where(row == i, part.astype(F32), stats)
+        out_ref[head, width:, :] = stats.astype(BF)
 
 
 def attend(q8, own, other):
     heads, rows, width = q8.shape
     return pl.pallas_call(
         attend_kernel,
-        grid=(heads,),
-        in_specs=[
-            pl.BlockSpec((1, rows, width), lambda h: (h, 0, 0)),
-            pl.BlockSpec(own.shape, lambda h: (0, 0)),
-            pl.BlockSpec(other.shape, lambda h: (0, 0)),
-        ],
-        out_specs=pl.BlockSpec((1, width + STAT_ROWS, rows), lambda h: (h, 0, 0)),
+        in_specs=[IN_VMEM] * 3,
+        out_specs=IN_VMEM,
         out_shape=jax.ShapeDtypeStruct((heads, width + STAT_ROWS, rows), BF),
         name="attend",
     )(q8, own, other)
@@ -156,6 +157,8 @@
     width = parts.shape[1] - STAT_ROWS
     return pl.pallas_call(
         combine_kernel,
+        in_specs=[IN_VMEM],
+        out_specs=IN_VMEM,
         out_shape=jax.ShapeDtypeStruct((NT, width, parts.shape[2]), BF),
         name="combine",
     )(parts)
@@ -169,67 +172,115 @@
 def deal(classes):
     return pl.pallas_call(
         deal_kernel,
+        in_specs=[IN_VMEM],
+        out_specs=IN_VMEM,
         out_shape=jax.ShapeDtypeStruct((NT, *classes.shape[1:]), BF),
         name="deal",
     )(classes)
 
 
-def experts_kernel(rows_ref, *refs):
-    pieces, out_ref, held, acc, sems = refs[:-4], refs[-4], refs[-3], refs[-2], refs[-1]
-    count, depth, _ = held.shape
-    waits = [[] for _ in range(count)]
-    chunk, at = 0, 0
-    for i, piece in enumerate(pieces):
-        size = piece.shape[0]
-        copy = pltpu.make_async_copy(piece, held.at[chunk, pl.ds(at, size), :], sems.at[i])
+def collect_kernel(back_ref, out_ref):
+    for k in range(2):
+        total = None
+        for i, colour in enumerate(COLOURS):
+            if colour == k:
+                part = back_ref[i].astype(F32)
+                total = part if total is None else total + part
+        out_ref[k] = total.astype(BF)
+
+
+def collect(back):
+    return pl.pallas_call(
+        collect_kernel,
+        in_specs=[IN_VMEM],
+        out_specs=IN_VMEM,
+        out_shape=jax.ShapeDtypeStruct((2, *back.shape[1:]), BF),
+        name="collect",
+    )(back)
+
+
+def pack_kernel(gate_ref, up_ref, down_ref, *out_refs):
+    gate, upper, down = gate_ref[0].T, up_ref[0].T, down_ref[0]
+    for i in range(2):
+        part = slice(i * SHARE, (i + 1) * SHARE)
+        packed = jnp.concatenate([gate[part], upper[part], down[part]], axis=0)
+        for half in range(2):
+            @pl.when(pl.program_id(0) == half)
+            def _():
+                out_refs[2 * half + i][...] = packed
+
+
+def pack(w_gate, w_up, w_down):
+    _, depth, _ = w_gate.shape
+    wide = pl.BlockSpec((1, depth, 2 * SHARE), lambda i: (0, 0, i))
+    shape = (3 * SHARE, depth)
+    return pl.pallas_call(
+        pack_kernel,
+        grid=(2,),
+        in_specs=[wide, wide, pl.BlockSpec((1, 2 * SHARE, depth), lambda i: (0, i, 0))],
+        out_specs=[pl.BlockSpec(shape, lambda i: (0, 0))] * 4,
+        out_shape=[jax.ShapeDtypeStruct(shape, BF)] * 4,
+        name="pack",
+    )(w_gate, w_up, w_down)
+
+
+def swish(gate, upper):
+    return (gate / (1.0 + jnp.exp(-gate)) * upper).astype(BF)
+
+
+def experts_kernel(rows_ref, gate_hbm, up_hbm, down_hbm, *refs):
+    near_hbm, refs = refs[:4], refs[4:]
+    out_ref, gate_ref, up_ref, down_ref, near_ref, acc, sems = refs
+    jobs = [(gate_hbm.at[0], gate_ref), (up_hbm.at[0], up_ref), (down_hbm.at[0], down_ref)]
+    for i, source in enumerate(near_hbm):
+        for j in range(3):
+            jobs.append(
+                (
+                    source.at[pl.ds(j * SHARE, SHARE)],
+                    near_ref.at[j, pl.ds(i * SHARE, SHARE)],
+                )
+            )
+    copies = [
+        pltpu.make_async_copy(source, target, sems.at[i])
+        for i, (source, target) in enumerate(jobs)
+    ]
+    for copy in copies:
         copy.start()
-        waits[chunk].append(copy)
-        at += size
-        if at == depth:
-            chunk, at = chunk + 1, 0
-    units = held.shape[2] // 3
-    for pair in range(count // 2):
-        hidden, down = [], []
-        for k in (2 * pair, 2 * pair + 1):
-            for copy in waits[k]:
-                copy.wait()
-            both = jnp.dot(
-                rows_ref[...], held[k, :, : 2 * units], preferred_element_type=F32
-            )
-            gate, upper = both[:, :units], both[:, units:]
-            hidden.append((gate / (1.0 + jnp.exp(-gate)) * upper).astype(BF))
-            down.append(held[k, :, 2 * units :])
-        part = lax.dot_general(
-            jnp.concatenate(hidden, axis=1),
-            jnp.concatenate(down, axis=1),
-            (((1,), (1,)), ((), ())),
-            preferred_element_type=F32,
-        )
-        if pair == 0:
-            acc[...] = part
-        elif pair < count // 2 - 1:
-            acc[...] += part
-        else:
-            out_ref[...] = (acc[...] + part).astype(BF)
-
-
-def experts(rows, pieces):
-    depth = sum(p.shape[0] for p in pieces) // 8
-    width = pieces[0].shape[1]
+    copies[0].wait()
+    gate = jnp.dot(rows_ref[...], gate_ref[...], preferred_element_type=F32)
+    copies[1].wait()
+    upper = jnp.dot(rows_ref[...], up_ref[...], preferred_element_type=F32)
+    hidden = swish(gate, upper)
+    copies[2].wait()
+    acc[...] = jnp.dot(hidden, down_ref[...], preferred_element_type=F32)
+    for copy in copies[3:]:
+        copy.wait()
+    across = (((1,), (1,)), ((), ()))
+    gate = lax.dot_general(rows_ref[...], near_ref[0], across, preferred_element_type=F32)
+    upper = lax.dot_general(rows_ref[...], near_ref[1], across, preferred_element_type=F32)
+    hidden = swish(gate, upper)
+    part = jnp.dot(hidden, near_ref[2], preferred_element_type=F32)
+    out_ref[...] = (acc[...] + part).astype(BF)
+
+
+def experts(rows, w_gate, w_up, w_down, near):
+    _, depth, units = w_gate.shape
     return pl.pallas_call(
         experts_kernel,
-        in_specs=[pl.BlockSpec(memory_space=pltpu.VMEM)]
-        + [pl.BlockSpec(memory_space=pl.ANY)] * len(pieces),
-        out_specs=pl.BlockSpec(memory_space=pltpu.VMEM),
+        in_specs=[IN_VMEM] + [IN_HBM] * (3 + len(near)),
+        out_specs=IN_VMEM,
         out_shape=jax.ShapeDtypeStruct(rows.shape, BF),
         scratch_shapes=[
-            pltpu.VMEM((8, depth, width), BF),
+            pltpu.VMEM((depth, units), BF),
+            pltpu.VMEM((depth, units), BF),
+            pltpu.VMEM((units, depth), BF),
+            pltpu.VMEM((3, 4 * SHARE, depth), BF),
             pltpu.VMEM(rows.shape, F32),
-            pltpu.SemaphoreType.DMA((len(pieces),)),
+            pltpu.SemaphoreType.DMA((3 + 3 * len(near),)),
         ],
         compiler_params=pltpu.CompilerParams(vmem_limit_bytes=40 * 1024 * 1024),
         name="experts",
-    )(rows, *pieces)
+    )(rows, w_gate, w_up, w_down, *near)
 
 
 def local(
@@ -263,13 +314,13 @@
     kv_mine = exchange(kv, "z").reshape(-1, 2 * width)
     kv_other = swap_cores(kv_mine)
 
-    units = w_gate.shape[2] // 2
-    pieces = []
-    for s, axis in ((slice(0, units), "x"), (slice(units, 2 * units), ("yh", "yl"))):
-        pack = jnp.concatenate([w_gate[0][:, s], w_up[0][:, s], w_down[0][s, :].T], axis=1)
-        left, right = ring(pack, axis, 1), ring(pack, axis, -1)
-        far = ring(left, axis, 1)
-        pieces += [pack, left, right, far]
+    packs = pack(w_gate, w_up, w_down)
+    near = [
+        ring(packs[0], "x", 1),
+        ring(packs[1], "x", -1),
+        ring(packs[2], ("yh", "yl"), 1),
+        ring(packs[3], ("yh", "yl"), -1),
+    ]
 
     parts = attend(q8, kv_mine, kv_other)
     parts = exchange(parts, GROUP)
@@ -290,9 +341,7 @@
     tok = jnp.arange(tok_dev, dtype=jnp.int32)
     before = tok[None, :] < tok[:, None]
     place = jnp.arange(NZ * NC * cap, dtype=jnp.int32)
-    rel, zc_slot = place // (NZ * cap), place % (NZ * cap)
-    expert_of = (zc_slot // cap) * NC + (c + rel) % NC
-    slot_of = zc_slot % cap
+    expert_of, slot_of = place // cap, place % cap
     hits = []
     for k in range(top):
         mine = routes[:, k]
@@ -309,25 +358,12 @@
     sent = lax.dot_general(
         selector, normed, (((0,), (0,)), ((), ())), preferred_element_type=F32
     ).astype(BF)
-    half = NZ * cap
-    from_other = swap_cores(sent[half:])
-    outgoing = jnp.concatenate(
-        [sent[:half].reshape(NZ, cap, depth), from_other.reshape(NZ, cap, depth)], axis=1
-    )
-    arrived = exchange(outgoing, "z")
-
-    rows = exchange(deal(arrived.reshape(4, NZ * NC * cap // 4, depth)), TP)
-    partial = experts(rows.reshape(-1, depth), pieces).reshape(rows.shape)
-    back = exchange(partial, TP)
-    expert_out = jnp.stack(
-        [
-            sum(back[i].astype(F32) for i in range(NT) if COLOURS[i] == k).astype(BF)
-            for k in range(4)
-        ]
-    ).reshape(NZ, NC * cap, depth)
-    returned = exchange(expert_out, "z")
-    for_other = swap_cores(returned[:, cap:].reshape(half, depth))
-    picked_from = jnp.concatenate([returned[:, :cap].reshape(half, depth), for_other], axis=0)
+    arrived = exchange(sent, ("z", "c"))
+
+    rows = exchange(deal(arrived.reshape(2, NZ * NC * cap // 2, depth)), TP)
+    partial = experts(rows.reshape(-1, depth), w_gate, w_up, w_down, near)
+    back = exchange(partial.reshape(rows.shape), TP)
+    picked_from = exchange(collect(back).reshape(arrived.shape), ("z", "c"))
     moe = sum(
         jnp.dot(hits[k].astype(BF), picked_from, preferred_element_type=F32)
         * route_weights[:, k][:, None]

time: 274 us -> 283 us (1.033)
  blocking collectives: 63.1 us -> 121 us
  starting transfers between devices: 74.5 us -> 41.4 us
  waiting for transfers between devices: 91.7 us -> 74.3 us
  other arithmetic: 6.47 us -> 0.96 us
  Pallas kernels: 23.7 us -> 27.8 us
  local copies, waits for them, and re-layouts: 10.4 us -> 13.4 us
    all_to_all x3 -> x5, blocking collectives: 63.1 us -> 121 us  [exchange(): return lax.all_to_all(blocks, axis, split_axis=0, concat_axis=0, tiled=True)]
    all_to_all x1, waiting for transfers between devices: 28.9 us -> 6.54 us  [local(): lax.all_to_all(columns, TP, split_axis=0, concat_axis=1, tiled=True)]
    ppermute x3 -> x1, starting transfers between devices: 23 us -> 8.66 us  [swap_cores(): return lax.ppermute(value, 'c', [(0, 1), (1, 0)])]
    all_to_all x5 -> x3, starting transfers between devices: 28.5 us -> 15 us  [exchange(): return lax.all_to_all(blocks, axis, split_axis=0, concat_axis=0, tiled=True)]
    all_to_all x5 -> x3, waiting for transfers between devices: 29.6 us -> 37.4 us  [exchange(): return lax.all_to_all(blocks, axis, split_axis=0, concat_axis=0, tiled=True)]
    unnamed x23 -> x32, local copies, waits for them, and re-layouts: 4.67 us -> 10.4 us
    concatenate x3 -> x0, other arithmetic: 5.26 us -> none  [the longest x2 4.29 us: local(): jnp.concatenate([w_gate[0][:, s], w_up[0][:, s], w_down[0][s, :].T], axis=1)]
    pallas_call x4 -> x6, Pallas kernels: 20.6 us -> 24.7 us  [the longest x1 7.88 us: attend(): pl.pallas_call(attend_kernel, in_specs=[IN_VMEM] * 3, out_specs=IN_VMEM,...]
  transfers between devices with their start and end apart: 15 -> 9, of which waited for: 12 -> 6; matrix products, arithmetic and copies ran while one was open for 5% -> 0% of each run, Pallas kernels for 1% -> 1%
where the time goes in v1:
time: 283 us; the launch traced here: 282 us
  blocking collectives  121 us (43%)
  waiting for transfers between devices  74.3 us (26%)
  starting transfers between devices  41.4 us (15%)
  Pallas kernels  27.8 us (10%)
  local copies, waits for them, and re-layouts  13.4 us (5%)
    all_to_all x5, blocking collectives, exchange(): return lax.all_to_all(blocks, axis, split_axis=0, concat_axis=0, tiled=True)  121 us
    all_to_all x3, waiting for transfers between devices, exchange(): return lax.all_to_all(blocks, axis, split_axis=0, concat_axis=0, tiled=True)  37.4 us
    ppermute x4, waiting for transfers between devices, ring(): return lax.ppermute(value, axis, [(i, (i + step) % 4) for i in range(4)])  29.2 us
    all_to_all x3, starting transfers between devices, exchange(): return lax.all_to_all(blocks, axis, split_axis=0, concat_axis=0, tiled=True)  15 us
    ppermute x4, starting transfers between devices, ring(): return lax.ppermute(value, axis, [(i, (i + step) % 4) for i in range(4)])  13.2 us
    unnamed x32, local copies, waits for them, and re-layouts  10.4 us
    ppermute x1, starting transfers between devices, swap_cores(): return lax.ppermute(value, 'c', [(0, 1), (1, 0)])  8.66 us
    pallas_call x1, Pallas kernels, attend(): pl.pallas_call(attend_kernel, in_specs=[IN_VMEM] * 3, out_specs=IN_VMEM,...  7.88 us
  transfers between devices with their start and end apart: 9, of which 6 were waited for; matrix products, arithmetic and copies ran while one was open for 0% of the time, Pallas kernels for 1%

profile of v1, /device:TPU:1, one launch (start us, length us, event | category | flops | bytes accessed | tf_op | source)
XLA Modules:
  0.0 281.6 jit_solution(14048813684226112643)
XLA Ops:
  0.0 0.6 pad_add_fusion.at_ref
  0.6 3.1 %prepare.1 = (bf16[8,256,128]{2,1,0:T(8,128)(2,1)}, bf16[16,32,256]{2,1,0:T(8,128)(2,1)}) custom-call(s32[4]{0:T(128)} %pad_add_fusion.at_ref, bf16[256,128]{1,0:T(8,128)(2,1)} %q_ref.1, bf16[256,256]{1,0:T(8,128)(2,1)} %k_ref.1, bf16[256,256]{1,0:T(8,128)(2,1)} %v_ref.1, f32[1,128]{1,0:T(1,128)} %bitcast.37, f32[1,128]{1,0:T(1,128)} %bitcast.38), custom_call_target="tpu_custom_call" | custom-call | tf_op jit(solution)/shard_map/prepare/pallas_call | solution.py:79
  3.7 13.5 %all_to_all.64.q_ref = bf16[8,256,128]{2,1,0:T(8,128)(2,1)} all-to-all(bf16[8,256,128]{2,1,0:T(8,128)(2,1)} %get-tuple-element.13), channel_id=1, replica_groups=mesh['z'=16,'c'=2,'yh'=2,'yl'=2,'x'=4] {'yl','x'}, dimensions={0} | all-to-all | bytes 1048576 | tf_op jit(solution)/shard_map/all_to_all | solution.py:34
  17.2 29.3 %all_to_all.65 = bf16[16,32,256]{2,1,0:T(8,128)(2,1)S(1)} all-to-all(bf16[16,32,256]{2,1,0:T(8,128)(2,1)} %get-tuple-element.16), channel_id=1, replica_groups=mesh['z'=16,'c'=2,'yh'=2,'yl'=2,'x'=4] {'z'}, dimensions={0} | all-to-all | bytes 524288 | tf_op jit(solution)/shard_map/all_to_all | solution.py:34
  46.5 8.7 %collective-permute-start = (bf16[512,256]{1,0:T(8,128)(2,1)S(1)}, bf16[512,256]{1,0:T(8,128)(2,1)S(1)}, u32[]{:S(2)}, u32[]{:S(2)}) collective-permute-start(bf16[512,256]{1,0:T(8,128)(2,1)S(1)} %bitcast.35), channel_id=1, source_target_pairs={{0,16},{16,0},{1,17},{17,1},{2,18},{18,2},{3,19},{19,3},{4,20},{20... | collective-permute-start | bytes 786440 | tf_op jit(solution)/shard_map/ppermute | solution.py:38
  55.2 1.1 collective-permute-done.other_ref
  56.3 0.7 copy-done.11
  57.0 7.9 %attend.1 = bf16[8,144,256]{2,1,0:T(8,128)(2,1)} custom-call(bf16[8,256,128]{2,1,0:T(8,128)(2,1)} %all_to_all.64.q_ref, bf16[512,256]{1,0:T(8,128)(2,1)} %bitcast.36, bf16[512,256]{1,0:T(8,128)(2,1)} %copy-done.11), custom_call_target="tpu_custom_call" | custom-call | tf_op jit(solution)/shard_map/attend/pallas_call | solution.py:126
  64.9 15.0 %all_to_all.66.parts_ref = bf16[8,144,256]{2,1,0:T(8,128)(2,1)} all-to-all(bf16[8,144,256]{2,1,0:T(8,128)(2,1)} %attend.1), channel_id=1, replica_groups=mesh['z'=16,'c'=2,'yh'=2,'yl'=2,'x'=4] {'yl','x'}, dimensions={0} | all-to-all | bytes 1179648 | tf_op jit(solution)/shard_map/all_to_all | solution.py:34
  79.8 2.2 combine.1
  82.1 4.6 %all-to-all-start.3 = ((bf16[16,128,256]{2,1,0:T(8,128)(2,1)}), bf16[16,128,256]{2,1,0:T(8,128)(2,1)S(1)}, u32[]{:S(2)}, u32[]{:S(2)}) async-start(bf16[16,128,256]{2,1,0:T(8,128)(2,1)} %combine.1), calls=%async_computation.3 | async-start | bytes 2097152 | tf_op jit(solution)/shard_map/all_to_all | solution.py:34
  86.7 0.2 convert_reduce_fusion.2
  87.0 15.1 %all-to-all-done.3 = bf16[16,128,256]{2,1,0:T(8,128)(2,1)S(1)} async-done(((bf16[16,128,256]{2,1,0:T(8,128)(2,1)}), bf16[16,128,256]{2,1,0:T(8,128)(2,1)S(1)}, u32[]{:S(2)}, u32[]{:S(2)}) %all-to-all-start.3) | async-done | bytes 1048608 | tf_op jit(solution)/shard_map/all_to_all | solution.py:34
  102.1 1.1 convolution_convert_fusion.1
  103.2 4.6 %all-to-all-start.4 = ((bf16[16,16,128]{2,1,0:T(8,128)(2,1)}), bf16[16,16,128]{2,1,0:T(8,128)(2,1)S(1)}, u32[]{:S(2)}, u32[]{:S(2)}) async-start(bf16[16,16,128]{2,1,0:T(8,128)(2,1)} %bitcast.8), calls=%async_computation.4 | async-start | bytes 131072 | tf_op jit(solution)/shard_map/all_to_all | solution.py:331
  107.8 6.5 %all-to-all-done.4 = bf16[16,16,128]{2,1,0:T(8,128)(2,1)S(1)} async-done(((bf16[16,16,128]{2,1,0:T(8,128)(2,1)}), bf16[16,16,128]{2,1,0:T(8,128)(2,1)S(1)}, u32[]{:S(2)}, u32[]{:S(2)}) %all-to-all-start.4) | async-done | bytes 65568 | tf_op jit(solution)/shard_map/all_to_all | solution.py:331
  114.3 0.1 fusion.3
  114.5 0.3 convolution_convert_fusion
  114.8 0.2 all_to_all.48
  115.0 30.8 %all_to_all.67 = bf16[32,2,2048]{2,1,0:T(2,128)(2,1)S(1)} all-to-all(bf16[32,2,2048]{2,1,0:T(2,128)(2,1)S(1)} %all_to_all.48), channel_id=1, replica_groups=mesh['z'=16,'c'=2,'yh'=2,'yl'=2,'x'=4] {'z','c'}, dimensions={0} | all-to-all | bytes 524288 | tf_op jit(solution)/shard_map/all_to_all | solution.py:34
  145.8 0.8 reshape.72.classes_ref
  146.6 2.4 deal.1
  149.0 3.7 %all-to-all-start.6 = ((bf16[16,32,2048]{2,1,0:T(8,128)(2,1)}), bf16[16,32,2048]{2,1,0:T(8,128)(2,1)S(1)}, u32[]{:S(2)}, u32[]{:S(2)}) async-start(bf16[16,32,2048]{2,1,0:T(8,128)(2,1)} %deal.1), calls=%async_computation.6 | async-start | bytes 4194304 | tf_op jit(solution)/shard_map/all_to_all | solution.py:34
  152.7 4.0 %pack.1 = (bf16[192,2048]{1,0:T(8,128)(2,1)}, bf16[192,2048]{1,0:T(8,128)(2,1)}, bf16[192,2048]{1,0:T(8,128)(2,1)}, bf16[192,2048]{1,0:T(8,128)(2,1)}) custom-call(bf16[1,2048,256]{2,1,0:T(8,128)(2,1)} %gate_hbm.1, bf16[1,2048,256]{2,1,0:T(8,128)(2,1)} %up_hbm.1, bf16[1,256,2048]{2,1,0:T(8,128)(2,1)} %down_hbm.1), custom_call_target="tpu_custom_call" | custom-call | tf_op jit(solution)/shard_map/pack/pallas_call | solution.py:217
  156.7 3.1 %collective-permute-start.1 = (bf16[192,2048]{1,0:T(8,128)(2,1)}, bf16[192,2048]{1,0:T(8,128)(2,1)S(1)}, u32[]{:S(2)}, u32[]{:S(2)}) collective-permute-start(bf16[192,2048]{1,0:T(8,128)(2,1)} %get-tuple-element.17), channel_id=1, source_target_pairs={{0,1},{1,2},{2,3},{3,0},{4,5},{5,6},{6,7},{7,4},{8,9},{9,10},{10,1... | collective-permute-start | bytes 2359304 | tf_op jit(solution)/shard_map/ppermute | solution.py:42
  159.9 3.3 %collective-permute-start.2 = (bf16[192,2048]{1,0:T(8,128)(2,1)}, bf16[192,2048]{1,0:T(8,128)(2,1)S(1)}, u32[]{:S(2)}, u32[]{:S(2)}) collective-permute-start(bf16[192,2048]{1,0:T(8,128)(2,1)} %get-tuple-element.18), channel_id=1, source_target_pairs={{0,3},{1,0},{2,1},{3,2},{4,7},{5,4},{6,5},{7,6},{8,11},{9,8},{10,9... | collective-permute-start | bytes 2359304 | tf_op jit(solution)/shard_map/ppermute | solution.py:42
  163.2 3.2 %collective-permute-start.3 = (bf16[192,2048]{1,0:T(8,128)(2,1)}, bf16[192,2048]{1,0:T(8,128)(2,1)S(1)}, u32[]{:S(2)}, u32[]{:S(2)}) collective-permute-start(bf16[192,2048]{1,0:T(8,128)(2,1)} %get-tuple-element.19), channel_id=1, source_target_pairs={{0,4},{4,8},{8,12},{12,0},{1,5},{5,9},{9,13},{13,1},{2,6},{6,10},{... | collective-permute-start | bytes 2359304 | tf_op jit(solution)/shard_map/ppermute | solution.py:42
  166.4 3.5 %collective-permute-start.4 = (bf16[192,2048]{1,0:T(8,128)(2,1)}, bf16[192,2048]{1,0:T(8,128)(2,1)S(1)}, u32[]{:S(2)}, u32[]{:S(2)}) collective-permute-start(bf16[192,2048]{1,0:T(8,128)(2,1)} %get-tuple-element.20), channel_id=1, source_target_pairs={{0,12},{4,0},{8,4},{12,8},{1,13},{5,1},{9,5},{13,9},{2,14},{6,2},{... | collective-permute-start | bytes 2359304 | tf_op jit(solution)/shard_map/ppermute | solution.py:42
  169.9 28.5 %collective-permute-done.1.refs_0_ = bf16[192,2048]{1,0:T(8,128)(2,1)S(1)} collective-permute-done((bf16[192,2048]{1,0:T(8,128)(2,1)}, bf16[192,2048]{1,0:T(8,128)(2,1)S(1)}, u32[]{:S(2)}, u32[]{:S(2)}) %collective-permute-start.1) | collective-permute-done | bytes 786464 | tf_op jit(solution)/shard_map/ppermute | solution.py:42
  198.4 0.8 collective-permute-done.2.refs_1_
  199.1 0.9 copy-done.4
  200.0 0.9 copy-done.6
  200.9 0.9 copy-done.8
  201.8 1.2 copy-done.1
  203.0 1.2 copy-done.2
  204.2 1.2 copy-done.3
  205.4 1.1 copy-done.5
  206.6 1.1 copy-done.7
  207.7 1.1 copy-done.9
  208.8 5.6 %experts.1 = bf16[512,2048]{1,0:T(8,128)(2,1)S(1)} custom-call(bf16[512,2048]{1,0:T(8,128)(2,1)S(1)} %bitcast.32, bf16[1,2048,256]{2,1,0:T(8,128)(2,1)S(1)} %copy-done.1, bf16[1,2048,256]{2,1,0:T(8,128)(2,1)S(1)} %copy-done.2, bf16[1,256,2048]{2,1,0:T(8,128)(2,1)S(1)} %copy-done.3, bf16[192,2048]{1,0:T(8,128)(2,1)S(1)} %collective-permute-done.1.refs_0_, ...), custom_call_target="tpu_custom_call" | custom-call | tf_op jit(solution)/shard_map/experts/pallas_call | solution.py:268
  214.4 32.5 %all_to_all.68.back_ref = bf16[16,32,2048]{2,1,0:T(8,128)(2,1)} all-to-all(bf16[16,32,2048]{2,1,0:T(8,128)(2,1)S(1)} %bitcast.33), channel_id=1, replica_groups=mesh['z'=16,'c'=2,'yh'=2,'yl'=2,'x'=4] {'yh','yl','x'}, dimensions={0} | all-to-all | bytes 4194304 | tf_op jit(solution)/shard_map/all_to_all | solution.py:34
  247.0 2.6 collect.1
  249.6 1.8 all_to_all.52
  251.4 6.7 %all-to-all-start.8 = ((bf16[32,2,2048]{2,1,0:T(2,128)(2,1)}), bf16[32,2,2048]{2,1,0:T(2,128)(2,1)S(1)}, u32[]{:S(2)}, u32[]{:S(2)}) async-start(bf16[32,2,2048]{2,1,0:T(2,128)(2,1)} %all_to_all.52), calls=%async_computation.8 | async-start | bytes 524288 | tf_op jit(solution)/shard_map/all_to_all | solution.py:34
  258.1 22.2 %all-to-all-done.8 = bf16[32,2,2048]{2,1,0:T(2,128)(2,1)S(1)} async-done(((bf16[32,2,2048]{2,1,0:T(2,128)(2,1)}), bf16[32,2,2048]{2,1,0:T(2,128)(2,1)S(1)}, u32[]{:S(2)}, u32[]{:S(2)}) %all-to-all-start.8) | async-done | bytes 262176 | tf_op jit(solution)/shard_map/all_to_all | solution.py:34
  280.4 0.1 all_to_all.54
  280.5 0.2 convolution_multiply_fusion.1
  280.7 0.9 fusion.2
  (31 shorter events, 0.1 us)
Async XLA Ops:
  0.0 102.1 %copy-start = (bf16[2048,128]{1,0:T(8,128)(2,1)S(1)}, bf16[2048,128]{1,0:T(8,128)(2,1)}, u32[]{:S(2)}) copy-start(bf16[2048,128]{1,0:T(8,128)(2,1)} %param.18) | copy-start | bytes 1572868
  46.5 9.8 %copy-start.10 = (bf16[16,32,256]{2,1,0:T(8,128)(2,1)}, bf16[16,32,256]{2,1,0:T(8,128)(2,1)S(1)}, u32[]{:S(2)}) copy-start(bf16[16,32,256]{2,1,0:T(8,128)(2,1)S(1)} %all_to_all.65) | copy-start | bytes 786436
  46.5 9.8 %collective-permute-start = (bf16[512,256]{1,0:T(8,128)(2,1)S(1)}, bf16[512,256]{1,0:T(8,128)(2,1)S(1)}, u32[]{:S(2)}, u32[]{:S(2)}) collective-permute-start(bf16[512,256]{1,0:T(8,128)(2,1)S(1)} %bitcast.35), channel_id=1, source_target_pairs={{0,16},{16,0},{1,17},{17,1},{2,18},{18,2},{3,19},{19,3},{4,20},{20... | collective-permute-start | bytes 786440 | tf_op jit(solution)/shard_map/ppermute | solution.py:38
  56.3 0.7 copy-start.11
  79.8 6.8 %copy-start.14 = (s32[16,2]{0,1:T(2,128)S(1)}, s32[16,2]{0,1:T(2,128)}, u32[]{:S(2)}) copy-start(s32[16,2]{0,1:T(2,128)} %param.21) | copy-start | bytes 388
  82.1 32.2 %copy-start.12 = (bf16[16,2048]{1,0:T(8,128)(2,1)S(1)}, bf16[16,2048]{1,0:T(8,128)(2,1)}, u32[]{:S(2)}) copy-start(bf16[16,2048]{1,0:T(8,128)(2,1)} %param.20) | copy-start | bytes 196612
  82.1 32.4 %copy-start.13 = (f32[2048]{0:T(1024)S(1)}, f32[2048]{0:T(1024)}, u32[]{:S(2)}) copy-start(f32[2048]{0:T(1024)} %param.19) | copy-start | bytes 24580
  82.1 20.0 %all-to-all-start.3 = ((bf16[16,128,256]{2,1,0:T(8,128)(2,1)}), bf16[16,128,256]{2,1,0:T(8,128)(2,1)S(1)}, u32[]{:S(2)}, u32[]{:S(2)}) async-start(bf16[16,128,256]{2,1,0:T(8,128)(2,1)} %combine.1), calls=%async_computation.3 | async-start | bytes 2097152 | tf_op jit(solution)/shard_map/all_to_all | solution.py:34
  103.2 11.1 %all-to-all-start.4 = ((bf16[16,16,128]{2,1,0:T(8,128)(2,1)}), bf16[16,16,128]{2,1,0:T(8,128)(2,1)S(1)}, u32[]{:S(2)}, u32[]{:S(2)}) async-start(bf16[16,16,128]{2,1,0:T(8,128)(2,1)} %bitcast.8), calls=%async_computation.4 | async-start | bytes 131072 | tf_op jit(solution)/shard_map/all_to_all | solution.py:331
  149.0 52.8 %all-to-all-start.6 = ((bf16[16,32,2048]{2,1,0:T(8,128)(2,1)}), bf16[16,32,2048]{2,1,0:T(8,128)(2,1)S(1)}, u32[]{:S(2)}, u32[]{:S(2)}) async-start(bf16[16,32,2048]{2,1,0:T(8,128)(2,1)} %deal.1), calls=%async_computation.6 | async-start | bytes 4194304 | tf_op jit(solution)/shard_map/all_to_all | solution.py:34
  156.7 41.6 %collective-permute-start.1 = (bf16[192,2048]{1,0:T(8,128)(2,1)}, bf16[192,2048]{1,0:T(8,128)(2,1)S(1)}, u32[]{:S(2)}, u32[]{:S(2)}) collective-permute-start(bf16[192,2048]{1,0:T(8,128)(2,1)} %get-tuple-element.17), channel_id=1, source_target_pairs={{0,1},{1,2},{2,3},{3,0},{4,5},{5,6},{6,7},{7,4},{8,9},{9,10},{10,1... | collective-permute-start | bytes 2359304 | tf_op jit(solution)/shard_map/ppermute | solution.py:42
  159.9 39.3 %collective-permute-start.2 = (bf16[192,2048]{1,0:T(8,128)(2,1)}, bf16[192,2048]{1,0:T(8,128)(2,1)S(1)}, u32[]{:S(2)}, u32[]{:S(2)}) collective-permute-start(bf16[192,2048]{1,0:T(8,128)(2,1)} %get-tuple-element.18), channel_id=1, source_target_pairs={{0,3},{1,0},{2,1},{3,2},{4,7},{5,4},{6,5},{7,6},{8,11},{9,8},{10,9... | collective-permute-start | bytes 2359304 | tf_op jit(solution)/shard_map/ppermute | solution.py:42
  163.2 36.8 %collective-permute-start.3 = (bf16[192,2048]{1,0:T(8,128)(2,1)}, bf16[192,2048]{1,0:T(8,128)(2,1)S(1)}, u32[]{:S(2)}, u32[]{:S(2)}) collective-permute-start(bf16[192,2048]{1,0:T(8,128)(2,1)} %get-tuple-element.19), channel_id=1, source_target_pairs={{0,4},{4,8},{8,12},{12,0},{1,5},{5,9},{9,13},{13,1},{2,6},{6,10},{... | collective-permute-start | bytes 2359304 | tf_op jit(solution)/shard_map/ppermute | solution.py:42
  166.4 34.5 %collective-permute-start.4 = (bf16[192,2048]{1,0:T(8,128)(2,1)}, bf16[192,2048]{1,0:T(8,128)(2,1)S(1)}, u32[]{:S(2)}, u32[]{:S(2)}) collective-permute-start(bf16[192,2048]{1,0:T(8,128)(2,1)} %get-tuple-element.20), channel_id=1, source_target_pairs={{0,12},{4,0},{8,4},{12,8},{1,13},{5,1},{9,5},{13,9},{2,14},{6,2},{... | collective-permute-start | bytes 2359304 | tf_op jit(solution)/shard_map/ppermute | solution.py:42
  199.1 0.9 copy-start.4
  200.0 0.9 copy-start.6
  200.9 0.9 copy-start.8
  201.8 1.2 copy-start.1
  203.0 1.2 copy-start.2
  204.2 1.2 copy-start.3
  205.4 1.1 copy-start.5
  206.6 1.1 copy-start.7
  207.7 1.1 copy-start.9
  247.0 11.1 %copy-start.15 = (f32[16,2]{0,1:T(2,128)S(1)}, f32[16,2]{0,1:T(2,128)}, u32[]{:S(2)}) copy-start(f32[16,2]{0,1:T(2,128)} %param.22) | copy-start | bytes 388
  251.4 29.0 %all-to-all-start.8 = ((bf16[32,2,2048]{2,1,0:T(2,128)(2,1)}), bf16[32,2,2048]{2,1,0:T(2,128)(2,1)S(1)}, u32[]{:S(2)}, u32[]{:S(2)}) async-start(bf16[32,2,2048]{2,1,0:T(2,128)(2,1)} %all_to_all.52), calls=%async_computation.8 | async-start | bytes 524288 | tf_op jit(solution)/shard_map/all_to_all | solution.py:34

commit v2 on v1

--- a/solution.py
+++ b/solution.py
@@ -22,12 +22,17 @@
 TP = ("yh", "yl", "x")
 GROUP = ("yl", "x")
 STAT_ROWS = 16
-SHARE = 64
-COLOURS = tuple((i % NX + i // NX) % 2 for i in range(NT))
+SHARE = 128
+NSHARE = 4
+COLOURS = tuple((i % NX + i // NX) % NSHARE for i in range(NT))
 
 
 IN_VMEM = pl.BlockSpec(memory_space=pltpu.VMEM)
 IN_HBM = pl.BlockSpec(memory_space=pltpu.HBM)
+
+
+def grant(mib):
+    return pltpu.CompilerParams(vmem_limit_bytes=mib * 1024 * 1024)
 
 
 def exchange(blocks, axis):
@@ -128,6 +133,7 @@
         in_specs=[IN_VMEM] * 3,
         out_specs=IN_VMEM,
         out_shape=jax.ShapeDtypeStruct((heads, width + STAT_ROWS, rows), BF),
+        compiler_params=grant(24),
         name="attend",
     )(q8, own, other)
 
@@ -160,6 +166,7 @@
         in_specs=[IN_VMEM],
         out_specs=IN_VMEM,
         out_shape=jax.ShapeDtypeStruct((NT, width, parts.shape[2]), BF),
+        compiler_params=grant(16),
         name="combine",
     )(parts)
 
@@ -175,12 +182,13 @@
         in_specs=[IN_VMEM],
         out_specs=IN_VMEM,
         out_shape=jax.ShapeDtypeStruct((NT, *classes.shape[1:]), BF),
+        compiler_params=grant(16),
         name="deal",
     )(classes)
 
 
 def collect_kernel(back_ref, out_ref):
-    for k in range(2):
+    for k in range(NSHARE):
         total = None
         for i, colour in enumerate(COLOURS):
             if colour == k:
@@ -194,93 +202,90 @@
         collect_kernel,
         in_specs=[IN_VMEM],
         out_specs=IN_VMEM,
-        out_shape=jax.ShapeDtypeStruct((2, *back.shape[1:]), BF),
+        out_shape=jax.ShapeDtypeStruct((NSHARE, *back.shape[1:]), BF),
+        compiler_params=grant(16),
         name="collect",
     )(back)
 
 
 def pack_kernel(gate_ref, up_ref, down_ref, *out_refs):
-    gate, upper, down = gate_ref[0].T, up_ref[0].T, down_ref[0]
-    for i in range(2):
-        part = slice(i * SHARE, (i + 1) * SHARE)
-        packed = jnp.concatenate([gate[part], upper[part], down[part]], axis=0)
-        for half in range(2):
-            @pl.when(pl.program_id(0) == half)
-            def _():
-                out_refs[2 * half + i][...] = packed
+    packed = jnp.concatenate([gate_ref[0].T, up_ref[0].T, down_ref[0]], axis=0)
+    for half, out_ref in enumerate(out_refs):
+        @pl.when(pl.program_id(0) == half)
+        def _():
+            out_ref[...] = packed
 
 
 def pack(w_gate, w_up, w_down):
-    _, depth, _ = w_gate.shape
-    wide = pl.BlockSpec((1, depth, 2 * SHARE), lambda i: (0, 0, i))
+    _, depth, units = w_gate.shape
+    wide = pl.BlockSpec((1, depth, SHARE), lambda i: (0, 0, i))
     shape = (3 * SHARE, depth)
     return pl.pallas_call(
         pack_kernel,
-        grid=(2,),
-        in_specs=[wide, wide, pl.BlockSpec((1, 2 * SHARE, depth), lambda i: (0, i, 0))],
-        out_specs=[pl.BlockSpec(shape, lambda i: (0, 0))] * 4,
-        out_shape=[jax.ShapeDtypeStruct(shape, BF)] * 4,
+        grid=(units // SHARE,),
+        in_specs=[wide, wide, pl.BlockSpec((1, SHARE, depth), lambda i: (0, i, 0))],
+        out_specs=[pl.BlockSpec(shape, lambda i: (0, 0))] * 2,
+        out_shape=[jax.ShapeDtypeStruct(shape, BF)] * 2,
         name="pack",
     )(w_gate, w_up, w_down)
 
 
-def swish(gate, upper):
-    return (gate / (1.0 + jnp.exp(-gate)) * upper).astype(BF)
-
-
-def experts_kernel(rows_ref, gate_hbm, up_hbm, down_hbm, *refs):
-    near_hbm, refs = refs[:4], refs[4:]
-    out_ref, gate_ref, up_ref, down_ref, near_ref, acc, sems = refs
-    jobs = [(gate_hbm.at[0], gate_ref), (up_hbm.at[0], up_ref), (down_hbm.at[0], down_ref)]
-    for i, source in enumerate(near_hbm):
-        for j in range(3):
-            jobs.append(
-                (
-                    source.at[pl.ds(j * SHARE, SHARE)],
-                    near_ref.at[j, pl.ds(i * SHARE, SHARE)],
+def experts_kernel(rows_ref, *refs):
+    pieces, (out_ref, held, acc, sems) = refs[:-4], refs[-4:]
+    pairs = len(pieces) // 2
+    copies = [
+        pltpu.make_async_copy(
+            pieces[2 * p + i].at[pl.ds(j * SHARE, SHARE)],
+            held.at[p, j, pl.ds(i * SHARE, SHARE)],
+            sems.at[p, j, i],
+        )
+        for p in range(pairs)
+        for j in range(3)
+        for i in range(2)
+    ]
+    for copy in copies[:12]:
+        copy.start()
+    across = (((1,), (1,)), ((), ()))
+    for p in range(pairs):
+        gate_up = []
+        for j in range(2):
+            for copy in copies[6 * p + 2 * j : 6 * p + 2 * j + 2]:
+                copy.wait()
+            gate_up.append(
+                lax.dot_general(
+                    rows_ref[...], held[p, j], across, preferred_element_type=F32
                 )
             )
-    copies = [
-        pltpu.make_async_copy(source, target, sems.at[i])
-        for i, (source, target) in enumerate(jobs)
-    ]
-    for copy in copies:
-        copy.start()
-    copies[0].wait()
-    gate = jnp.dot(rows_ref[...], gate_ref[...], preferred_element_type=F32)
-    copies[1].wait()
-    upper = jnp.dot(rows_ref[...], up_ref[...], preferred_element_type=F32)
-    hidden = swish(gate, upper)
-    copies[2].wait()
-    acc[...] = jnp.dot(hidden, down_ref[...], preferred_element_type=F32)
-    for copy in copies[3:]:
-        copy.wait()
-    across = (((1,), (1,)), ((), ()))
-    gate = lax.dot_general(rows_ref[...], near_ref[0], across, preferred_element_type=F32)
-    upper = lax.dot_general(rows_ref[...], near_ref[1], across, preferred_element_type=F32)
-    hidden = swish(gate, upper)
-    part = jnp.dot(hidden, near_ref[2], preferred_element_type=F32)
-    out_ref[...] = (acc[...] + part).astype(BF)
-
-
-def experts(rows, w_gate, w_up, w_down, near):
-    _, depth, units = w_gate.shape
+        gate, upper = gate_up
+        hidden = (gate / (1.0 + jnp.exp(-gate)) * upper).astype(BF)
+        for copy in copies[6 * p + 4 : 6 * p + 6]:
+            copy.wait()
+        for copy in copies[6 * (p + 2) : 6 * (p + 3)]:
+            copy.start()
+        part = jnp.dot(hidden, held[p, 2], preferred_element_type=F32)
+        if p == 0:
+            acc[...] = part
+        elif p < pairs - 1:
+            acc[...] += part
+        else:
+            out_ref[...] = (acc[...] + part).astype(BF)
+
+
+def experts(rows, pieces):
+    depth = rows.shape[1]
     return pl.pallas_call(
         experts_kernel,
-        in_specs=[IN_VMEM] + [IN_HBM] * (3 + len(near)),
+        in_specs=[IN_VMEM] + [IN_HBM] * len(pieces),
         out_specs=IN_VMEM,
         out_shape=jax.ShapeDtypeStruct(rows.shape, BF),
         scratch_shapes=[
-            pltpu.VMEM((depth, units), BF),
-            pltpu.VMEM((depth, units), BF),
-            pltpu.VMEM((units, depth), BF),
-            pltpu.VMEM((3, 4 * SHARE, depth), BF),
+            pltpu.VMEM((len(pieces) // 2, 3, 2 * SHARE, depth), BF),
             pltpu.VMEM(rows.shape, F32),
-            pltpu.SemaphoreType.DMA((3 + 3 * len(near),)),
+            pltpu.SemaphoreType.DMA((len(pieces) // 2, 3, 2)),
         ],
-        compiler_params=pltpu.CompilerParams(vmem_limit_bytes=40 * 1024 * 1024),
+        compiler_params=grant(32),
         name="experts",
-    )(rows, w_gate, w_up, w_down, *near)
+    )(rows, *pieces)
 
 
 def local(
@@ -315,12 +320,11 @@
     kv_other = swap_cores(kv_mine)
 
     packs = pack(w_gate, w_up, w_down)
-    near = [
-        ring(packs[0], "x", 1),
-        ring(packs[1], "x", -1),
-        ring(packs[2], ("yh", "yl"), 1),
-        ring(packs[3], ("yh", "yl"), -1),
-    ]
+    axes = ("x", ("yh", "yl"))
+    left = [ring(p, axis, 1) for p, axis in zip(packs, axes)]
+    right = [ring(p, axis, -1) for p, axis in zip(packs, axes)]
+    far = [ring(p, axis, 1) for p, axis in zip(left, axes)]
+    pieces = [*packs, *left, *right, *far]
 
     parts = attend(q8, kv_mine, kv_other)
     parts = exchange(parts, GROUP)
@@ -360,8 +364,9 @@
     ).astype(BF)
     arrived = exchange(sent, ("z", "c"))
 
-    rows = exchange(deal(arrived.reshape(2, NZ * NC * cap // 2, depth)), TP)
-    partial = experts(rows.reshape(-1, depth), w_gate, w_up, w_down, near)
+    classes = arrived.reshape(NSHARE, NZ * NC * cap // NSHARE, depth)
+    rows = exchange(deal(classes), TP)
+    partial = experts(rows.reshape(-1, depth), pieces)
     back = exchange(partial.reshape(rows.shape), TP)
     picked_from = exchange(collect(back).reshape(arrived.shape), ("z", "c"))
     moe = sum(

time: 283 us -> 266 us (0.940)
  blocking collectives: 121 us -> 75.1 us
  waiting for transfers between devices: 74.3 us -> 98.8 us
  starting transfers between devices: 41.4 us -> 60.4 us
  local copies, waits for them, and re-layouts: 13.4 us -> 3.4 us
  Pallas kernels: 27.8 us -> 23.1 us
    all_to_all x5 -> x4, blocking collectives: 121 us -> 75.1 us  [exchange(): return lax.all_to_all(blocks, axis, split_axis=0, concat_axis=0, tiled=True)]
    all_to_all x1, waiting for transfers between devices: 6.54 us -> 29.7 us  [local(): lax.all_to_all(columns, TP, split_axis=0, concat_axis=1, tiled=True)]
    all_to_all x3 -> x4, starting transfers between devices: 15 us -> 29.7 us  [exchange(): return lax.all_to_all(blocks, axis, split_axis=0, concat_axis=0, tiled=True)]
    unnamed x32 -> x14, local copies, waits for them, and re-layouts: 10.4 us -> 1.43 us
    all_to_all x3 -> x4, waiting for transfers between devices: 37.4 us -> 42.4 us  [exchange(): return lax.all_to_all(blocks, axis, split_axis=0, concat_axis=0, tiled=True)]
    ppermute x4 -> x6, starting transfers between devices: 13.2 us -> 17.1 us  [ring(): return lax.ppermute(value, axis, [(i, (i + step) % 4) for i in range(4)])]
    ppermute x4 -> x6, waiting for transfers between devices: 29.2 us -> 25.6 us  [ring(): return lax.ppermute(value, axis, [(i, (i + step) % 4) for i in range(4)])]
  transfers between devices with their start and end apart: 9 -> 12, of which waited for: 6 -> 10; matrix products, arithmetic and copies ran while one was open for 0% -> 1% of each run, Pallas kernels for 1% -> 2%
where the time goes in v2:
time: 266 us; the launch traced here: 265 us
  waiting for transfers between devices  98.8 us (37%)
  blocking collectives  75.1 us (28%)
  starting transfers between devices  60.4 us (23%)
  Pallas kernels  23.1 us (9%)
  local copies, waits for them, and re-layouts  3.4 us (1%)
    all_to_all x4, blocking collectives, exchange(): return lax.all_to_all(blocks, axis, split_axis=0, concat_axis=0, tiled=True)  75.1 us
    all_to_all x4, waiting for transfers between devices, exchange(): return lax.all_to_all(blocks, axis, split_axis=0, concat_axis=0, tiled=True)  42.4 us
    all_to_all x1, waiting for transfers between devices, local(): lax.all_to_all(columns, TP, split_axis=0, concat_axis=1, tiled=True)  29.7 us
    all_to_all x4, starting transfers between devices, exchange(): return lax.all_to_all(blocks, axis, split_axis=0, concat_axis=0, tiled=True)  29.7 us
    ppermute x6, waiting for transfers between devices, ring(): return lax.ppermute(value, axis, [(i, (i + step) % 4) for i in range(4)])  25.6 us
    ppermute x6, starting transfers between devices, ring(): return lax.ppermute(value, axis, [(i, (i + step) % 4) for i in range(4)])  17.1 us
    ppermute x1, starting transfers between devices, swap_cores(): return lax.ppermute(value, 'c', [(0, 1), (1, 0)])  8.66 us
    pallas_call x1, Pallas kernels, experts(): pl.pallas_call(experts_kernel, in_specs=[IN_VMEM] + [IN_HBM] * len(pieces...  7.87 us
  transfers between devices with their start and end apart: 12, of which 10 were waited for; matrix products, arithmetic and copies ran while one was open for 1% of the time, Pallas kernels for 2%

profile of v2, /device:TPU:1, one launch (start us, length us, event | category | flops | bytes accessed | tf_op | source)
XLA Modules:
  0.0 264.5 jit_solution(11505639256721598632)
XLA Ops:
  0.0 0.6 pad_add_fusion.at_ref
  0.6 3.1 %prepare.1 = (bf16[8,256,128]{2,1,0:T(8,128)(2,1)}, bf16[16,32,256]{2,1,0:T(8,128)(2,1)}) custom-call(s32[4]{0:T(128)} %pad_add_fusion.at_ref, bf16[256,128]{1,0:T(8,128)(2,1)} %q_ref.1, bf16[256,256]{1,0:T(8,128)(2,1)} %k_ref.1, bf16[256,256]{1,0:T(8,128)(2,1)} %v_ref.1, f32[1,128]{1,0:T(1,128)} %bitcast.37, f32[1,128]{1,0:T(1,128)} %bitcast.38), custom_call_target="tpu_custom_call" | custom-call | tf_op jit(solution)/shard_map/prepare/pallas_call | solution.py:84
  3.7 13.4 %all_to_all.64.q_ref = bf16[8,256,128]{2,1,0:T(8,128)(2,1)S(1)} all-to-all(bf16[8,256,128]{2,1,0:T(8,128)(2,1)} %get-tuple-element.11), channel_id=1, replica_groups=mesh['z'=16,'c'=2,'yh'=2,'yl'=2,'x'=4] {'yl','x'}, dimensions={0} | all-to-all | bytes 1048576 | tf_op jit(solution)/shard_map/all_to_all | solution.py:39
  17.1 29.3 %all_to_all.65 = bf16[16,32,256]{2,1,0:T(8,128)(2,1)S(1)} all-to-all(bf16[16,32,256]{2,1,0:T(8,128)(2,1)} %get-tuple-element.14), channel_id=1, replica_groups=mesh['z'=16,'c'=2,'yh'=2,'yl'=2,'x'=4] {'z'}, dimensions={0} | all-to-all | bytes 524288 | tf_op jit(solution)/shard_map/all_to_all | solution.py:39
  46.4 8.7 %collective-permute-start = (bf16[512,256]{1,0:T(8,128)(2,1)S(1)}, bf16[512,256]{1,0:T(8,128)(2,1)S(1)}, u32[]{:S(2)}, u32[]{:S(2)}) collective-permute-start(bf16[512,256]{1,0:T(8,128)(2,1)S(1)} %bitcast.34), channel_id=1, source_target_pairs={{0,16},{16,0},{1,17},{17,1},{2,18},{18,2},{3,19},{19,3},{4,20},{20... | collective-permute-start | bytes 786440 | tf_op jit(solution)/shard_map/ppermute | solution.py:43
  55.0 1.1 collective-permute-done.other_ref
  56.2 5.9 %attend.1 = bf16[8,144,256]{2,1,0:T(8,128)(2,1)S(1)} custom-call(bf16[8,256,128]{2,1,0:T(8,128)(2,1)S(1)} %all_to_all.64.q_ref, bf16[512,256]{1,0:T(8,128)(2,1)S(1)} %bitcast.35, bf16[512,256]{1,0:T(8,128)(2,1)S(1)} %collective-permute-done.other_ref), custom_call_target="tpu_custom_call" | custom-call | tf_op jit(solution)/shard_map/attend/pallas_call | solution.py:131
  62.1 13.2 %all_to_all.66.parts_ref = bf16[8,144,256]{2,1,0:T(8,128)(2,1)S(1)} all-to-all(bf16[8,144,256]{2,1,0:T(8,128)(2,1)S(1)} %attend.1), channel_id=1, replica_groups=mesh['z'=16,'c'=2,'yh'=2,'yl'=2,'x'=4] {'yl','x'}, dimensions={0} | all-to-all | bytes 1179648 | tf_op jit(solution)/shard_map/all_to_all | solution.py:39
  75.2 1.2 combine.1
  76.4 4.2 %all-to-all-start.3 = ((bf16[16,128,256]{2,1,0:T(8,128)(2,1)}), bf16[16,128,256]{2,1,0:T(8,128)(2,1)S(1)}, u32[]{:S(2)}, u32[]{:S(2)}) async-start(bf16[16,128,256]{2,1,0:T(8,128)(2,1)} %combine.1), calls=%async_computation.3 | async-start | bytes 2097152 | tf_op jit(solution)/shard_map/all_to_all | solution.py:39
  80.6 0.0 copy-start.5
  80.6 4.0 %pack.1 = (bf16[384,2048]{1,0:T(8,128)(2,1)}, bf16[384,2048]{1,0:T(8,128)(2,1)}) custom-call(bf16[1,2048,256]{2,1,0:T(8,128)(2,1)} %gate_ref.1, bf16[1,2048,256]{2,1,0:T(8,128)(2,1)} %up_ref.1, bf16[1,256,2048]{2,1,0:T(8,128)(2,1)} %down_ref.1), custom_call_target="tpu_custom_call" | custom-call | tf_op jit(solution)/shard_map/pack/pallas_call | solution.py:223
  84.6 3.4 %collective-permute-start.1 = (bf16[384,2048]{1,0:T(8,128)(2,1)}, bf16[384,2048]{1,0:T(8,128)(2,1)}, u32[]{:S(2)}, u32[]{:S(2)}) collective-permute-start(bf16[384,2048]{1,0:T(8,128)(2,1)} %get-tuple-element.15.refs_0_), channel_id=1, source_target_pairs={{0,1},{1,2},{2,3},{3,0},{4,5},{5,6},{6,7},{7,4},{8,9},{9,10},{10,1... | collective-permute-start | bytes 4718600 | tf_op jit(solution)/shard_map/ppermute | solution.py:47
  88.0 3.1 %collective-permute-start.2 = (bf16[384,2048]{1,0:T(8,128)(2,1)}, bf16[384,2048]{1,0:T(8,128)(2,1)}, u32[]{:S(2)}, u32[]{:S(2)}) collective-permute-start(bf16[384,2048]{1,0:T(8,128)(2,1)} %get-tuple-element.16.refs_1_), channel_id=1, source_target_pairs={{0,4},{4,8},{8,12},{12,0},{1,5},{5,9},{9,13},{13,1},{2,6},{6,10},{... | collective-permute-start | bytes 4718600 | tf_op jit(solution)/shard_map/ppermute | solution.py:47
  91.1 0.2 convert_reduce_fusion.2
  91.4 4.4 %all-to-all-done.3 = bf16[16,128,256]{2,1,0:T(8,128)(2,1)S(1)} async-done(((bf16[16,128,256]{2,1,0:T(8,128)(2,1)}), bf16[16,128,256]{2,1,0:T(8,128)(2,1)S(1)}, u32[]{:S(2)}, u32[]{:S(2)}) %all-to-all-start.3) | async-done | bytes 1048608 | tf_op jit(solution)/shard_map/all_to_all | solution.py:39
  95.8 1.1 convolution_convert_fusion.1
  96.9 5.0 %all-to-all-start.4 = ((bf16[16,16,128]{2,1,0:T(8,128)(2,1)}), bf16[16,16,128]{2,1,0:T(8,128)(2,1)S(1)}, u32[]{:S(2)}, u32[]{:S(2)}) async-start(bf16[16,16,128]{2,1,0:T(8,128)(2,1)} %bitcast.8), calls=%async_computation.4 | async-start | bytes 131072 | tf_op jit(solution)/shard_map/all_to_all | solution.py:335
  101.9 29.7 %all-to-all-done.4 = bf16[16,16,128]{2,1,0:T(8,128)(2,1)S(1)} async-done(((bf16[16,16,128]{2,1,0:T(8,128)(2,1)}), bf16[16,16,128]{2,1,0:T(8,128)(2,1)S(1)}, u32[]{:S(2)}, u32[]{:S(2)}) %all-to-all-start.4) | async-done | bytes 65568 | tf_op jit(solution)/shard_map/all_to_all | solution.py:335
  131.7 0.1 fusion.3
  131.8 0.3 convolution_convert_fusion
  132.2 0.9 all_to_all.48
  133.0 7.2 %all-to-all-start.5 = ((bf16[32,2,2048]{2,1,0:T(2,128)(2,1)}), bf16[32,2,2048]{2,1,0:T(2,128)(2,1)S(1)}, u32[]{:S(2)}, u32[]{:S(2)}) async-start(bf16[32,2,2048]{2,1,0:T(2,128)(2,1)} %all_to_all.48), calls=%async_computation.5 | async-start | bytes 524288 | tf_op jit(solution)/shard_map/all_to_all | solution.py:39
  140.2 2.4 collective-permute-start.3
  142.6 2.8 %collective-permute-start.4 = (bf16[384,2048]{1,0:T(8,128)(2,1)}, bf16[384,2048]{1,0:T(8,128)(2,1)}, u32[]{:S(2)}, u32[]{:S(2)}) collective-permute-start(bf16[384,2048]{1,0:T(8,128)(2,1)} %get-tuple-element.16.refs_1_), channel_id=1, source_target_pairs={{0,12},{4,0},{8,4},{12,8},{1,13},{5,1},{9,5},{13,9},{2,14},{6,2},{... | collective-permute-start | bytes 4718600 | tf_op jit(solution)/shard_map/ppermute | solution.py:47
  145.4 0.0 collective-permute-done.1.refs_2_
  145.4 2.9 %collective-permute-start.5 = (bf16[384,2048]{1,0:T(8,128)(2,1)}, bf16[384,2048]{1,0:T(8,128)(2,1)}, u32[]{:S(2)}, u32[]{:S(2)}) collective-permute-start(bf16[384,2048]{1,0:T(8,128)(2,1)} %collective-permute-done.1.refs_2_), channel_id=1, source_target_pairs={{0,1},{1,2},{2,3},{3,0},{4,5},{5,6},{6,7},{7,4},{8,9},{9,10},{10,1... | collective-permute-start | bytes 4718600 | tf_op jit(solution)/shard_map/ppermute | solution.py:47
  148.3 0.0 collective-permute-done.2.refs_3_
  148.3 2.5 collective-permute-start.6
  150.9 11.6 %all-to-all-done.5 = bf16[32,2,2048]{2,1,0:T(2,128)(2,1)S(1)} async-done(((bf16[32,2,2048]{2,1,0:T(2,128)(2,1)}), bf16[32,2,2048]{2,1,0:T(2,128)(2,1)S(1)}, u32[]{:S(2)}, u32[]{:S(2)}) %all-to-all-start.5) | async-done | bytes 262176 | tf_op jit(solution)/shard_map/all_to_all | solution.py:39
  162.5 0.1 reshape.72.classes_ref
  162.6 1.0 deal.1
  163.6 3.8 %all-to-all-start.6 = ((bf16[16,16,2048]{2,1,0:T(8,128)(2,1)}), bf16[16,16,2048]{2,1,0:T(8,128)(2,1)S(1)}, u32[]{:S(2)}, u32[]{:S(2)}) async-start(bf16[16,16,2048]{2,1,0:T(8,128)(2,1)} %deal.1), calls=%async_computation.6 | async-start | bytes 2097152 | tf_op jit(solution)/shard_map/all_to_all | solution.py:39
  167.5 10.5 %collective-permute-done.3.refs_4_ = bf16[384,2048]{1,0:T(8,128)(2,1)} collective-permute-done((bf16[384,2048]{1,0:T(8,128)(2,1)S(1)}, bf16[384,2048]{1,0:T(8,128)(2,1)}, u32[]{:S(2)}, u32[]{:S(2)}) %collective-permute-start.3) | collective-permute-done | bytes 1572896 | tf_op jit(solution)/shard_map/ppermute | solution.py:47
  178.0 2.3 collective-permute-done.4.refs_5_
  180.3 4.8 %collective-permute-done.5.refs_6_ = bf16[384,2048]{1,0:T(8,128)(2,1)} collective-permute-done((bf16[384,2048]{1,0:T(8,128)(2,1)}, bf16[384,2048]{1,0:T(8,128)(2,1)}, u32[]{:S(2)}, u32[]{:S(2)}) %collective-permute-start.5) | collective-permute-done | bytes 1572896 | tf_op jit(solution)/shard_map/ppermute | solution.py:47
  185.1 7.9 %collective-permute-done.6.refs_7_ = bf16[384,2048]{1,0:T(8,128)(2,1)} collective-permute-done((bf16[384,2048]{1,0:T(8,128)(2,1)}, bf16[384,2048]{1,0:T(8,128)(2,1)}, u32[]{:S(2)}, u32[]{:S(2)}) %collective-permute-start.6) | collective-permute-done | bytes 1572896 | tf_op jit(solution)/shard_map/ppermute | solution.py:47
  193.0 4.1 %all-to-all-done.6 = bf16[16,16,2048]{2,1,0:T(8,128)(2,1)S(1)} async-done(((bf16[16,16,2048]{2,1,0:T(8,128)(2,1)}), bf16[16,16,2048]{2,1,0:T(8,128)(2,1)S(1)}, u32[]{:S(2)}, u32[]{:S(2)}) %all-to-all-start.6) | async-done | bytes 1048608 | tf_op jit(solution)/shard_map/all_to_all | solution.py:39
  197.2 1.4 copy-done.2
  198.6 7.9 %experts.1 = bf16[256,2048]{1,0:T(8,128)(2,1)S(1)} custom-call(bf16[256,2048]{1,0:T(8,128)(2,1)S(1)} %bitcast.32, bf16[384,2048]{1,0:T(8,128)(2,1)S(1)} %copy-done.1, bf16[384,2048]{1,0:T(8,128)(2,1)S(1)} %copy-done.2, bf16[384,2048]{1,0:T(8,128)(2,1)} %collective-permute-done.1.refs_2_, bf16[384,2048]{1,0:T(8,128)(2,1)} %collective-permute-done.2.refs_3_, ...), custom_call_target="tpu_custom_call" | custom-call | tf_op jit(solution)/shard_map/experts/pallas_call | solution.py:276
  206.4 19.2 %all_to_all.67.back_ref = bf16[16,16,2048]{2,1,0:T(8,128)(2,1)S(1)} all-to-all(bf16[16,16,2048]{2,1,0:T(8,128)(2,1)S(1)} %bitcast.33), channel_id=1, replica_groups=mesh['z'=16,'c'=2,'yh'=2,'yl'=2,'x'=4] {'yh','yl','x'}, dimensions={0} | all-to-all | bytes 2097152 | tf_op jit(solution)/shard_map/all_to_all | solution.py:39
  225.6 0.1 collect.1
  225.8 0.9 all_to_all.52
  226.6 14.4 %all-to-all-start.8 = ((bf16[32,2,2048]{2,1,0:T(2,128)(2,1)}), bf16[32,2,2048]{2,1,0:T(2,128)(2,1)S(1)}, u32[]{:S(2)}, u32[]{:S(2)}) async-start(bf16[32,2,2048]{2,1,0:T(2,128)(2,1)} %all_to_all.52), calls=%async_computation.8 | async-start | bytes 524288 | tf_op jit(solution)/shard_map/all_to_all | solution.py:39
  241.1 22.2 %all-to-all-done.8 = bf16[32,2,2048]{2,1,0:T(2,128)(2,1)S(1)} async-done(((bf16[32,2,2048]{2,1,0:T(2,128)(2,1)}), bf16[32,2,2048]{2,1,0:T(2,128)(2,1)S(1)}, u32[]{:S(2)}, u32[]{:S(2)}) %all-to-all-start.8) | async-done | bytes 262176 | tf_op jit(solution)/shard_map/all_to_all | solution.py:39
  263.3 0.1 all_to_all.54
  263.4 0.2 convolution_multiply_fusion.1
  263.6 0.9 fusion.2
  (18 shorter events, 0.1 us)
Async XLA Ops:
  0.0 95.8 %copy-start = (bf16[2048,128]{1,0:T(8,128)(2,1)S(1)}, bf16[2048,128]{1,0:T(8,128)(2,1)}, u32[]{:S(2)}) copy-start(bf16[2048,128]{1,0:T(8,128)(2,1)} %param.18) | copy-start | bytes 1572868
  46.4 9.8 %collective-permute-start = (bf16[512,256]{1,0:T(8,128)(2,1)S(1)}, bf16[512,256]{1,0:T(8,128)(2,1)S(1)}, u32[]{:S(2)}, u32[]{:S(2)}) collective-permute-start(bf16[512,256]{1,0:T(8,128)(2,1)S(1)} %bitcast.34), channel_id=1, source_target_pairs={{0,16},{16,0},{1,17},{17,1},{2,18},{18,2},{3,19},{19,3},{4,20},{20... | collective-permute-start | bytes 786440 | tf_op jit(solution)/shard_map/ppermute | solution.py:43
  76.4 19.4 %all-to-all-start.3 = ((bf16[16,128,256]{2,1,0:T(8,128)(2,1)}), bf16[16,128,256]{2,1,0:T(8,128)(2,1)S(1)}, u32[]{:S(2)}, u32[]{:S(2)}) async-start(bf16[16,128,256]{2,1,0:T(8,128)(2,1)} %combine.1), calls=%async_computation.3 | async-start | bytes 2097152 | tf_op jit(solution)/shard_map/all_to_all | solution.py:39
  80.6 10.5 %copy-start.5 = (s32[16,2]{0,1:T(2,128)S(1)}, s32[16,2]{0,1:T(2,128)}, u32[]{:S(2)}) copy-start(s32[16,2]{0,1:T(2,128)} %param.21) | copy-start | bytes 388
  84.6 47.1 %copy-start.3 = (bf16[16,2048]{1,0:T(8,128)(2,1)S(1)}, bf16[16,2048]{1,0:T(8,128)(2,1)}, u32[]{:S(2)}) copy-start(bf16[16,2048]{1,0:T(8,128)(2,1)} %param.20) | copy-start | bytes 196612
  84.6 47.2 %copy-start.4 = (f32[2048]{0:T(1024)S(1)}, f32[2048]{0:T(1024)}, u32[]{:S(2)}) copy-start(f32[2048]{0:T(1024)} %param.19) | copy-start | bytes 24580
  84.6 60.8 %collective-permute-start.1 = (bf16[384,2048]{1,0:T(8,128)(2,1)}, bf16[384,2048]{1,0:T(8,128)(2,1)}, u32[]{:S(2)}, u32[]{:S(2)}) collective-permute-start(bf16[384,2048]{1,0:T(8,128)(2,1)} %get-tuple-element.15.refs_0_), channel_id=1, source_target_pairs={{0,1},{1,2},{2,3},{3,0},{4,5},{5,6},{6,7},{7,4},{8,9},{9,10},{10,1... | collective-permute-start | bytes 4718600 | tf_op jit(solution)/shard_map/ppermute | solution.py:47
  88.0 60.3 %collective-permute-start.2 = (bf16[384,2048]{1,0:T(8,128)(2,1)}, bf16[384,2048]{1,0:T(8,128)(2,1)}, u32[]{:S(2)}, u32[]{:S(2)}) collective-permute-start(bf16[384,2048]{1,0:T(8,128)(2,1)} %get-tuple-element.16.refs_1_), channel_id=1, source_target_pairs={{0,4},{4,8},{8,12},{12,0},{1,5},{5,9},{9,13},{13,1},{2,6},{6,10},{... | collective-permute-start | bytes 4718600 | tf_op jit(solution)/shard_map/ppermute | solution.py:47
  95.8 44.4 %copy-start.1 = (bf16[384,2048]{1,0:T(8,128)(2,1)S(1)}, bf16[384,2048]{1,0:T(8,128)(2,1)}, u32[]{:S(2)}) copy-start(bf16[384,2048]{1,0:T(8,128)(2,1)} %get-tuple-element.15.refs_0_) | copy-start | bytes 4718596
  96.9 34.8 %all-to-all-start.4 = ((bf16[16,16,128]{2,1,0:T(8,128)(2,1)}), bf16[16,16,128]{2,1,0:T(8,128)(2,1)S(1)}, u32[]{:S(2)}, u32[]{:S(2)}) async-start(bf16[16,16,128]{2,1,0:T(8,128)(2,1)} %bitcast.8), calls=%async_computation.4 | async-start | bytes 131072 | tf_op jit(solution)/shard_map/all_to_all | solution.py:335
  133.0 29.5 %all-to-all-start.5 = ((bf16[32,2,2048]{2,1,0:T(2,128)(2,1)}), bf16[32,2,2048]{2,1,0:T(2,128)(2,1)S(1)}, u32[]{:S(2)}, u32[]{:S(2)}) async-start(bf16[32,2,2048]{2,1,0:T(2,128)(2,1)} %all_to_all.48), calls=%async_computation.5 | async-start | bytes 524288 | tf_op jit(solution)/shard_map/all_to_all | solution.py:39
  140.2 37.7 %collective-permute-start.3 = (bf16[384,2048]{1,0:T(8,128)(2,1)S(1)}, bf16[384,2048]{1,0:T(8,128)(2,1)}, u32[]{:S(2)}, u32[]{:S(2)}) collective-permute-start(bf16[384,2048]{1,0:T(8,128)(2,1)S(1)} %copy-done.1), channel_id=1, source_target_pairs={{0,3},{1,0},{2,1},{3,2},{4,7},{5,4},{6,5},{7,6},{8,11},{9,8},{10,9... | collective-permute-start | bytes 4718600 | tf_op jit(solution)/shard_map/ppermute | solution.py:47
  142.6 37.6 %collective-permute-start.4 = (bf16[384,2048]{1,0:T(8,128)(2,1)}, bf16[384,2048]{1,0:T(8,128)(2,1)}, u32[]{:S(2)}, u32[]{:S(2)}) collective-permute-start(bf16[384,2048]{1,0:T(8,128)(2,1)} %get-tuple-element.16.refs_1_), channel_id=1, source_target_pairs={{0,12},{4,0},{8,4},{12,8},{1,13},{5,1},{9,5},{13,9},{2,14},{6,2},{... | collective-permute-start | bytes 4718600 | tf_op jit(solution)/shard_map/ppermute | solution.py:47
  145.4 39.6 %collective-permute-start.5 = (bf16[384,2048]{1,0:T(8,128)(2,1)}, bf16[384,2048]{1,0:T(8,128)(2,1)}, u32[]{:S(2)}, u32[]{:S(2)}) collective-permute-start(bf16[384,2048]{1,0:T(8,128)(2,1)} %collective-permute-done.1.refs_2_), channel_id=1, source_target_pairs={{0,1},{1,2},{2,3},{3,0},{4,5},{5,6},{6,7},{7,4},{8,9},{9,10},{10,1... | collective-permute-start | bytes 4718600 | tf_op jit(solution)/shard_map/ppermute | solution.py:47
  148.3 44.7 %collective-permute-start.6 = (bf16[384,2048]{1,0:T(8,128)(2,1)}, bf16[384,2048]{1,0:T(8,128)(2,1)}, u32[]{:S(2)}, u32[]{:S(2)}) collective-permute-start(bf16[384,2048]{1,0:T(8,128)(2,1)} %collective-permute-done.2.refs_3_), channel_id=1, source_target_pairs={{0,4},{4,8},{8,12},{12,0},{1,5},{5,9},{9,13},{13,1},{2,6},{6,10},{... | collective-permute-start | bytes 4718600 | tf_op jit(solution)/shard_map/ppermute | solution.py:47
  163.6 33.5 %all-to-all-start.6 = ((bf16[16,16,2048]{2,1,0:T(8,128)(2,1)}), bf16[16,16,2048]{2,1,0:T(8,128)(2,1)S(1)}, u32[]{:S(2)}, u32[]{:S(2)}) async-start(bf16[16,16,2048]{2,1,0:T(8,128)(2,1)} %deal.1), calls=%async_computation.6 | async-start | bytes 2097152 | tf_op jit(solution)/shard_map/all_to_all | solution.py:39
  197.2 1.4 copy-start.2
  225.6 15.5 %copy-start.6 = (f32[16,2]{0,1:T(2,128)S(1)}, f32[16,2]{0,1:T(2,128)}, u32[]{:S(2)}) copy-start(f32[16,2]{0,1:T(2,128)} %param.22) | copy-start | bytes 388
  226.6 36.7 %all-to-all-start.8 = ((bf16[32,2,2048]{2,1,0:T(2,128)(2,1)}), bf16[32,2,2048]{2,1,0:T(2,128)(2,1)S(1)}, u32[]{:S(2)}, u32[]{:S(2)}) async-start(bf16[32,2,2048]{2,1,0:T(2,128)(2,1)} %all_to_all.52), calls=%async_computation.8 | async-start | bytes 524288 | tf_op jit(solution)/shard_map/all_to_all | solution.py:39

commit v3 on v2

--- a/solution.py
+++ b/solution.py
@@ -209,81 +209,89 @@
 
 
 def pack_kernel(gate_ref, up_ref, down_ref, *out_refs):
-    packed = jnp.concatenate([gate_ref[0].T, up_ref[0].T, down_ref[0]], axis=0)
-    for half, out_ref in enumerate(out_refs):
+    gate_up = jnp.concatenate([gate_ref[0].T, up_ref[0].T], axis=0)
+    for half in range(2):
         @pl.when(pl.program_id(0) == half)
         def _():
-            out_ref[...] = packed
+            out_refs[half][...] = gate_up
+            out_refs[2 + half][...] = down_ref[0]
 
 
 def pack(w_gate, w_up, w_down):
     _, depth, units = w_gate.shape
     wide = pl.BlockSpec((1, depth, SHARE), lambda i: (0, 0, i))
-    shape = (3 * SHARE, depth)
-    return pl.pallas_call(
+    shapes = [(2 * SHARE, depth)] * 2 + [(SHARE, depth)] * 2
+    outs = pl.pallas_call(
         pack_kernel,
         grid=(units // SHARE,),
         in_specs=[wide, wide, pl.BlockSpec((1, SHARE, depth), lambda i: (0, i, 0))],
-        out_specs=[pl.BlockSpec(shape, lambda i: (0, 0))] * 2,
-        out_shape=[jax.ShapeDtypeStruct(shape, BF)] * 2,
+        out_specs=[pl.BlockSpec(shape, lambda i: (0, 0)) for shape in shapes],
+        out_shape=[jax.ShapeDtypeStruct(shape, BF) for shape in shapes],
         name="pack",
     )(w_gate, w_up, w_down)
+    return outs[:2], outs[2:]
 
 
 def experts_kernel(rows_ref, *refs):
-    pieces, (out_ref, held, acc, sems) = refs[:-4], refs[-4:]
-    pairs = len(pieces) // 2
+    pieces, (out_ref, ups, downs, acc, sems) = refs[:-5], refs[-5:]
+    count = len(pieces) // 4
+    copies = []
+    for p in range(count):
+        for i in range(2):
+            copies.append((pieces[2 * p + i], ups.at[p, pl.ds(2 * i * SHARE, 2 * SHARE)]))
+        for i in range(2):
+            copies.append(
+                (pieces[2 * (count + p) + i], downs.at[p, pl.ds(i * SHARE, SHARE)])
+            )
     copies = [
-        pltpu.make_async_copy(
-            pieces[2 * p + i].at[pl.ds(j * SHARE, SHARE)],
-            held.at[p, j, pl.ds(i * SHARE, SHARE)],
-            sems.at[p, j, i],
+        pltpu.make_async_copy(source, target, sems.at[i])
+        for i, (source, target) in enumerate(copies)
+    ]
+    for copy in copies[:8]:
+        copy.start()
+    for p in range(count):
+        for copy in copies[4 * p : 4 * p + 2]:
+            copy.wait()
+        both = lax.dot_general(
+            ups[p], rows_ref[...], (((1,), (1,)), ((), ())), preferred_element_type=F32
         )
-        for p in range(pairs)
-        for j in range(3)
-        for i in range(2)
-    ]
-    for copy in copies[:12]:
-        copy.start()
-    across = (((1,), (1,)), ((), ()))
-    for p in range(pairs):
-        gate_up = []
-        for j in range(2):
-            for copy in copies[6 * p + 2 * j : 6 * p + 2 * j + 2]:
-                copy.wait()
-            gate_up.append(
-                lax.dot_general(
-                    rows_ref[...], held[p, j], across, preferred_element_type=F32
-                )
-            )
-        gate, upper = gate_up
-        hidden = (gate / (1.0 + jnp.exp(-gate)) * upper).astype(BF)
-        for copy in copies[6 * p + 4 : 6 * p + 6]:
+        for copy in copies[4 * (p + 2) : 4 * (p + 3)]:
+            copy.start()
+        hidden = []
+        for i in range(2):
+            gate = both[2 * i * SHARE : (2 * i + 1) * SHARE]
+            upper = both[(2 * i + 1) * SHARE : (2 * i + 2) * SHARE]
+            hidden.append((gate / (1.0 + jnp.exp(-gate)) * upper).astype(BF))
+        for copy in copies[4 * p + 2 : 4 * p + 4]:
             copy.wait()
-        for copy in copies[6 * (p + 2) : 6 * (p + 3)]:
-            copy.start()
-        part = jnp.dot(hidden, held[p, 2], preferred_element_type=F32)
+        part = lax.dot_general(
+            jnp.concatenate(hidden, axis=0),
+            downs[p],
+            (((0,), (0,)), ((), ())),
+            preferred_element_type=F32,
+        )
         if p == 0:
             acc[...] = part
-        elif p < pairs - 1:
+        elif p < count - 1:
             acc[...] += part
         else:
             out_ref[...] = (acc[...] + part).astype(BF)
 
 
 def experts(rows, pieces):
-    depth = rows.shape[1]
+    count, depth = len(pieces) // 4, rows.shape[1]
     return pl.pallas_call(
         experts_kernel,
         in_specs=[IN_VMEM] + [IN_HBM] * len(pieces),
         out_specs=IN_VMEM,
         out_shape=jax.ShapeDtypeStruct(rows.shape, BF),
         scratch_shapes=[
-            pltpu.VMEM((len(pieces) // 2, 3, 2 * SHARE, depth), BF),
+            pltpu.VMEM((count, 4 * SHARE, depth), BF),
+            pltpu.VMEM((count, 2 * SHARE, depth), BF),
             pltpu.VMEM(rows.shape, F32),
-            pltpu.SemaphoreType.DMA((len(pieces) // 2, 3, 2)),
+            pltpu.SemaphoreType.DMA((len(pieces),)),
         ],
-        compiler_params=grant(32),
+        compiler_params=grant(54),
         name="experts",
     )(rows, *pieces)
 
@@ -319,12 +327,14 @@
     kv_mine = exchange(kv, "z").reshape(-1, 2 * width)
     kv_other = swap_cores(kv_mine)
 
-    packs = pack(w_gate, w_up, w_down)
+    ups, downs = pack(w_gate, w_up, w_down)
     axes = ("x", ("yh", "yl"))
-    left = [ring(p, axis, 1) for p, axis in zip(packs, axes)]
-    right = [ring(p, axis, -1) for p, axis in zip(packs, axes)]
-    far = [ring(p, axis, 1) for p, axis in zip(left, axes)]
-    pieces = [*packs, *left, *right, *far]
+    pieces = []
+    for packs in (ups, downs):
+        left = [ring(p, axis, 1) for p, axis in zip(packs, axes)]
+        right = [ring(p, axis, -1) for p, axis in zip(packs, axes)]
+        last = [ring(p, axis, 1) for p, axis in zip(left, axes)]
+        pieces += [*packs, *left, *right, *last]
 
     parts = attend(q8, kv_mine, kv_other)
     parts = exchange(parts, GROUP)

time: 266 us -> 289 us (1.086)
  starting transfers between devices: 60.4 us -> 82.6 us
  Pallas kernels: 23.1 us -> 27.1 us
    all_to_all x4, waiting for transfers between devices: 42.4 us -> 23.7 us  [exchange(): return lax.all_to_all(blocks, axis, split_axis=0, concat_axis=0, tiled=True)]
    ppermute x6 -> x12, starting transfers between devices: 17.1 us -> 34.2 us  [ring(): return lax.ppermute(value, axis, [(i, (i + step) % 4) for i in range(4)])]
    ppermute x6 -> x12, waiting for transfers between devices: 25.6 us -> 41.6 us  [ring(): return lax.ppermute(value, axis, [(i, (i + step) % 4) for i in range(4)])]
    all_to_all x4, starting transfers between devices: 29.7 us -> 34.6 us  [exchange(): return lax.all_to_all(blocks, axis, split_axis=0, concat_axis=0, tiled=True)]
    pallas_call x1, Pallas kernels: 7.87 us -> 11.7 us  [experts(): pl.pallas_call(experts_kernel, in_specs=[IN_VMEM] + [IN_HBM] * len(pieces...]
  transfers between devices with their start and end apart: 12 -> 18, of which waited for: 10 -> 6; matrix products, arithmetic and copies ran while one was open for 1% -> 1% of each run, Pallas kernels for 2% -> 2%
where the time goes in v3:
time: 289 us; the launch traced here: 288 us
  waiting for transfers between devices  96.1 us (33%)
  starting transfers between devices  82.6 us (29%)
  blocking collectives  74.5 us (26%)
  Pallas kernels  27.1 us (9%)
  local copies, waits for them, and re-layouts  3.9 us (1%)
    all_to_all x4, blocking collectives, exchange(): return lax.all_to_all(blocks, axis, split_axis=0, concat_axis=0, tiled=True)  74.5 us
    ppermute x12, waiting for transfers between devices, ring(): return lax.ppermute(value, axis, [(i, (i + step) % 4) for i in range(4)])  41.6 us
    all_to_all x4, starting transfers between devices, exchange(): return lax.all_to_all(blocks, axis, split_axis=0, concat_axis=0, tiled=True)  34.6 us
    ppermute x12, starting transfers between devices, ring(): return lax.ppermute(value, axis, [(i, (i + step) % 4) for i in range(4)])  34.2 us
    all_to_all x1, waiting for transfers between devices, local(): lax.all_to_all(columns, TP, split_axis=0, concat_axis=1, tiled=True)  29.6 us
    all_to_all x4, waiting for transfers between devices, exchange(): return lax.all_to_all(blocks, axis, split_axis=0, concat_axis=0, tiled=True)  23.7 us
    pallas_call x1, Pallas kernels, experts(): pl.pallas_call(experts_kernel, in_specs=[IN_VMEM] + [IN_HBM] * len(pieces...  11.7 us
    ppermute x1, starting transfers between devices, swap_cores(): return lax.ppermute(value, 'c', [(0, 1), (1, 0)])  8.66 us
  transfers between devices with their start and end apart: 18, of which 6 were waited for; matrix products, arithmetic and copies ran while one was open for 1% of the time, Pallas kernels for 2%

profile of v3, /device:TPU:1, one launch (start us, length us, event | category | flops | bytes accessed | tf_op | source)
XLA Modules:
  0.0 288.2 jit_solution(801214357982242269)
XLA Ops:
  0.0 0.7 pad_add_fusion.at_ref
  0.7 3.1 %prepare.1 = (bf16[8,256,128]{2,1,0:T(8,128)(2,1)}, bf16[16,32,256]{2,1,0:T(8,128)(2,1)}) custom-call(s32[4]{0:T(128)} %pad_add_fusion.at_ref, bf16[256,128]{1,0:T(8,128)(2,1)} %q_ref.1, bf16[256,256]{1,0:T(8,128)(2,1)} %k_ref.1, bf16[256,256]{1,0:T(8,128)(2,1)} %v_ref.1, f32[1,128]{1,0:T(1,128)} %bitcast.37, f32[1,128]{1,0:T(1,128)} %bitcast.38), custom_call_target="tpu_custom_call" | custom-call | tf_op jit(solution)/shard_map/prepare/pallas_call | solution.py:84
  3.8 13.5 %all_to_all.64.q_ref = bf16[8,256,128]{2,1,0:T(8,128)(2,1)S(1)} all-to-all(bf16[8,256,128]{2,1,0:T(8,128)(2,1)} %get-tuple-element.13), channel_id=1, replica_groups=mesh['z'=16,'c'=2,'yh'=2,'yl'=2,'x'=4] {'yl','x'}, dimensions={0} | all-to-all | bytes 1048576 | tf_op jit(solution)/shard_map/all_to_all | solution.py:39
  17.3 29.1 %all_to_all.65 = bf16[16,32,256]{2,1,0:T(8,128)(2,1)S(1)} all-to-all(bf16[16,32,256]{2,1,0:T(8,128)(2,1)S(1)} %copy-done.10), channel_id=1, replica_groups=mesh['z'=16,'c'=2,'yh'=2,'yl'=2,'x'=4] {'z'}, dimensions={0} | all-to-all | bytes 524288 | tf_op jit(solution)/shard_map/all_to_all | solution.py:39
  46.4 8.7 %collective-permute-start = (bf16[512,256]{1,0:T(8,128)(2,1)S(1)}, bf16[512,256]{1,0:T(8,128)(2,1)S(1)}, u32[]{:S(2)}, u32[]{:S(2)}) collective-permute-start(bf16[512,256]{1,0:T(8,128)(2,1)S(1)} %bitcast.32), channel_id=1, source_target_pairs={{0,16},{16,0},{1,17},{17,1},{2,18},{18,2},{3,19},{19,3},{4,20},{20... | collective-permute-start | bytes 786440 | tf_op jit(solution)/shard_map/ppermute | solution.py:43
  55.1 1.1 collective-permute-done.other_ref
  56.2 5.9 %attend.1 = bf16[8,144,256]{2,1,0:T(8,128)(2,1)S(1)} custom-call(bf16[8,256,128]{2,1,0:T(8,128)(2,1)S(1)} %all_to_all.64.q_ref, bf16[512,256]{1,0:T(8,128)(2,1)S(1)} %bitcast.33, bf16[512,256]{1,0:T(8,128)(2,1)S(1)} %collective-permute-done.other_ref), custom_call_target="tpu_custom_call" | custom-call | tf_op jit(solution)/shard_map/attend/pallas_call | solution.py:131
  62.1 13.2 %all_to_all.66.parts_ref = bf16[8,144,256]{2,1,0:T(8,128)(2,1)S(1)} all-to-all(bf16[8,144,256]{2,1,0:T(8,128)(2,1)S(1)} %attend.1), channel_id=1, replica_groups=mesh['z'=16,'c'=2,'yh'=2,'yl'=2,'x'=4] {'yl','x'}, dimensions={0} | all-to-all | bytes 1179648 | tf_op jit(solution)/shard_map/all_to_all | solution.py:39
  75.3 1.2 combine.1
  76.5 4.2 %all-to-all-start.3 = ((bf16[16,128,256]{2,1,0:T(8,128)(2,1)}), bf16[16,128,256]{2,1,0:T(8,128)(2,1)S(1)}, u32[]{:S(2)}, u32[]{:S(2)}) async-start(bf16[16,128,256]{2,1,0:T(8,128)(2,1)} %combine.1), calls=%async_computation.3 | async-start | bytes 2097152 | tf_op jit(solution)/shard_map/all_to_all | solution.py:39
  80.7 4.0 %pack.1 = (bf16[256,2048]{1,0:T(8,128)(2,1)}, bf16[256,2048]{1,0:T(8,128)(2,1)}, bf16[128,2048]{1,0:T(8,128)(2,1)}, bf16[128,2048]{1,0:T(8,128)(2,1)}) custom-call(bf16[1,2048,256]{2,1,0:T(8,128)(2,1)} %gate_ref.1, bf16[1,2048,256]{2,1,0:T(8,128)(2,1)} %up_ref.1, bf16[1,256,2048]{2,1,0:T(8,128)(2,1)} %down_ref.1), custom_call_target="tpu_custom_call" | custom-call | tf_op jit(solution)/shard_map/pack/pallas_call | solution.py:224
  84.7 3.3 %collective-permute-start.1 = (bf16[256,2048]{1,0:T(8,128)(2,1)}, bf16[256,2048]{1,0:T(8,128)(2,1)}, u32[]{:S(2)}, u32[]{:S(2)}) collective-permute-start(bf16[256,2048]{1,0:T(8,128)(2,1)} %get-tuple-element.17.refs_0_), channel_id=1, source_target_pairs={{0,1},{1,2},{2,3},{3,0},{4,5},{5,6},{6,7},{7,4},{8,9},{9,10},{10,1... | collective-permute-start | bytes 3145736 | tf_op jit(solution)/shard_map/ppermute | solution.py:47
  87.9 3.1 %collective-permute-start.2 = (bf16[256,2048]{1,0:T(8,128)(2,1)}, bf16[256,2048]{1,0:T(8,128)(2,1)}, u32[]{:S(2)}, u32[]{:S(2)}) collective-permute-start(bf16[256,2048]{1,0:T(8,128)(2,1)} %get-tuple-element.18.refs_1_), channel_id=1, source_target_pairs={{0,4},{4,8},{8,12},{12,0},{1,5},{5,9},{9,13},{13,1},{2,6},{6,10},{... | collective-permute-start | bytes 3145736 | tf_op jit(solution)/shard_map/ppermute | solution.py:47
  91.0 3.1 %collective-permute-start.7 = (bf16[128,2048]{1,0:T(8,128)(2,1)}, bf16[128,2048]{1,0:T(8,128)(2,1)}, u32[]{:S(2)}, u32[]{:S(2)}) collective-permute-start(bf16[128,2048]{1,0:T(8,128)(2,1)} %get-tuple-element.19.refs_8_), channel_id=1, source_target_pairs={{0,1},{1,2},{2,3},{3,0},{4,5},{5,6},{6,7},{7,4},{8,9},{9,10},{10,1... | collective-permute-start | bytes 1572872 | tf_op jit(solution)/shard_map/ppermute | solution.py:47
  94.2 0.2 convert_reduce_fusion.2
  94.4 1.5 all-to-all-done.3
  95.9 1.1 convolution_convert_fusion.1
  97.0 5.1 %all-to-all-start.4 = ((bf16[16,16,128]{2,1,0:T(8,128)(2,1)}), bf16[16,16,128]{2,1,0:T(8,128)(2,1)S(1)}, u32[]{:S(2)}, u32[]{:S(2)}) async-start(bf16[16,16,128]{2,1,0:T(8,128)(2,1)} %bitcast.8), calls=%async_computation.4 | async-start | bytes 131072 | tf_op jit(solution)/shard_map/all_to_all | solution.py:345
  102.1 29.6 %all-to-all-done.4 = bf16[16,16,128]{2,1,0:T(8,128)(2,1)S(1)} async-done(((bf16[16,16,128]{2,1,0:T(8,128)(2,1)}), bf16[16,16,128]{2,1,0:T(8,128)(2,1)S(1)}, u32[]{:S(2)}, u32[]{:S(2)}) %all-to-all-start.4) | async-done | bytes 65568 | tf_op jit(solution)/shard_map/all_to_all | solution.py:345
  131.7 0.1 fusion.3
  131.9 0.3 convolution_convert_fusion
  132.2 0.9 all_to_all.48
  133.1 7.2 %all-to-all-start.5 = ((bf16[32,2,2048]{2,1,0:T(2,128)(2,1)}), bf16[32,2,2048]{2,1,0:T(2,128)(2,1)S(1)}, u32[]{:S(2)}, u32[]{:S(2)}) async-start(bf16[32,2,2048]{2,1,0:T(2,128)(2,1)} %all_to_all.48), calls=%async_computation.5 | async-start | bytes 524288 | tf_op jit(solution)/shard_map/all_to_all | solution.py:39
  140.3 2.1 collective-permute-start.8
  142.5 4.3 %collective-permute-start.10 = (bf16[128,2048]{1,0:T(8,128)(2,1)S(1)}, bf16[128,2048]{1,0:T(8,128)(2,1)S(1)}, u32[]{:S(2)}, u32[]{:S(2)}) collective-permute-start(bf16[128,2048]{1,0:T(8,128)(2,1)S(1)} %copy-done.4), channel_id=1, source_target_pairs={{0,12},{4,0},{8,4},{12,8},{1,13},{5,1},{9,5},{13,9},{2,14},{6,2},{... | collective-permute-start | bytes 1572872 | tf_op jit(solution)/shard_map/ppermute | solution.py:47
  146.9 2.4 collective-permute-start.9
  149.2 7.4 %collective-permute-done.8.refs_11_ = bf16[128,2048]{1,0:T(8,128)(2,1)S(1)} collective-permute-done((bf16[128,2048]{1,0:T(8,128)(2,1)S(1)}, bf16[128,2048]{1,0:T(8,128)(2,1)S(1)}, u32[]{:S(2)}, u32[]{:S(2)}) %collective-permute-start.8) | collective-permute-done | bytes 524320 | tf_op jit(solution)/shard_map/ppermute | solution.py:47
  156.7 2.4 collective-permute-start.3
  159.1 2.9 %collective-permute-start.11 = (bf16[128,2048]{1,0:T(8,128)(2,1)}, bf16[128,2048]{1,0:T(8,128)(2,1)}, u32[]{:S(2)}, u32[]{:S(2)}) collective-permute-start(bf16[128,2048]{1,0:T(8,128)(2,1)} %collective-permute-done.7.refs_10_), channel_id=1, source_target_pairs={{0,1},{1,2},{2,3},{3,0},{4,5},{5,6},{6,7},{7,4},{8,9},{9,10},{10,1... | collective-permute-start | bytes 1572872 | tf_op jit(solution)/shard_map/ppermute | solution.py:47
  162.0 2.8 collective-permute-start.4
  164.9 2.2 collective-permute-start.5
  167.1 2.2 collective-permute-start.6
  169.3 0.1 reshape.72.classes_ref
  169.4 1.1 deal.1
  170.5 7.2 %all-to-all-start.6 = ((bf16[16,16,2048]{2,1,0:T(8,128)(2,1)}), bf16[16,16,2048]{2,1,0:T(8,128)(2,1)S(1)}, u32[]{:S(2)}, u32[]{:S(2)}) async-start(bf16[16,16,2048]{2,1,0:T(8,128)(2,1)} %deal.1), calls=%async_computation.6 | async-start | bytes 2097152 | tf_op jit(solution)/shard_map/all_to_all | solution.py:39
  177.8 3.5 %collective-permute-start.12 = (bf16[128,2048]{1,0:T(8,128)(2,1)S(1)}, bf16[128,2048]{1,0:T(8,128)(2,1)S(1)}, u32[]{:S(2)}, u32[]{:S(2)}) collective-permute-start(bf16[128,2048]{1,0:T(8,128)(2,1)S(1)} %copy-done.6), channel_id=1, source_target_pairs={{0,4},{4,8},{8,12},{12,0},{1,5},{5,9},{9,13},{13,1},{2,6},{6,10},{... | collective-permute-start | bytes 1572872 | tf_op jit(solution)/shard_map/ppermute | solution.py:47
  181.2 34.2 %collective-permute-done.12.refs_15_ = bf16[128,2048]{1,0:T(8,128)(2,1)S(1)} collective-permute-done((bf16[128,2048]{1,0:T(8,128)(2,1)S(1)}, bf16[128,2048]{1,0:T(8,128)(2,1)S(1)}, u32[]{:S(2)}, u32[]{:S(2)}) %collective-permute-start.12) | collective-permute-done | bytes 524320 | tf_op jit(solution)/shard_map/ppermute | solution.py:47
  215.4 0.8 copy-done.9
  216.2 1.0 copy-done.1
  217.3 11.7 %experts.1 = bf16[256,2048]{1,0:T(8,128)(2,1)} custom-call(bf16[256,2048]{1,0:T(8,128)(2,1)} %bitcast.34, bf16[256,2048]{1,0:T(8,128)(2,1)} %get-tuple-element.17.refs_0_, bf16[256,2048]{1,0:T(8,128)(2,1)} %get-tuple-element.18.refs_1_, bf16[256,2048]{1,0:T(8,128)(2,1)} %collective-permute-done.1.refs_2_, bf16[256,2048]{1,0:T(8,128)(2,1)} %collective-permute-done.2.refs_3_, ...), custom_call_target="tpu_custom_call" | custom-call | tf_op jit(solution)/shard_map/experts/pallas_call | solution.py:283
  229.0 18.7 %all_to_all.67.back_ref = bf16[16,16,2048]{2,1,0:T(8,128)(2,1)S(1)} all-to-all(bf16[16,16,2048]{2,1,0:T(8,128)(2,1)} %bitcast.35), channel_id=1, replica_groups=mesh['z'=16,'c'=2,'yh'=2,'yl'=2,'x'=4] {'yh','yl','x'}, dimensions={0} | all-to-all | bytes 2097152 | tf_op jit(solution)/shard_map/all_to_all | solution.py:39
  247.7 0.1 collect.1
  247.8 0.9 all_to_all.52
  248.7 16.0 %all-to-all-start.8 = ((bf16[32,2,2048]{2,1,0:T(2,128)(2,1)}), bf16[32,2,2048]{2,1,0:T(2,128)(2,1)S(1)}, u32[]{:S(2)}, u32[]{:S(2)}) async-start(bf16[32,2,2048]{2,1,0:T(2,128)(2,1)} %all_to_all.52), calls=%async_computation.8 | async-start | bytes 524288 | tf_op jit(solution)/shard_map/all_to_all | solution.py:39
  264.8 22.2 %all-to-all-done.8 = bf16[32,2,2048]{2,1,0:T(2,128)(2,1)S(1)} async-done(((bf16[32,2,2048]{2,1,0:T(2,128)(2,1)}), bf16[32,2,2048]{2,1,0:T(2,128)(2,1)S(1)}, u32[]{:S(2)}, u32[]{:S(2)}) %all-to-all-start.8) | async-done | bytes 262176 | tf_op jit(solution)/shard_map/all_to_all | solution.py:39
  287.0 0.1 all_to_all.54
  287.1 0.2 convolution_multiply_fusion.1
  287.3 0.9 fusion.2
  (46 shorter events, 0.1 us)
Async XLA Ops:
  0.0 95.9 %copy-start = (bf16[2048,128]{1,0:T(8,128)(2,1)S(1)}, bf16[2048,128]{1,0:T(8,128)(2,1)}, u32[]{:S(2)}) copy-start(bf16[2048,128]{1,0:T(8,128)(2,1)} %param.18) | copy-start | bytes 1572868
  3.8 13.5 %copy-start.10 = (bf16[16,32,256]{2,1,0:T(8,128)(2,1)S(1)}, bf16[16,32,256]{2,1,0:T(8,128)(2,1)}, u32[]{:S(2)}) copy-start(bf16[16,32,256]{2,1,0:T(8,128)(2,1)} %get-tuple-element.16) | copy-start | bytes 786436
  46.4 9.8 %collective-permute-start = (bf16[512,256]{1,0:T(8,128)(2,1)S(1)}, bf16[512,256]{1,0:T(8,128)(2,1)S(1)}, u32[]{:S(2)}, u32[]{:S(2)}) collective-permute-start(bf16[512,256]{1,0:T(8,128)(2,1)S(1)} %bitcast.32), channel_id=1, source_target_pairs={{0,16},{16,0},{1,17},{17,1},{2,18},{18,2},{3,19},{19,3},{4,20},{20... | collective-permute-start | bytes 786440 | tf_op jit(solution)/shard_map/ppermute | solution.py:43
  76.5 19.4 %all-to-all-start.3 = ((bf16[16,128,256]{2,1,0:T(8,128)(2,1)}), bf16[16,128,256]{2,1,0:T(8,128)(2,1)S(1)}, u32[]{:S(2)}, u32[]{:S(2)}) async-start(bf16[16,128,256]{2,1,0:T(8,128)(2,1)} %combine.1), calls=%async_computation.3 | async-start | bytes 2097152 | tf_op jit(solution)/shard_map/all_to_all | solution.py:39
  84.7 80.2 %collective-permute-start.1 = (bf16[256,2048]{1,0:T(8,128)(2,1)}, bf16[256,2048]{1,0:T(8,128)(2,1)}, u32[]{:S(2)}, u32[]{:S(2)}) collective-permute-start(bf16[256,2048]{1,0:T(8,128)(2,1)} %get-tuple-element.17.refs_0_), channel_id=1, source_target_pairs={{0,1},{1,2},{2,3},{3,0},{4,5},{5,6},{6,7},{7,4},{8,9},{9,10},{10,1... | collective-permute-start | bytes 3145736 | tf_op jit(solution)/shard_map/ppermute | solution.py:47
  87.9 6.2 %copy-start.13 = (s32[16,2]{0,1:T(2,128)S(1)}, s32[16,2]{0,1:T(2,128)}, u32[]{:S(2)}) copy-start(s32[16,2]{0,1:T(2,128)} %param.21) | copy-start | bytes 388
  87.9 79.1 %collective-permute-start.2 = (bf16[256,2048]{1,0:T(8,128)(2,1)}, bf16[256,2048]{1,0:T(8,128)(2,1)}, u32[]{:S(2)}, u32[]{:S(2)}) collective-permute-start(bf16[256,2048]{1,0:T(8,128)(2,1)} %get-tuple-element.18.refs_1_), channel_id=1, source_target_pairs={{0,4},{4,8},{8,12},{12,0},{1,5},{5,9},{9,13},{13,1},{2,6},{6,10},{... | collective-permute-start | bytes 3145736 | tf_op jit(solution)/shard_map/ppermute | solution.py:47
  91.0 55.8 %collective-permute-start.7 = (bf16[128,2048]{1,0:T(8,128)(2,1)}, bf16[128,2048]{1,0:T(8,128)(2,1)}, u32[]{:S(2)}, u32[]{:S(2)}) collective-permute-start(bf16[128,2048]{1,0:T(8,128)(2,1)} %get-tuple-element.19.refs_8_), channel_id=1, source_target_pairs={{0,1},{1,2},{2,3},{3,0},{4,5},{5,6},{6,7},{7,4},{8,9},{9,10},{10,1... | collective-permute-start | bytes 1572872 | tf_op jit(solution)/shard_map/ppermute | solution.py:47
  95.9 35.9 %copy-start.11 = (bf16[16,2048]{1,0:T(8,128)(2,1)S(1)}, bf16[16,2048]{1,0:T(8,128)(2,1)}, u32[]{:S(2)}) copy-start(bf16[16,2048]{1,0:T(8,128)(2,1)} %param.20) | copy-start | bytes 196612
  95.9 36.0 %copy-start.12 = (f32[2048]{0:T(1024)S(1)}, f32[2048]{0:T(1024)}, u32[]{:S(2)}) copy-start(f32[2048]{0:T(1024)} %param.19) | copy-start | bytes 24580
  95.9 44.5 %copy-start.4 = (bf16[128,2048]{1,0:T(8,128)(2,1)S(1)}, bf16[128,2048]{1,0:T(8,128)(2,1)}, u32[]{:S(2)}) copy-start(bf16[128,2048]{1,0:T(8,128)(2,1)} %get-tuple-element.20.refs_9_) | copy-start | bytes 1572868
  97.0 59.7 %copy-start.2 = (bf16[256,2048]{1,0:T(8,128)(2,1)S(1)}, bf16[256,2048]{1,0:T(8,128)(2,1)}, u32[]{:S(2)}) copy-start(bf16[256,2048]{1,0:T(8,128)(2,1)} %get-tuple-element.17.refs_0_) | copy-start | bytes 3145732
  97.0 34.7 %all-to-all-start.4 = ((bf16[16,16,128]{2,1,0:T(8,128)(2,1)}), bf16[16,16,128]{2,1,0:T(8,128)(2,1)S(1)}, u32[]{:S(2)}, u32[]{:S(2)}) async-start(bf16[16,16,128]{2,1,0:T(8,128)(2,1)} %bitcast.8), calls=%async_computation.4 | async-start | bytes 131072 | tf_op jit(solution)/shard_map/all_to_all | solution.py:345
  132.2 14.6 %copy-start.3 = (bf16[128,2048]{1,0:T(8,128)(2,1)S(1)}, bf16[128,2048]{1,0:T(8,128)(2,1)}, u32[]{:S(2)}) copy-start(bf16[128,2048]{1,0:T(8,128)(2,1)} %get-tuple-element.19.refs_8_) | copy-start | bytes 1572868
  133.1 36.2 %all-to-all-start.5 = ((bf16[32,2,2048]{2,1,0:T(2,128)(2,1)}), bf16[32,2,2048]{2,1,0:T(2,128)(2,1)S(1)}, u32[]{:S(2)}, u32[]{:S(2)}) async-start(bf16[32,2,2048]{2,1,0:T(2,128)(2,1)} %all_to_all.48), calls=%async_computation.5 | async-start | bytes 524288 | tf_op jit(solution)/shard_map/all_to_all | solution.py:39
  140.3 16.4 %collective-permute-start.8 = (bf16[128,2048]{1,0:T(8,128)(2,1)S(1)}, bf16[128,2048]{1,0:T(8,128)(2,1)S(1)}, u32[]{:S(2)}, u32[]{:S(2)}) collective-permute-start(bf16[128,2048]{1,0:T(8,128)(2,1)S(1)} %copy-done.4), channel_id=1, source_target_pairs={{0,4},{4,8},{8,12},{12,0},{1,5},{5,9},{9,13},{13,1},{2,6},{6,10},{... | collective-permute-start | bytes 1572872 | tf_op jit(solution)/shard_map/ppermute | solution.py:47
  142.5 16.6 %collective-permute-start.10 = (bf16[128,2048]{1,0:T(8,128)(2,1)S(1)}, bf16[128,2048]{1,0:T(8,128)(2,1)S(1)}, u32[]{:S(2)}, u32[]{:S(2)}) collective-permute-start(bf16[128,2048]{1,0:T(8,128)(2,1)S(1)} %copy-done.4), channel_id=1, source_target_pairs={{0,12},{4,0},{8,4},{12,8},{1,13},{5,1},{9,5},{13,9},{2,14},{6,2},{... | collective-permute-start | bytes 1572872 | tf_op jit(solution)/shard_map/ppermute | solution.py:47
  146.9 15.1 %collective-permute-start.9 = (bf16[128,2048]{1,0:T(8,128)(2,1)S(1)}, bf16[128,2048]{1,0:T(8,128)(2,1)S(1)}, u32[]{:S(2)}, u32[]{:S(2)}) collective-permute-start(bf16[128,2048]{1,0:T(8,128)(2,1)S(1)} %copy-done.3), channel_id=1, source_target_pairs={{0,3},{1,0},{2,1},{3,2},{4,7},{5,4},{6,5},{7,6},{8,11},{9,8},{10,9... | collective-permute-start | bytes 1572872 | tf_op jit(solution)/shard_map/ppermute | solution.py:47
  156.7 10.4 %copy-start.5 = (bf16[128,2048]{1,0:T(8,128)(2,1)}, bf16[128,2048]{1,0:T(8,128)(2,1)S(1)}, u32[]{:S(2)}) copy-start(bf16[128,2048]{1,0:T(8,128)(2,1)S(1)} %collective-permute-done.8.refs_11_) | copy-start | bytes 1572868
  156.7 58.7 %collective-permute-start.3 = (bf16[256,2048]{1,0:T(8,128)(2,1)S(1)}, bf16[256,2048]{1,0:T(8,128)(2,1)}, u32[]{:S(2)}, u32[]{:S(2)}) collective-permute-start(bf16[256,2048]{1,0:T(8,128)(2,1)S(1)} %copy-done.2), channel_id=1, source_target_pairs={{0,3},{1,0},{2,1},{3,2},{4,7},{5,4},{6,5},{7,6},{8,11},{9,8},{10,9... | collective-permute-start | bytes 3145736 | tf_op jit(solution)/shard_map/ppermute | solution.py:47
  159.1 8.0 %copy-start.7 = (bf16[128,2048]{1,0:T(8,128)(2,1)}, bf16[128,2048]{1,0:T(8,128)(2,1)S(1)}, u32[]{:S(2)}) copy-start(bf16[128,2048]{1,0:T(8,128)(2,1)S(1)} %collective-permute-done.10.refs_13_) | copy-start | bytes 1572868
  159.1 18.7 %collective-permute-start.11 = (bf16[128,2048]{1,0:T(8,128)(2,1)}, bf16[128,2048]{1,0:T(8,128)(2,1)}, u32[]{:S(2)}, u32[]{:S(2)}) collective-permute-start(bf16[128,2048]{1,0:T(8,128)(2,1)} %collective-permute-done.7.refs_10_), channel_id=1, source_target_pairs={{0,1},{1,2},{2,3},{3,0},{4,5},{5,6},{6,7},{7,4},{8,9},{9,10},{10,1... | collective-permute-start | bytes 1572872 | tf_op jit(solution)/shard_map/ppermute | solution.py:47
  162.0 5.1 %copy-start.8 = (bf16[128,2048]{1,0:T(8,128)(2,1)}, bf16[128,2048]{1,0:T(8,128)(2,1)S(1)}, u32[]{:S(2)}) copy-start(bf16[128,2048]{1,0:T(8,128)(2,1)S(1)} %collective-permute-done.9.refs_12_) | copy-start | bytes 1572868
  162.0 53.4 %collective-permute-start.4 = (bf16[256,2048]{1,0:T(8,128)(2,1)}, bf16[256,2048]{1,0:T(8,128)(2,1)}, u32[]{:S(2)}, u32[]{:S(2)}) collective-permute-start(bf16[256,2048]{1,0:T(8,128)(2,1)} %get-tuple-element.18.refs_1_), channel_id=1, source_target_pairs={{0,12},{4,0},{8,4},{12,8},{1,13},{5,1},{9,5},{13,9},{2,14},{6,2},{... | collective-permute-start | bytes 3145736 | tf_op jit(solution)/shard_map/ppermute | solution.py:47
  164.9 50.5 %collective-permute-start.5 = (bf16[256,2048]{1,0:T(8,128)(2,1)}, bf16[256,2048]{1,0:T(8,128)(2,1)}, u32[]{:S(2)}, u32[]{:S(2)}) collective-permute-start(bf16[256,2048]{1,0:T(8,128)(2,1)} %collective-permute-done.1.refs_2_), channel_id=1, source_target_pairs={{0,1},{1,2},{2,3},{3,0},{4,5},{5,6},{6,7},{7,4},{8,9},{9,10},{10,1... | collective-permute-start | bytes 3145736 | tf_op jit(solution)/shard_map/ppermute | solution.py:47
  167.1 49.1 %collective-permute-start.6 = (bf16[256,2048]{1,0:T(8,128)(2,1)}, bf16[256,2048]{1,0:T(8,128)(2,1)}, u32[]{:S(2)}, u32[]{:S(2)}) collective-permute-start(bf16[256,2048]{1,0:T(8,128)(2,1)} %collective-permute-done.2.refs_3_), channel_id=1, source_target_pairs={{0,4},{4,8},{8,12},{12,0},{1,5},{5,9},{9,13},{13,1},{2,6},{6,10},{... | collective-permute-start | bytes 3145736 | tf_op jit(solution)/shard_map/ppermute | solution.py:47
  170.5 7.2 %copy-start.6 = (bf16[128,2048]{1,0:T(8,128)(2,1)S(1)}, bf16[128,2048]{1,0:T(8,128)(2,1)}, u32[]{:S(2)}) copy-start(bf16[128,2048]{1,0:T(8,128)(2,1)} %copy-done.5) | copy-start | bytes 1572868
  170.5 45.7 %all-to-all-start.6 = ((bf16[16,16,2048]{2,1,0:T(8,128)(2,1)}), bf16[16,16,2048]{2,1,0:T(8,128)(2,1)S(1)}, u32[]{:S(2)}, u32[]{:S(2)}) async-start(bf16[16,16,2048]{2,1,0:T(8,128)(2,1)} %deal.1), calls=%async_computation.6 | async-start | bytes 2097152 | tf_op jit(solution)/shard_map/all_to_all | solution.py:39
  177.8 37.6 %collective-permute-start.12 = (bf16[128,2048]{1,0:T(8,128)(2,1)S(1)}, bf16[128,2048]{1,0:T(8,128)(2,1)S(1)}, u32[]{:S(2)}, u32[]{:S(2)}) collective-permute-start(bf16[128,2048]{1,0:T(8,128)(2,1)S(1)} %copy-done.6), channel_id=1, source_target_pairs={{0,4},{4,8},{8,12},{12,0},{1,5},{5,9},{9,13},{13,1},{2,6},{6,10},{... | collective-permute-start | bytes 1572872 | tf_op jit(solution)/shard_map/ppermute | solution.py:47
  215.4 0.8 copy-start.9
  216.2 1.0 copy-start.1
  248.7 16.0 %copy-start.14 = (f32[16,2]{0,1:T(2,128)S(1)}, f32[16,2]{0,1:T(2,128)}, u32[]{:S(2)}) copy-start(f32[16,2]{0,1:T(2,128)} %param.22) | copy-start | bytes 388
  248.7 38.3 %all-to-all-start.8 = ((bf16[32,2,2048]{2,1,0:T(2,128)(2,1)}), bf16[32,2,2048]{2,1,0:T(2,128)(2,1)S(1)}, u32[]{:S(2)}, u32[]{:S(2)}) async-start(bf16[32,2,2048]{2,1,0:T(2,128)(2,1)} %all_to_all.52), calls=%async_computation.8 | async-start | bytes 524288 | tf_op jit(solution)/shard_map/all_to_all | solution.py:39

commit v4 on v2

--- a/solution.py
+++ b/solution.py
@@ -22,6 +22,7 @@
 TP = ("yh", "yl", "x")
 GROUP = ("yl", "x")
 STAT_ROWS = 16
+EXPERT_GRANT = 46
 SHARE = 128
 NSHARE = 4
 COLOURS = tuple((i % NX + i // NX) % NSHARE for i in range(NT))
@@ -102,7 +103,7 @@
     return hi, mid, lo
 
 
-def attend_kernel(q_ref, own_ref, other_ref, out_ref):
+def attend_kernel(q_ref, own_ref, other_ref, out_ref, scores_ref):
     heads, rows, width = q_ref.shape
     factor = width ** (-0.5) * LOG2E
     keys = jnp.concatenate([own_ref[:, :width], other_ref[:, :width]], axis=0)
@@ -111,10 +112,17 @@
         [values.T, jnp.ones((STAT_ROWS, values.shape[0]), BF)], axis=0
     )
     row = lax.broadcasted_iota(jnp.int32, (STAT_ROWS, rows), 0)
-    for head in range(heads):
-        scores = lax.dot_general(
+
+    def score(head):
+        scores_ref[head % 2] = lax.dot_general(
             keys, q_ref[head], (((1,), (1,)), ((), ())), preferred_element_type=F32
         )
+
+    score(0)
+    for head in range(heads):
+        if head + 1 < heads:
+            score(head + 1)
+        scores = scores_ref[head % 2]
         top = jnp.max(scores, axis=0, keepdims=True)
         weights = jnp.exp2((scores - top) * factor).astype(BF)
         summed = jnp.dot(values, weights, preferred_element_type=F32)
@@ -133,6 +141,7 @@
         in_specs=[IN_VMEM] * 3,
         out_specs=IN_VMEM,
         out_shape=jax.ShapeDtypeStruct((heads, width + STAT_ROWS, rows), BF),
+        scratch_shapes=[pltpu.VMEM((2, NC * own.shape[0], rows), F32)],
         compiler_params=grant(24),
         name="attend",
     )(q8, own, other)
@@ -209,40 +218,45 @@
 
 
 def pack_kernel(gate_ref, up_ref, down_ref, *out_refs):
-    packed = jnp.concatenate([gate_ref[0].T, up_ref[0].T, down_ref[0]], axis=0)
-    for half, out_ref in enumerate(out_refs):
+    gate_up = jnp.concatenate([gate_ref[0].T, up_ref[0].T], axis=0)
+    for half in range(2):
         @pl.when(pl.program_id(0) == half)
         def _():
-            out_ref[...] = packed
+            out_refs[half][...] = gate_up
+            out_refs[2 + half][...] = down_ref[0]
 
 
 def pack(w_gate, w_up, w_down):
     _, depth, units = w_gate.shape
     wide = pl.BlockSpec((1, depth, SHARE), lambda i: (0, 0, i))
-    shape = (3 * SHARE, depth)
-    return pl.pallas_call(
+    shapes = [(2 * SHARE, depth)] * 2 + [(SHARE, depth)] * 2
+    outs = pl.pallas_call(
         pack_kernel,
         grid=(units // SHARE,),
         in_specs=[wide, wide, pl.BlockSpec((1, SHARE, depth), lambda i: (0, i, 0))],
-        out_specs=[pl.BlockSpec(shape, lambda i: (0, 0))] * 2,
-        out_shape=[jax.ShapeDtypeStruct(shape, BF)] * 2,
+        out_specs=[pl.BlockSpec(shape, lambda i: (0, 0)) for shape in shapes],
+        out_shape=[jax.ShapeDtypeStruct(shape, BF) for shape in shapes],
         name="pack",
     )(w_gate, w_up, w_down)
+    return outs[:2], outs[2:]
 
 
 def experts_kernel(rows_ref, *refs):
     pieces, (out_ref, held, acc, sems) = refs[:-4], refs[-4:]
-    pairs = len(pieces) // 2
-    copies = [
-        pltpu.make_async_copy(
-            pieces[2 * p + i].at[pl.ds(j * SHARE, SHARE)],
-            held.at[p, j, pl.ds(i * SHARE, SHARE)],
-            sems.at[p, j, i],
-        )
-        for p in range(pairs)
-        for j in range(3)
-        for i in range(2)
-    ]
+    pairs = len(pieces) // 4
+    ups, downs = pieces[: 2 * pairs], pieces[2 * pairs :]
+    copies = []
+    for p in range(pairs):
+        for j in range(3):
+            for i in range(2):
+                source = downs[2 * p + i]
+                if j < 2:
+                    source = ups[2 * p + i].at[pl.ds(j * SHARE, SHARE)]
+                copies.append(
+                    pltpu.make_async_copy(
+                        source, held.at[p, j, pl.ds(i * SHARE, SHARE)], sems.at[p, j, i]
+                    )
+                )
     for copy in copies[:12]:
         copy.start()
     across = (((1,), (1,)), ((), ()))
@@ -272,18 +286,18 @@
 
 
 def experts(rows, pieces):
-    depth = rows.shape[1]
+    pairs, depth = len(pieces) // 4, rows.shape[1]
     return pl.pallas_call(
         experts_kernel,
         in_specs=[IN_VMEM] + [IN_HBM] * len(pieces),
         out_specs=IN_VMEM,
         out_shape=jax.ShapeDtypeStruct(rows.shape, BF),
         scratch_shapes=[
-            pltpu.VMEM((len(pieces) // 2, 3, 2 * SHARE, depth), BF),
+            pltpu.VMEM((pairs, 3, 2 * SHARE, depth), BF),
             pltpu.VMEM(rows.shape, F32),
-            pltpu.SemaphoreType.DMA((len(pieces) // 2, 3, 2)),
+            pltpu.SemaphoreType.DMA((pairs, 3, 2)),
         ],
-        compiler_params=grant(32),
+        compiler_params=grant(EXPERT_GRANT),
         name="experts",
     )(rows, *pieces)
 
@@ -319,12 +333,14 @@
     kv_mine = exchange(kv, "z").reshape(-1, 2 * width)
     kv_other = swap_cores(kv_mine)
 
-    packs = pack(w_gate, w_up, w_down)
+    ups, downs = pack(w_gate, w_up, w_down)
     axes = ("x", ("yh", "yl"))
-    left = [ring(p, axis, 1) for p, axis in zip(packs, axes)]
-    right = [ring(p, axis, -1) for p, axis in zip(packs, axes)]
-    far = [ring(p, axis, 1) for p, axis in zip(left, axes)]
-    pieces = [*packs, *left, *right, *far]
+    pieces = []
+    for packs in (ups, downs):
+        left = [ring(p, axis, 1) for p, axis in zip(packs, axes)]
+        right = [ring(p, axis, -1) for p, axis in zip(packs, axes)]
+        last = [ring(p, axis, 1) for p, axis in zip(left, axes)]
+        pieces += [*packs, *left, *right, *last]
 
     parts = attend(q8, kv_mine, kv_other)
     parts = exchange(parts, GROUP)

time: 266 us -> 289 us (1.086)
  starting transfers between devices: 60.4 us -> 82.5 us
  local copies, waits for them, and re-layouts: 3.4 us -> 9.57 us
    all_to_all x4, waiting for transfers between devices: 42.4 us -> 23.8 us  [exchange(): return lax.all_to_all(blocks, axis, split_axis=0, concat_axis=0, tiled=True)]
    ppermute x6 -> x12, starting transfers between devices: 17.1 us -> 34.2 us  [ring(): return lax.ppermute(value, axis, [(i, (i + step) % 4) for i in range(4)])]
    ppermute x6 -> x12, waiting for transfers between devices: 25.6 us -> 41.7 us  [ring(): return lax.ppermute(value, axis, [(i, (i + step) % 4) for i in range(4)])]
    unnamed x14 -> x36, local copies, waits for them, and re-layouts: 1.43 us -> 7.61 us
    all_to_all x4, starting transfers between devices: 29.7 us -> 34.5 us  [exchange(): return lax.all_to_all(blocks, axis, split_axis=0, concat_axis=0, tiled=True)]
  transfers between devices with their start and end apart: 12 -> 18, of which waited for: 10 -> 6; matrix products, arithmetic and copies ran while one was open for 1% -> 1% of each run, Pallas kernels for 2% -> 2%
where the time goes in v4:
time: 289 us; the launch traced here: 288 us
  waiting for transfers between devices  96.2 us (33%)
  starting transfers between devices  82.5 us (29%)
  blocking collectives  74.3 us (26%)
  Pallas kernels  21.6 us (7%)
  local copies, waits for them, and re-layouts  9.57 us (3%)
    all_to_all x4, blocking collectives, exchange(): return lax.all_to_all(blocks, axis, split_axis=0, concat_axis=0, tiled=True)  74.3 us
    ppermute x12, waiting for transfers between devices, ring(): return lax.ppermute(value, axis, [(i, (i + step) % 4) for i in range(4)])  41.7 us
    all_to_all x4, starting transfers between devices, exchange(): return lax.all_to_all(blocks, axis, split_axis=0, concat_axis=0, tiled=True)  34.5 us
    ppermute x12, starting transfers between devices, ring(): return lax.ppermute(value, axis, [(i, (i + step) % 4) for i in range(4)])  34.2 us
    all_to_all x1, waiting for transfers between devices, local(): lax.all_to_all(columns, TP, split_axis=0, concat_axis=1, tiled=True)  29.6 us
    all_to_all x4, waiting for transfers between devices, exchange(): return lax.all_to_all(blocks, axis, split_axis=0, concat_axis=0, tiled=True)  23.8 us
    pallas_call x1, Pallas kernels, experts(): pl.pallas_call(experts_kernel, in_specs=[IN_VMEM] + [IN_HBM] * len(pieces...  8.83 us
    ppermute x1, starting transfers between devices, swap_cores(): return lax.ppermute(value, 'c', [(0, 1), (1, 0)])  8.66 us
  transfers between devices with their start and end apart: 18, of which 6 were waited for; matrix products, arithmetic and copies ran while one was open for 1% of the time, Pallas kernels for 2%

profile of v4, /device:TPU:1, one launch (start us, length us, event | category | flops | bytes accessed | tf_op | source)
XLA Modules:
  0.0 288.1 jit_solution(9768760942493475184)
XLA Ops:
  0.0 0.7 pad_add_fusion.at_ref
  0.7 3.1 %prepare.1 = (bf16[8,256,128]{2,1,0:T(8,128)(2,1)}, bf16[16,32,256]{2,1,0:T(8,128)(2,1)}) custom-call(s32[4]{0:T(128)} %pad_add_fusion.at_ref, bf16[256,128]{1,0:T(8,128)(2,1)} %q_ref.1, bf16[256,256]{1,0:T(8,128)(2,1)} %k_ref.1, bf16[256,256]{1,0:T(8,128)(2,1)} %v_ref.1, f32[1,128]{1,0:T(1,128)} %bitcast.37, f32[1,128]{1,0:T(1,128)} %bitcast.38), custom_call_target="tpu_custom_call" | custom-call | tf_op jit(solution)/shard_map/prepare/pallas_call | solution.py:85
  3.7 13.5 %all_to_all.64.q_ref = bf16[8,256,128]{2,1,0:T(8,128)(2,1)S(1)} all-to-all(bf16[8,256,128]{2,1,0:T(8,128)(2,1)} %get-tuple-element.13), channel_id=1, replica_groups=mesh['z'=16,'c'=2,'yh'=2,'yl'=2,'x'=4] {'yl','x'}, dimensions={0} | all-to-all | bytes 1048576 | tf_op jit(solution)/shard_map/all_to_all | solution.py:40
  17.3 29.1 %all_to_all.65 = bf16[16,32,256]{2,1,0:T(8,128)(2,1)S(1)} all-to-all(bf16[16,32,256]{2,1,0:T(8,128)(2,1)S(1)} %copy-done.13), channel_id=1, replica_groups=mesh['z'=16,'c'=2,'yh'=2,'yl'=2,'x'=4] {'z'}, dimensions={0} | all-to-all | bytes 524288 | tf_op jit(solution)/shard_map/all_to_all | solution.py:40
  46.4 8.7 %collective-permute-start = (bf16[512,256]{1,0:T(8,128)(2,1)S(1)}, bf16[512,256]{1,0:T(8,128)(2,1)S(1)}, u32[]{:S(2)}, u32[]{:S(2)}) collective-permute-start(bf16[512,256]{1,0:T(8,128)(2,1)S(1)} %bitcast.34), channel_id=1, source_target_pairs={{0,16},{16,0},{1,17},{17,1},{2,18},{18,2},{3,19},{19,3},{4,20},{20... | collective-permute-start | bytes 786440 | tf_op jit(solution)/shard_map/ppermute | solution.py:44
  55.0 1.1 collective-permute-done.other_ref
  56.2 3.3 %attend.1 = bf16[8,144,256]{2,1,0:T(8,128)(2,1)S(1)} custom-call(bf16[8,256,128]{2,1,0:T(8,128)(2,1)S(1)} %all_to_all.64.q_ref, bf16[512,256]{1,0:T(8,128)(2,1)S(1)} %bitcast.35, bf16[512,256]{1,0:T(8,128)(2,1)S(1)} %collective-permute-done.other_ref), custom_call_target="tpu_custom_call" | custom-call | tf_op jit(solution)/shard_map/attend/pallas_call | solution.py:139
  59.5 13.2 %all_to_all.66.parts_ref = bf16[8,144,256]{2,1,0:T(8,128)(2,1)S(1)} all-to-all(bf16[8,144,256]{2,1,0:T(8,128)(2,1)S(1)} %attend.1), channel_id=1, replica_groups=mesh['z'=16,'c'=2,'yh'=2,'yl'=2,'x'=4] {'yl','x'}, dimensions={0} | all-to-all | bytes 1179648 | tf_op jit(solution)/shard_map/all_to_all | solution.py:40
  72.7 1.2 combine.1
  73.8 4.2 %all-to-all-start.3 = ((bf16[16,128,256]{2,1,0:T(8,128)(2,1)}), bf16[16,128,256]{2,1,0:T(8,128)(2,1)S(1)}, u32[]{:S(2)}, u32[]{:S(2)}) async-start(bf16[16,128,256]{2,1,0:T(8,128)(2,1)} %combine.1), calls=%async_computation.3 | async-start | bytes 2097152 | tf_op jit(solution)/shard_map/all_to_all | solution.py:40
  78.0 3.9 %pack.1 = (bf16[256,2048]{1,0:T(8,128)(2,1)}, bf16[256,2048]{1,0:T(8,128)(2,1)}, bf16[128,2048]{1,0:T(8,128)(2,1)}, bf16[128,2048]{1,0:T(8,128)(2,1)}) custom-call(bf16[1,2048,256]{2,1,0:T(8,128)(2,1)} %gate_ref.1, bf16[1,2048,256]{2,1,0:T(8,128)(2,1)} %up_ref.1, bf16[1,256,2048]{2,1,0:T(8,128)(2,1)} %down_ref.1), custom_call_target="tpu_custom_call" | custom-call | tf_op jit(solution)/shard_map/pack/pallas_call | solution.py:233
  82.0 3.3 %collective-permute-start.1 = (bf16[256,2048]{1,0:T(8,128)(2,1)}, bf16[256,2048]{1,0:T(8,128)(2,1)}, u32[]{:S(2)}, u32[]{:S(2)}) collective-permute-start(bf16[256,2048]{1,0:T(8,128)(2,1)} %get-tuple-element.17.refs_0_), channel_id=1, source_target_pairs={{0,1},{1,2},{2,3},{3,0},{4,5},{5,6},{6,7},{7,4},{8,9},{9,10},{10,1... | collective-permute-start | bytes 3145736 | tf_op jit(solution)/shard_map/ppermute | solution.py:48
  85.2 3.1 %collective-permute-start.2 = (bf16[256,2048]{1,0:T(8,128)(2,1)}, bf16[256,2048]{1,0:T(8,128)(2,1)}, u32[]{:S(2)}, u32[]{:S(2)}) collective-permute-start(bf16[256,2048]{1,0:T(8,128)(2,1)} %get-tuple-element.18.refs_1_), channel_id=1, source_target_pairs={{0,4},{4,8},{8,12},{12,0},{1,5},{5,9},{9,13},{13,1},{2,6},{6,10},{... | collective-permute-start | bytes 3145736 | tf_op jit(solution)/shard_map/ppermute | solution.py:48
  88.3 3.1 %collective-permute-start.7 = (bf16[128,2048]{1,0:T(8,128)(2,1)}, bf16[128,2048]{1,0:T(8,128)(2,1)}, u32[]{:S(2)}, u32[]{:S(2)}) collective-permute-start(bf16[128,2048]{1,0:T(8,128)(2,1)} %get-tuple-element.19.refs_8_), channel_id=1, source_target_pairs={{0,1},{1,2},{2,3},{3,0},{4,5},{5,6},{6,7},{7,4},{8,9},{9,10},{10,1... | collective-permute-start | bytes 1572872 | tf_op jit(solution)/shard_map/ppermute | solution.py:48
  91.7 1.5 all-to-all-done.3
  93.2 1.1 convolution_convert_fusion.1
  94.3 5.1 %all-to-all-start.4 = ((bf16[16,16,128]{2,1,0:T(8,128)(2,1)}), bf16[16,16,128]{2,1,0:T(8,128)(2,1)S(1)}, u32[]{:S(2)}, u32[]{:S(2)}) async-start(bf16[16,16,128]{2,1,0:T(8,128)(2,1)} %bitcast.8), calls=%async_computation.4 | async-start | bytes 131072 | tf_op jit(solution)/shard_map/all_to_all | solution.py:351
  99.5 29.6 %all-to-all-done.4 = bf16[16,16,128]{2,1,0:T(8,128)(2,1)S(1)} async-done(((bf16[16,16,128]{2,1,0:T(8,128)(2,1)}), bf16[16,16,128]{2,1,0:T(8,128)(2,1)S(1)}, u32[]{:S(2)}, u32[]{:S(2)}) %all-to-all-start.4) | async-done | bytes 65568 | tf_op jit(solution)/shard_map/all_to_all | solution.py:351
  129.2 0.3 convolution_convert_fusion
  129.6 0.9 all_to_all.48
  130.5 7.2 %all-to-all-start.5 = ((bf16[32,2,2048]{2,1,0:T(2,128)(2,1)}), bf16[32,2,2048]{2,1,0:T(2,128)(2,1)S(1)}, u32[]{:S(2)}, u32[]{:S(2)}) async-start(bf16[32,2,2048]{2,1,0:T(2,128)(2,1)} %all_to_all.48), calls=%async_computation.5 | async-start | bytes 524288 | tf_op jit(solution)/shard_map/all_to_all | solution.py:40
  137.7 2.1 collective-permute-start.8
  139.8 4.3 %collective-permute-start.10 = (bf16[128,2048]{1,0:T(8,128)(2,1)S(1)}, bf16[128,2048]{1,0:T(8,128)(2,1)S(1)}, u32[]{:S(2)}, u32[]{:S(2)}) collective-permute-start(bf16[128,2048]{1,0:T(8,128)(2,1)S(1)} %copy-done.3), channel_id=1, source_target_pairs={{0,12},{4,0},{8,4},{12,8},{1,13},{5,1},{9,5},{13,9},{2,14},{6,2},{... | collective-permute-start | bytes 1572872 | tf_op jit(solution)/shard_map/ppermute | solution.py:48
  144.2 2.4 collective-permute-start.9
  146.6 7.4 %collective-permute-done.8.refs_11_ = bf16[128,2048]{1,0:T(8,128)(2,1)S(1)} collective-permute-done((bf16[128,2048]{1,0:T(8,128)(2,1)S(1)}, bf16[128,2048]{1,0:T(8,128)(2,1)S(1)}, u32[]{:S(2)}, u32[]{:S(2)}) %collective-permute-start.8) | collective-permute-done | bytes 524320 | tf_op jit(solution)/shard_map/ppermute | solution.py:48
  154.0 2.4 collective-permute-start.3
  156.4 0.8 copy-done.7
  157.2 2.9 %collective-permute-start.11 = (bf16[128,2048]{1,0:T(8,128)(2,1)}, bf16[128,2048]{1,0:T(8,128)(2,1)}, u32[]{:S(2)}, u32[]{:S(2)}) collective-permute-start(bf16[128,2048]{1,0:T(8,128)(2,1)} %collective-permute-done.7.refs_10_), channel_id=1, source_target_pairs={{0,1},{1,2},{2,3},{3,0},{4,5},{5,6},{6,7},{7,4},{8,9},{9,10},{10,1... | collective-permute-start | bytes 1572872 | tf_op jit(solution)/shard_map/ppermute | solution.py:48
  160.1 0.8 copy-done.9
  160.9 2.8 collective-permute-start.4
  163.8 2.2 collective-permute-start.5
  165.9 2.2 collective-permute-start.6
  168.3 1.2 deal.1
  169.4 7.1 %all-to-all-start.6 = ((bf16[16,16,2048]{2,1,0:T(8,128)(2,1)}), bf16[16,16,2048]{2,1,0:T(8,128)(2,1)S(1)}, u32[]{:S(2)}, u32[]{:S(2)}) async-start(bf16[16,16,2048]{2,1,0:T(8,128)(2,1)} %deal.1), calls=%async_computation.6 | async-start | bytes 2097152 | tf_op jit(solution)/shard_map/all_to_all | solution.py:40
  176.5 3.5 %collective-permute-start.12 = (bf16[128,2048]{1,0:T(8,128)(2,1)}, bf16[128,2048]{1,0:T(8,128)(2,1)S(1)}, u32[]{:S(2)}, u32[]{:S(2)}) collective-permute-start(bf16[128,2048]{1,0:T(8,128)(2,1)} %copy-done.5), channel_id=1, source_target_pairs={{0,4},{4,8},{8,12},{12,0},{1,5},{5,9},{9,13},{13,1},{2,6},{6,10},{... | collective-permute-start | bytes 1572872 | tf_op jit(solution)/shard_map/ppermute | solution.py:48
  180.0 34.3 %collective-permute-done.12.refs_15_ = bf16[128,2048]{1,0:T(8,128)(2,1)S(1)} collective-permute-done((bf16[128,2048]{1,0:T(8,128)(2,1)}, bf16[128,2048]{1,0:T(8,128)(2,1)S(1)}, u32[]{:S(2)}, u32[]{:S(2)}) %collective-permute-start.12) | collective-permute-done | bytes 524320 | tf_op jit(solution)/shard_map/ppermute | solution.py:48
  214.2 0.8 copy-done.11
  215.1 1.0 copy-done.4
  216.1 1.0 copy-done.6
  217.2 1.0 copy-done.8
  218.2 1.0 copy-done.10
  219.2 1.0 copy-done.12
  220.3 8.8 %experts.1 = bf16[256,2048]{1,0:T(8,128)(2,1)S(1)} custom-call(bf16[256,2048]{1,0:T(8,128)(2,1)S(1)} %bitcast.32, bf16[256,2048]{1,0:T(8,128)(2,1)S(1)} %copy-done.1, bf16[256,2048]{1,0:T(8,128)(2,1)} %get-tuple-element.18.refs_1_, bf16[256,2048]{1,0:T(8,128)(2,1)} %collective-permute-done.1.refs_2_, bf16[256,2048]{1,0:T(8,128)(2,1)} %collective-permute-done.2.refs_3_, ...), custom_call_target="tpu_custom_call" | custom-call | tf_op jit(solution)/shard_map/experts/pallas_call | solution.py:290
  229.1 18.5 %all_to_all.67.back_ref = bf16[16,16,2048]{2,1,0:T(8,128)(2,1)S(1)} all-to-all(bf16[16,16,2048]{2,1,0:T(8,128)(2,1)S(1)} %bitcast.33), channel_id=1, replica_groups=mesh['z'=16,'c'=2,'yh'=2,'yl'=2,'x'=4] {'yh','yl','x'}, dimensions={0} | all-to-all | bytes 2097152 | tf_op jit(solution)/shard_map/all_to_all | solution.py:40
  247.8 0.9 all_to_all.52
  248.6 16.0 %all-to-all-start.8 = ((bf16[32,2,2048]{2,1,0:T(2,128)(2,1)}), bf16[32,2,2048]{2,1,0:T(2,128)(2,1)S(1)}, u32[]{:S(2)}, u32[]{:S(2)}) async-start(bf16[32,2,2048]{2,1,0:T(2,128)(2,1)} %all_to_all.52), calls=%async_computation.8 | async-start | bytes 524288 | tf_op jit(solution)/shard_map/all_to_all | solution.py:40
  264.7 22.2 %all-to-all-done.8 = bf16[32,2,2048]{2,1,0:T(2,128)(2,1)S(1)} async-done(((bf16[32,2,2048]{2,1,0:T(2,128)(2,1)}), bf16[32,2,2048]{2,1,0:T(2,128)(2,1)S(1)}, u32[]{:S(2)}, u32[]{:S(2)}) %all-to-all-start.8) | async-done | bytes 262176 | tf_op jit(solution)/shard_map/all_to_all | solution.py:40
  287.2 0.9 fusion.2
  (52 shorter events, 1.0 us)
Async XLA Ops:
  0.0 93.2 %copy-start = (bf16[2048,128]{1,0:T(8,128)(2,1)S(1)}, bf16[2048,128]{1,0:T(8,128)(2,1)}, u32[]{:S(2)}) copy-start(bf16[2048,128]{1,0:T(8,128)(2,1)} %param.18) | copy-start | bytes 1572868
  3.7 13.5 %copy-start.13 = (bf16[16,32,256]{2,1,0:T(8,128)(2,1)S(1)}, bf16[16,32,256]{2,1,0:T(8,128)(2,1)}, u32[]{:S(2)}) copy-start(bf16[16,32,256]{2,1,0:T(8,128)(2,1)} %get-tuple-element.16) | copy-start | bytes 786436
  46.4 9.8 %collective-permute-start = (bf16[512,256]{1,0:T(8,128)(2,1)S(1)}, bf16[512,256]{1,0:T(8,128)(2,1)S(1)}, u32[]{:S(2)}, u32[]{:S(2)}) collective-permute-start(bf16[512,256]{1,0:T(8,128)(2,1)S(1)} %bitcast.34), channel_id=1, source_target_pairs={{0,16},{16,0},{1,17},{17,1},{2,18},{18,2},{3,19},{19,3},{4,20},{20... | collective-permute-start | bytes 786440 | tf_op jit(solution)/shard_map/ppermute | solution.py:44
  73.8 19.4 %all-to-all-start.3 = ((bf16[16,128,256]{2,1,0:T(8,128)(2,1)}), bf16[16,128,256]{2,1,0:T(8,128)(2,1)S(1)}, u32[]{:S(2)}, u32[]{:S(2)}) async-start(bf16[16,128,256]{2,1,0:T(8,128)(2,1)} %combine.1), calls=%async_computation.3 | async-start | bytes 2097152 | tf_op jit(solution)/shard_map/all_to_all | solution.py:40
  82.0 81.8 %collective-permute-start.1 = (bf16[256,2048]{1,0:T(8,128)(2,1)}, bf16[256,2048]{1,0:T(8,128)(2,1)}, u32[]{:S(2)}, u32[]{:S(2)}) collective-permute-start(bf16[256,2048]{1,0:T(8,128)(2,1)} %get-tuple-element.17.refs_0_), channel_id=1, source_target_pairs={{0,1},{1,2},{2,3},{3,0},{4,5},{5,6},{6,7},{7,4},{8,9},{9,10},{10,1... | collective-permute-start | bytes 3145736 | tf_op jit(solution)/shard_map/ppermute | solution.py:48
  85.2 6.2 %copy-start.16 = (s32[16,2]{0,1:T(2,128)S(1)}, s32[16,2]{0,1:T(2,128)}, u32[]{:S(2)}) copy-start(s32[16,2]{0,1:T(2,128)} %param.21) | copy-start | bytes 388
  85.2 80.7 %collective-permute-start.2 = (bf16[256,2048]{1,0:T(8,128)(2,1)}, bf16[256,2048]{1,0:T(8,128)(2,1)}, u32[]{:S(2)}, u32[]{:S(2)}) collective-permute-start(bf16[256,2048]{1,0:T(8,128)(2,1)} %get-tuple-element.18.refs_1_), channel_id=1, source_target_pairs={{0,4},{4,8},{8,12},{12,0},{1,5},{5,9},{9,13},{13,1},{2,6},{6,10},{... | collective-permute-start | bytes 3145736 | tf_op jit(solution)/shard_map/ppermute | solution.py:48
  88.3 55.8 %collective-permute-start.7 = (bf16[128,2048]{1,0:T(8,128)(2,1)}, bf16[128,2048]{1,0:T(8,128)(2,1)}, u32[]{:S(2)}, u32[]{:S(2)}) collective-permute-start(bf16[128,2048]{1,0:T(8,128)(2,1)} %get-tuple-element.19.refs_8_), channel_id=1, source_target_pairs={{0,1},{1,2},{2,3},{3,0},{4,5},{5,6},{6,7},{7,4},{8,9},{9,10},{10,1... | collective-permute-start | bytes 1572872 | tf_op jit(solution)/shard_map/ppermute | solution.py:48
  93.2 35.9 %copy-start.14 = (bf16[16,2048]{1,0:T(8,128)(2,1)S(1)}, bf16[16,2048]{1,0:T(8,128)(2,1)}, u32[]{:S(2)}) copy-start(bf16[16,2048]{1,0:T(8,128)(2,1)} %param.20) | copy-start | bytes 196612
  93.2 36.0 %copy-start.15 = (f32[2048]{0:T(1024)S(1)}, f32[2048]{0:T(1024)}, u32[]{:S(2)}) copy-start(f32[2048]{0:T(1024)} %param.19) | copy-start | bytes 24580
  93.2 44.4 %copy-start.3 = (bf16[128,2048]{1,0:T(8,128)(2,1)S(1)}, bf16[128,2048]{1,0:T(8,128)(2,1)}, u32[]{:S(2)}) copy-start(bf16[128,2048]{1,0:T(8,128)(2,1)} %get-tuple-element.20.refs_9_) | copy-start | bytes 1572868
  94.3 59.7 %copy-start.1 = (bf16[256,2048]{1,0:T(8,128)(2,1)S(1)}, bf16[256,2048]{1,0:T(8,128)(2,1)}, u32[]{:S(2)}) copy-start(bf16[256,2048]{1,0:T(8,128)(2,1)} %get-tuple-element.17.refs_0_) | copy-start | bytes 3145732
  94.3 34.7 %all-to-all-start.4 = ((bf16[16,16,128]{2,1,0:T(8,128)(2,1)}), bf16[16,16,128]{2,1,0:T(8,128)(2,1)S(1)}, u32[]{:S(2)}, u32[]{:S(2)}) async-start(bf16[16,16,128]{2,1,0:T(8,128)(2,1)} %bitcast.8), calls=%async_computation.4 | async-start | bytes 131072 | tf_op jit(solution)/shard_map/all_to_all | solution.py:351
  129.6 14.6 %copy-start.2 = (bf16[128,2048]{1,0:T(8,128)(2,1)S(1)}, bf16[128,2048]{1,0:T(8,128)(2,1)}, u32[]{:S(2)}) copy-start(bf16[128,2048]{1,0:T(8,128)(2,1)} %get-tuple-element.19.refs_8_) | copy-start | bytes 1572868
  130.5 37.7 %all-to-all-start.5 = ((bf16[32,2,2048]{2,1,0:T(2,128)(2,1)}), bf16[32,2,2048]{2,1,0:T(2,128)(2,1)S(1)}, u32[]{:S(2)}, u32[]{:S(2)}) async-start(bf16[32,2,2048]{2,1,0:T(2,128)(2,1)} %all_to_all.48), calls=%async_computation.5 | async-start | bytes 524288 | tf_op jit(solution)/shard_map/all_to_all | solution.py:40
  137.7 16.4 %collective-permute-start.8 = (bf16[128,2048]{1,0:T(8,128)(2,1)S(1)}, bf16[128,2048]{1,0:T(8,128)(2,1)S(1)}, u32[]{:S(2)}, u32[]{:S(2)}) collective-permute-start(bf16[128,2048]{1,0:T(8,128)(2,1)S(1)} %copy-done.3), channel_id=1, source_target_pairs={{0,4},{4,8},{8,12},{12,0},{1,5},{5,9},{9,13},{13,1},{2,6},{6,10},{... | collective-permute-start | bytes 1572872 | tf_op jit(solution)/shard_map/ppermute | solution.py:48
  139.8 16.6 %collective-permute-start.10 = (bf16[128,2048]{1,0:T(8,128)(2,1)S(1)}, bf16[128,2048]{1,0:T(8,128)(2,1)S(1)}, u32[]{:S(2)}, u32[]{:S(2)}) collective-permute-start(bf16[128,2048]{1,0:T(8,128)(2,1)S(1)} %copy-done.3), channel_id=1, source_target_pairs={{0,12},{4,0},{8,4},{12,8},{1,13},{5,1},{9,5},{13,9},{2,14},{6,2},{... | collective-permute-start | bytes 1572872 | tf_op jit(solution)/shard_map/ppermute | solution.py:48
  144.2 15.9 %collective-permute-start.9 = (bf16[128,2048]{1,0:T(8,128)(2,1)S(1)}, bf16[128,2048]{1,0:T(8,128)(2,1)S(1)}, u32[]{:S(2)}, u32[]{:S(2)}) collective-permute-start(bf16[128,2048]{1,0:T(8,128)(2,1)S(1)} %copy-done.2), channel_id=1, source_target_pairs={{0,3},{1,0},{2,1},{3,2},{4,7},{5,4},{6,5},{7,6},{8,11},{9,8},{10,9... | collective-permute-start | bytes 1572872 | tf_op jit(solution)/shard_map/ppermute | solution.py:48
  154.0 6.1 %copy-start.5 = (bf16[128,2048]{1,0:T(8,128)(2,1)}, bf16[128,2048]{1,0:T(8,128)(2,1)S(1)}, u32[]{:S(2)}) copy-start(bf16[128,2048]{1,0:T(8,128)(2,1)S(1)} %collective-permute-done.8.refs_11_) | copy-start | bytes 1572868
  154.0 61.0 %collective-permute-start.3 = (bf16[256,2048]{1,0:T(8,128)(2,1)S(1)}, bf16[256,2048]{1,0:T(8,128)(2,1)}, u32[]{:S(2)}, u32[]{:S(2)}) collective-permute-start(bf16[256,2048]{1,0:T(8,128)(2,1)S(1)} %copy-done.1), channel_id=1, source_target_pairs={{0,3},{1,0},{2,1},{3,2},{4,7},{5,4},{6,5},{7,6},{8,11},{9,8},{10,9... | collective-permute-start | bytes 3145736 | tf_op jit(solution)/shard_map/ppermute | solution.py:48
  156.4 0.8 copy-start.7
  157.2 19.3 %collective-permute-start.11 = (bf16[128,2048]{1,0:T(8,128)(2,1)}, bf16[128,2048]{1,0:T(8,128)(2,1)}, u32[]{:S(2)}, u32[]{:S(2)}) collective-permute-start(bf16[128,2048]{1,0:T(8,128)(2,1)} %collective-permute-done.7.refs_10_), channel_id=1, source_target_pairs={{0,1},{1,2},{2,3},{3,0},{4,5},{5,6},{6,7},{7,4},{8,9},{9,10},{10,1... | collective-permute-start | bytes 1572872 | tf_op jit(solution)/shard_map/ppermute | solution.py:48
  160.1 0.8 copy-start.9
  160.9 54.1 %collective-permute-start.4 = (bf16[256,2048]{1,0:T(8,128)(2,1)}, bf16[256,2048]{1,0:T(8,128)(2,1)}, u32[]{:S(2)}, u32[]{:S(2)}) collective-permute-start(bf16[256,2048]{1,0:T(8,128)(2,1)} %get-tuple-element.18.refs_1_), channel_id=1, source_target_pairs={{0,12},{4,0},{8,4},{12,8},{1,13},{5,1},{9,5},{13,9},{2,14},{6,2},{... | collective-permute-start | bytes 3145736 | tf_op jit(solution)/shard_map/ppermute | solution.py:48
  163.8 51.3 %collective-permute-start.5 = (bf16[256,2048]{1,0:T(8,128)(2,1)}, bf16[256,2048]{1,0:T(8,128)(2,1)}, u32[]{:S(2)}, u32[]{:S(2)}) collective-permute-start(bf16[256,2048]{1,0:T(8,128)(2,1)} %collective-permute-done.1.refs_2_), channel_id=1, source_target_pairs={{0,1},{1,2},{2,3},{3,0},{4,5},{5,6},{6,7},{7,4},{8,9},{9,10},{10,1... | collective-permute-start | bytes 3145736 | tf_op jit(solution)/shard_map/ppermute | solution.py:48
  165.9 49.1 %collective-permute-start.6 = (bf16[256,2048]{1,0:T(8,128)(2,1)}, bf16[256,2048]{1,0:T(8,128)(2,1)}, u32[]{:S(2)}, u32[]{:S(2)}) collective-permute-start(bf16[256,2048]{1,0:T(8,128)(2,1)} %collective-permute-done.2.refs_3_), channel_id=1, source_target_pairs={{0,4},{4,8},{8,12},{12,0},{1,5},{5,9},{9,13},{13,1},{2,6},{6,10},{... | collective-permute-start | bytes 3145736 | tf_op jit(solution)/shard_map/ppermute | solution.py:48
  169.4 45.6 %all-to-all-start.6 = ((bf16[16,16,2048]{2,1,0:T(8,128)(2,1)}), bf16[16,16,2048]{2,1,0:T(8,128)(2,1)S(1)}, u32[]{:S(2)}, u32[]{:S(2)}) async-start(bf16[16,16,2048]{2,1,0:T(8,128)(2,1)} %deal.1), calls=%async_computation.6 | async-start | bytes 2097152 | tf_op jit(solution)/shard_map/all_to_all | solution.py:40
  176.5 37.7 %collective-permute-start.12 = (bf16[128,2048]{1,0:T(8,128)(2,1)}, bf16[128,2048]{1,0:T(8,128)(2,1)S(1)}, u32[]{:S(2)}, u32[]{:S(2)}) collective-permute-start(bf16[128,2048]{1,0:T(8,128)(2,1)} %copy-done.5), channel_id=1, source_target_pairs={{0,4},{4,8},{8,12},{12,0},{1,5},{5,9},{9,13},{13,1},{2,6},{6,10},{... | collective-permute-start | bytes 1572872 | tf_op jit(solution)/shard_map/ppermute | solution.py:48
  214.2 0.8 copy-start.11
  215.1 1.0 copy-start.4
  216.1 1.0 copy-start.6
  217.2 1.0 copy-start.8
  218.2 1.0 copy-start.10
  219.2 1.0 copy-start.12
  248.6 16.0 %copy-start.17 = (f32[16,2]{0,1:T(2,128)S(1)}, f32[16,2]{0,1:T(2,128)}, u32[]{:S(2)}) copy-start(f32[16,2]{0,1:T(2,128)} %param.22) | copy-start | bytes 388
  248.6 38.3 %all-to-all-start.8 = ((bf16[32,2,2048]{2,1,0:T(2,128)(2,1)}), bf16[32,2,2048]{2,1,0:T(2,128)(2,1)S(1)}, u32[]{:S(2)}, u32[]{:S(2)}) async-start(bf16[32,2,2048]{2,1,0:T(2,128)(2,1)} %all_to_all.52), calls=%async_computation.8 | async-start | bytes 524288 | tf_op jit(solution)/shard_map/all_to_all | solution.py:40

commit v5 on v4

--- a/solution.py
+++ b/solution.py
@@ -22,6 +22,7 @@
 TP = ("yh", "yl", "x")
 GROUP = ("yl", "x")
 STAT_ROWS = 16
+FOLD = 8
 EXPERT_GRANT = 46
 SHARE = 128
 NSHARE = 4
@@ -65,34 +66,46 @@
     return (f * jnp.cos(angle) + other * jnp.sin(angle)).astype(BF)
 
 
-def prepare_kernel(at_ref, q_ref, k_ref, v_ref, q_gain_ref, k_gain_ref, q8_ref, kv_ref):
-    q_rot = turned(q_ref[...], q_gain_ref[...], at_ref[2])
-    for i in range(q8_ref.shape[0]):
-        q8_ref[i] = q_rot
-    k_rot = turned(k_ref[...], k_gain_ref[...], at_ref[3])
+def queries_kernel(start_ref, q_ref, gain_ref, out_ref):
+    q_rot = turned(q_ref[...], gain_ref[...], start_ref[0])
+    for i in range(out_ref.shape[0]):
+        out_ref[i] = q_rot
+
+
+def prepare_queries(queries, gain, start):
+    return pl.pallas_call(
+        queries_kernel,
+        in_specs=[pl.BlockSpec(memory_space=pltpu.SMEM), IN_VMEM, IN_VMEM],
+        out_specs=IN_VMEM,
+        out_shape=jax.ShapeDtypeStruct((NG, *queries.shape), BF),
+        name="prepare_queries",
+    )(start.reshape(1), queries, gain[None, :])
+
+
+def keys_kernel(at_ref, k_ref, v_ref, gain_ref, out_ref):
+    k_rot = turned(k_ref[...], gain_ref[...], at_ref[2])
     both = jnp.concatenate([k_rot, v_ref[...]], axis=1)
-    for i in range(kv_ref.shape[0]):
-        kv_ref[i] = both
-
-
-def prepare(queries, keys, values, query_gain, key_gain, block, head, start):
-    tokens, width = queries.shape
-    size = tokens // NG
-    at = jnp.stack([block, head, start, start + block * size]).astype(jnp.int32)
-    whole = lambda shape: pl.BlockSpec(shape, lambda i, at: (0,) * len(shape))
+    for i in range(out_ref.shape[0]):
+        out_ref[i] = both
+
+
+def prepare_keys(keys, values, gain, block, head, start):
+    width = gain.shape[0]
+    size = keys.shape[0] // NG
+    at = jnp.stack([block, head, start + block * size]).astype(jnp.int32)
     part = pl.BlockSpec((size, width), lambda i, at: (at[0], at[1]))
-    outs = ((NG, tokens, width), (NZ, size, 2 * width))
-    return pl.pallas_call(
-        prepare_kernel,
+    out = (NZ, size, 2 * width)
+    return pl.pallas_call(
+        keys_kernel,
         grid_spec=pltpu.PrefetchScalarGridSpec(
             num_scalar_prefetch=1,
             grid=(1,),
-            in_specs=[whole((tokens, width)), part, part, whole((1, width)), whole((1, width))],
-            out_specs=[whole(shape) for shape in outs],
+            in_specs=[part, part, pl.BlockSpec((1, width), lambda i, at: (0, 0))],
+            out_specs=pl.BlockSpec(out, lambda i, at: (0, 0, 0)),
         ),
-        out_shape=[jax.ShapeDtypeStruct(shape, BF) for shape in outs],
-        name="prepare",
-    )(at, queries, keys, values, query_gain[None, :], key_gain[None, :])
+        out_shape=jax.ShapeDtypeStruct(out, BF),
+        name="prepare_keys",
+    )(at, keys, values, gain[None, :])
 
 
 def split3(x):
@@ -180,41 +193,126 @@
     )(parts)
 
 
-def deal_kernel(classes_ref, out_ref):
-    for i, k in enumerate(COLOURS):
-        out_ref[i] = classes_ref[k]
-
-
-def deal(classes):
+def folded(rows):
+    width = rows.shape[1] // FOLD
+    return jnp.concatenate(
+        [rows[:, j * width : (j + 1) * width] for j in range(FOLD)], axis=0
+    )
+
+
+def picking(outs, ins, source_of):
+    i = lax.broadcasted_iota(jnp.int32, (outs, ins), 0)
+    r = lax.broadcasted_iota(jnp.int32, (outs, ins), 1)
+    return jnp.where(r == source_of(i), 1.0, 0.0).astype(BF)
+
+
+def mix_kernel(projected_ref, residual_ref, scale_ref, selector_ref, mixed_ref, sent_ref):
+    projected = jnp.concatenate(
+        [projected_ref[i].astype(F32) for i in range(projected_ref.shape[0])], axis=1
+    )
+    mixed = (residual_ref[...].astype(F32) + projected).astype(BF)
+    mixed_ref[...] = mixed
+    mixed = mixed.astype(F32)
+    mean = jnp.mean(mixed * mixed, axis=-1, keepdims=True)
+    normed = (mixed * lax.rsqrt(mean + EPS) * scale_ref[...]).astype(BF)
+    sent_ref[...] = jnp.dot(
+        selector_ref[...], folded(normed), preferred_element_type=F32
+    ).astype(BF)
+
+
+def mix(projected, residual, scale, selector):
+    shape = (selector.shape[0], residual.shape[1] // FOLD)
+    return pl.pallas_call(
+        mix_kernel,
+        in_specs=[IN_VMEM] * 4,
+        out_specs=[IN_VMEM] * 2,
+        out_shape=[
+            jax.ShapeDtypeStruct(residual.shape, BF),
+            jax.ShapeDtypeStruct(shape, BF),
+        ],
+        compiler_params=grant(16),
+        name="mix",
+    )(projected, residual, scale[None, :], selector)
+
+
+def deal_kernel(arrived_ref, out_ref):
+    total, _ = arrived_ref.shape
+    count, each = total // FOLD, out_ref.shape[1]
+    unfold = picking(total, total, lambda i: i % count * FOLD + i // count)
+    rows = jnp.dot(unfold, arrived_ref[...], preferred_element_type=F32).astype(BF)
+    for k in range(NSHARE):
+        mine = jnp.concatenate(
+            [rows[j * count + k * each : j * count + (k + 1) * each] for j in range(FOLD)],
+            axis=1,
+        )
+        for i, colour in enumerate(COLOURS):
+            if colour == k:
+                out_ref[i] = mine
+
+
+def deal(arrived):
+    total, width = arrived.shape
     return pl.pallas_call(
         deal_kernel,
         in_specs=[IN_VMEM],
         out_specs=IN_VMEM,
-        out_shape=jax.ShapeDtypeStruct((NT, *classes.shape[1:]), BF),
+        out_shape=jax.ShapeDtypeStruct((NT, total // FOLD // NSHARE, width * FOLD), BF),
         compiler_params=grant(16),
         name="deal",
-    )(classes)
+    )(arrived)
 
 
 def collect_kernel(back_ref, out_ref):
+    classes = []
     for k in range(NSHARE):
         total = None
         for i, colour in enumerate(COLOURS):
             if colour == k:
                 part = back_ref[i].astype(F32)
                 total = part if total is None else total + part
-        out_ref[k] = total.astype(BF)
+        classes.append(total.astype(BF))
+    rows = jnp.concatenate(classes, axis=0)
+    count = rows.shape[0]
+    fold = picking(
+        FOLD * count, FOLD * count, lambda i: i % FOLD * count + i // FOLD
+    )
+    out_ref[...] = jnp.dot(fold, folded(rows), preferred_element_type=F32).astype(BF)
 
 
 def collect(back):
+    _, each, depth = back.shape
     return pl.pallas_call(
         collect_kernel,
         in_specs=[IN_VMEM],
         out_specs=IN_VMEM,
-        out_shape=jax.ShapeDtypeStruct((NSHARE, *back.shape[1:]), BF),
+        out_shape=jax.ShapeDtypeStruct((NSHARE * each * FOLD, depth // FOLD), BF),
         compiler_params=grant(16),
         name="collect",
     )(back)
+
+
+def finish_kernel(mixed_ref, returned_ref, weights_ref, *refs):
+    picks, out_ref = refs[:-1], refs[-1]
+    tokens, depth = mixed_ref.shape
+    width = depth // FOLD
+    found = [
+        jnp.dot(pick[...], returned_ref[...], preferred_element_type=F32) for pick in picks
+    ]
+    for j in range(FOLD):
+        cols, rows = slice(j * width, (j + 1) * width), slice(j * tokens, (j + 1) * tokens)
+        moe = sum(f[rows] * weights_ref[:, k : k + 1] for k, f in enumerate(found))
+        out_ref[:, cols] = (mixed_ref[:, cols].astype(F32) + moe).astype(BF)
+
+
+def finish(mixed, returned, weights, picks):
+    return pl.pallas_call(
+        finish_kernel,
+        in_specs=[IN_VMEM] * (3 + len(picks)),
+        out_specs=IN_VMEM,
+        out_shape=jax.ShapeDtypeStruct(mixed.shape, BF),
+        compiler_params=grant(16),
+        name="finish",
+    )(mixed, returned, weights, *picks)
 
 
 def pack_kernel(gate_ref, up_ref, down_ref, *out_refs):
@@ -325,10 +423,9 @@
     yh, yl, x = lax.axis_index("yh"), lax.axis_index("yl"), lax.axis_index("x")
     start = (z * NC + c) * tok_sp
 
-    q8, kv = prepare(
-        queries, keys, values, query_gain, key_gain, yl * NX + x, yh, start
-    )
+    q8 = prepare_queries(queries, query_gain, start)
     q8 = exchange(q8, GROUP)
+    kv = prepare_keys(keys, values, key_gain, yl * NX + x, yh, start)
     q8, kv = lax.optimization_barrier((q8, kv))
     kv_mine = exchange(kv, "z").reshape(-1, 2 * width)
     kv_other = swap_cores(kv_mine)
@@ -348,21 +445,15 @@
     columns = lax.dot_general(
         attn_all, out_proj, (((0,), (0,)), ((), ())), preferred_element_type=F32
     ).astype(BF)
-    projected = lax.all_to_all(columns, TP, split_axis=0, concat_axis=1, tiled=True)
-    mixed = (residual.astype(F32) + projected.astype(F32)).astype(BF)
-    mixed_f = mixed.astype(F32)
-    normed = (
-        mixed_f
-        * lax.rsqrt(jnp.mean(mixed_f * mixed_f, axis=-1, keepdims=True) + EPS)
-        * expert_norm_scale
-    ).astype(BF)
+    projected = exchange(columns.reshape(NT, tok_dev, -1), TP)
 
     cap = max(2, 2 * tok_dev * top // (NZ * NC))
     tok = jnp.arange(tok_dev, dtype=jnp.int32)
     before = tok[None, :] < tok[:, None]
-    place = jnp.arange(NZ * NC * cap, dtype=jnp.int32)
-    expert_of, slot_of = place // cap, place % cap
-    hits = []
+    place = jnp.arange(NZ * NC * cap * FOLD, dtype=jnp.int32)
+    row = jnp.arange(FOLD * tok_dev, dtype=jnp.int32)
+    same_fold = (row // tok_dev)[:, None] == (place % FOLD)[None, :]
+    picks = []
     for k in range(top):
         mine = routes[:, k]
         slot = sum(
@@ -371,26 +462,19 @@
             )
             for j in range(top)
         )
-        hits.append(
-            (mine[:, None] == expert_of[None, :]) & (slot[:, None] == slot_of[None, :])
+        target = jnp.tile(mine * cap + slot, FOLD)
+        picks.append(
+            (same_fold & (target[:, None] == (place // FOLD)[None, :])).astype(BF)
         )
-    selector = sum(h.astype(BF) for h in hits)
-    sent = lax.dot_general(
-        selector, normed, (((0,), (0,)), ((), ())), preferred_element_type=F32
-    ).astype(BF)
-    arrived = exchange(sent, ("z", "c"))
-
-    classes = arrived.reshape(NSHARE, NZ * NC * cap // NSHARE, depth)
-    rows = exchange(deal(classes), TP)
+    mixed, sent = mix(projected, residual, expert_norm_scale, sum(picks).T)
+    blocks = (NZ * NC, cap * FOLD, depth // FOLD)
+    arrived = exchange(sent.reshape(blocks), ("z", "c"))
+
+    rows = exchange(deal(arrived.reshape(sent.shape)), TP)
     partial = experts(rows.reshape(-1, depth), pieces)
     back = exchange(partial.reshape(rows.shape), TP)
-    picked_from = exchange(collect(back).reshape(arrived.shape), ("z", "c"))
-    moe = sum(
-        jnp.dot(hits[k].astype(BF), picked_from, preferred_element_type=F32)
-        * route_weights[:, k][:, None]
-        for k in range(top)
-    )
-    return (mixed_f + moe).astype(BF)
+    returned = exchange(collect(back).reshape(blocks), ("z", "c"))
+    return finish(mixed, returned.reshape(sent.shape), route_weights, picks)
 
 
 def solution(mesh):

time: 289 us -> 284 us (0.983)
  blocking collectives: 74.3 us -> 63.8 us
  Pallas kernels: 21.6 us -> 26.3 us
    all_to_all x4 -> x6, waiting for transfers between devices: 23.8 us -> 56.4 us  [exchange(): return lax.all_to_all(blocks, axis, split_axis=0, concat_axis=0, tiled=True)]
    all_to_all x1 -> x0, waiting for transfers between devices: 29.6 us -> none  [local(): lax.all_to_all(columns, TP, split_axis=0, concat_axis=1, tiled=True)]
    all_to_all x4 -> x3, blocking collectives: 74.3 us -> 63.8 us  [exchange(): return lax.all_to_all(blocks, axis, split_axis=0, concat_axis=0, tiled=True)]
    all_to_all x4 -> x6, starting transfers between devices: 34.5 us -> 44 us  [exchange(): return lax.all_to_all(blocks, axis, split_axis=0, concat_axis=0, tiled=True)]
    all_to_all x1 -> x0, starting transfers between devices: 5.15 us -> none  [local(): lax.all_to_all(columns, TP, split_axis=0, concat_axis=1, tiled=True)]
    pallas_call x1 -> x4, Pallas kernels: 3.07 us -> 6.5 us  [the longest x1 2.33 us: prepare_queries(): pl.pallas_call(queries_kernel, in_specs=[pl.BlockSpec(memory_space=pltpu....]
    ppermute x12, starting transfers between devices: 34.2 us -> 30.9 us  [ring(): return lax.ppermute(value, axis, [(i, (i + step) % 4) for i in range(4)])]
    unnamed x36 -> x31, local copies, waits for them, and re-layouts: 7.61 us -> 6.64 us
  transfers between devices with their start and end apart: 18 -> 19, of which waited for: 6 -> 10; matrix products, arithmetic and copies ran while one was open for 1% -> 1% of each run, Pallas kernels for 2% -> 3%
where the time goes in v5:
time: 284 us; the launch traced here: 283 us
  waiting for transfers between devices  98.9 us (35%)
  starting transfers between devices  82.8 us (29%)
  blocking collectives  63.8 us (22%)
  Pallas kernels  26.3 us (9%)
  local copies, waits for them, and re-layouts  6.81 us (2%)
    all_to_all x3, blocking collectives, exchange(): return lax.all_to_all(blocks, axis, split_axis=0, concat_axis=0, tiled=True)  63.8 us
    all_to_all x6, waiting for transfers between devices, exchange(): return lax.all_to_all(blocks, axis, split_axis=0, concat_axis=0, tiled=True)  56.4 us
    all_to_all x6, starting transfers between devices, exchange(): return lax.all_to_all(blocks, axis, split_axis=0, concat_axis=0, tiled=True)  44 us
    ppermute x12, waiting for transfers between devices, ring(): return lax.ppermute(value, axis, [(i, (i + step) % 4) for i in range(4)])  41.3 us
    ppermute x12, starting transfers between devices, ring(): return lax.ppermute(value, axis, [(i, (i + step) % 4) for i in range(4)])  30.9 us
    pallas_call x1, Pallas kernels, experts(): pl.pallas_call(experts_kernel, in_specs=[IN_VMEM] + [IN_HBM] * len(pieces...  8.83 us
    ppermute x1, starting transfers between devices, swap_cores(): return lax.ppermute(value, 'c', [(0, 1), (1, 0)])  7.91 us
    unnamed x31, local copies, waits for them, and re-layouts  6.64 us
  transfers between devices with their start and end apart: 19, of which 10 were waited for; matrix products, arithmetic and copies ran while one was open for 1% of the time, Pallas kernels for 3%

profile of v5, /device:TPU:1, one launch (start us, length us, event | category | flops | bytes accessed | tf_op | source)
XLA Modules:
  0.0 282.6 jit_solution(1114291782371638819)
XLA Ops:
  0.0 2.3 prepare_queries.1
  2.3 5.9 %all-to-all-start = ((bf16[8,256,128]{2,1,0:T(8,128)(2,1)}), bf16[8,256,128]{2,1,0:T(8,128)(2,1)S(1)}, u32[]{:S(2)}, u32[]{:S(2)}) async-start(bf16[8,256,128]{2,1,0:T(8,128)(2,1)} %prepare_queries.1), calls=%async_computation | async-start | bytes 1048576 | tf_op jit(solution)/shard_map/all_to_all | solution.py:41
  8.8 2.3 prepare_keys.1
  11.1 4.7 %all-to-all-done.q_ref = bf16[8,256,128]{2,1,0:T(8,128)(2,1)S(1)} async-done(((bf16[8,256,128]{2,1,0:T(8,128)(2,1)}), bf16[8,256,128]{2,1,0:T(8,128)(2,1)S(1)}, u32[]{:S(2)}, u32[]{:S(2)}) %all-to-all-start) | async-done | bytes 524320 | tf_op jit(solution)/shard_map/all_to_all | solution.py:41
  15.7 31.2 %all_to_all.45 = bf16[16,32,256]{2,1,0:T(8,128)(2,1)S(1)} all-to-all(bf16[16,32,256]{2,1,0:T(8,128)(2,1)} %prepare_keys.1), channel_id=1, replica_groups=mesh['z'=16,'c'=2,'yh'=2,'yl'=2,'x'=4] {'z'}, dimensions={0} | all-to-all | bytes 524288 | tf_op jit(solution)/shard_map/all_to_all | solution.py:41
  46.9 7.9 %collective-permute-start = (bf16[512,256]{1,0:T(8,128)(2,1)S(1)}, bf16[512,256]{1,0:T(8,128)(2,1)S(1)}, u32[]{:S(2)}, u32[]{:S(2)}) collective-permute-start(bf16[512,256]{1,0:T(8,128)(2,1)S(1)} %bitcast.29), channel_id=1, source_target_pairs={{0,16},{16,0},{1,17},{17,1},{2,18},{18,2},{3,19},{19,3},{4,20},{20... | collective-permute-start | bytes 786440 | tf_op jit(solution)/shard_map/ppermute | solution.py:45
  54.8 1.1 collective-permute-done.other_ref
  55.9 3.3 %attend.1 = bf16[8,144,256]{2,1,0:T(8,128)(2,1)S(1)} custom-call(bf16[8,256,128]{2,1,0:T(8,128)(2,1)S(1)} %all-to-all-done.q_ref, bf16[512,256]{1,0:T(8,128)(2,1)S(1)} %bitcast.30, bf16[512,256]{1,0:T(8,128)(2,1)S(1)} %collective-permute-done.other_ref), custom_call_target="tpu_custom_call" | custom-call | tf_op jit(solution)/shard_map/attend/pallas_call | solution.py:152
  59.3 13.2 %all_to_all.46.parts_ref = bf16[8,144,256]{2,1,0:T(8,128)(2,1)S(1)} all-to-all(bf16[8,144,256]{2,1,0:T(8,128)(2,1)S(1)} %attend.1), channel_id=1, replica_groups=mesh['z'=16,'c'=2,'yh'=2,'yl'=2,'x'=4] {'yl','x'}, dimensions={0} | all-to-all | bytes 1179648 | tf_op jit(solution)/shard_map/all_to_all | solution.py:41
  72.4 1.2 combine.1
  73.7 4.5 %all-to-all-start.3 = ((bf16[16,128,256]{2,1,0:T(8,128)(2,1)}), bf16[16,128,256]{2,1,0:T(8,128)(2,1)}, u32[]{:S(2)}, u32[]{:S(2)}) async-start(bf16[16,128,256]{2,1,0:T(8,128)(2,1)} %combine.1), calls=%async_computation.3 | async-start | bytes 2097152 | tf_op jit(solution)/shard_map/all_to_all | solution.py:41
  78.2 4.0 %pack.1 = (bf16[256,2048]{1,0:T(8,128)(2,1)}, bf16[256,2048]{1,0:T(8,128)(2,1)}, bf16[128,2048]{1,0:T(8,128)(2,1)}, bf16[128,2048]{1,0:T(8,128)(2,1)}) custom-call(bf16[1,2048,256]{2,1,0:T(8,128)(2,1)} %gate_ref.1, bf16[1,2048,256]{2,1,0:T(8,128)(2,1)} %up_ref.1, bf16[1,256,2048]{2,1,0:T(8,128)(2,1)} %down_ref.1), custom_call_target="tpu_custom_call" | custom-call | tf_op jit(solution)/shard_map/pack/pallas_call | solution.py:331
  82.1 3.2 %collective-permute-start.1 = (bf16[256,2048]{1,0:T(8,128)(2,1)}, bf16[256,2048]{1,0:T(8,128)(2,1)}, u32[]{:S(2)}, u32[]{:S(2)}) collective-permute-start(bf16[256,2048]{1,0:T(8,128)(2,1)} %get-tuple-element.17.refs_0_), channel_id=1, source_target_pairs={{0,1},{1,2},{2,3},{3,0},{4,5},{5,6},{6,7},{7,4},{8,9},{9,10},{10,1... | collective-permute-start | bytes 3145736 | tf_op jit(solution)/shard_map/ppermute | solution.py:49
  85.3 3.1 %collective-permute-start.2 = (bf16[256,2048]{1,0:T(8,128)(2,1)}, bf16[256,2048]{1,0:T(8,128)(2,1)}, u32[]{:S(2)}, u32[]{:S(2)}) collective-permute-start(bf16[256,2048]{1,0:T(8,128)(2,1)} %get-tuple-element.18.refs_1_), channel_id=1, source_target_pairs={{0,4},{4,8},{8,12},{12,0},{1,5},{5,9},{9,13},{13,1},{2,6},{6,10},{... | collective-permute-start | bytes 3145736 | tf_op jit(solution)/shard_map/ppermute | solution.py:49
  88.4 3.1 %collective-permute-start.7 = (bf16[128,2048]{1,0:T(8,128)(2,1)}, bf16[128,2048]{1,0:T(8,128)(2,1)S(1)}, u32[]{:S(2)}, u32[]{:S(2)}) collective-permute-start(bf16[128,2048]{1,0:T(8,128)(2,1)} %get-tuple-element.19.refs_8_), channel_id=1, source_target_pairs={{0,1},{1,2},{2,3},{3,0},{4,5},{5,6},{6,7},{7,4},{8,9},{9,10},{10,1... | collective-permute-start | bytes 1572872 | tf_op jit(solution)/shard_map/ppermute | solution.py:49
  92.0 1.6 all-to-all-done.3
  93.6 2.4 convolution_convert_fusion
  96.1 4.7 %all-to-all-start.4 = ((bf16[16,16,128]{2,1,0:T(8,128)(2,1)}), bf16[16,16,128]{2,1,0:T(8,128)(2,1)S(1)}, u32[]{:S(2)}, u32[]{:S(2)}) async-start(bf16[16,16,128]{2,1,0:T(8,128)(2,1)} %bitcast.8), calls=%async_computation.4 | async-start | bytes 131072 | tf_op jit(solution)/shard_map/all_to_all | solution.py:41
  101.0 28.2 %all-to-all-done.4.projected_ref = bf16[16,16,128]{2,1,0:T(8,128)(2,1)S(1)} async-done(((bf16[16,16,128]{2,1,0:T(8,128)(2,1)}), bf16[16,16,128]{2,1,0:T(8,128)(2,1)S(1)}, u32[]{:S(2)}, u32[]{:S(2)}) %all-to-all-start.4) | async-done | bytes 65568 | tf_op jit(solution)/shard_map/all_to_all | solution.py:41
  129.2 1.0 mix.1
  130.2 7.1 %all-to-all-start.5 = ((bf16[32,16,256]{2,1,0:T(8,128)(2,1)}), bf16[32,16,256]{2,1,0:T(8,128)(2,1)S(1)}, u32[]{:S(2)}, u32[]{:S(2)}) async-start(bf16[32,16,256]{2,1,0:T(8,128)(2,1)} %bitcast.12), calls=%async_computation.5 | async-start | bytes 524288 | tf_op jit(solution)/shard_map/all_to_all | solution.py:41
  137.3 2.2 collective-permute-start.8
  139.5 2.4 collective-permute-start.9
  141.9 2.2 collective-permute-start.3
  144.1 9.8 %collective-permute-done.8.refs_11_ = bf16[128,2048]{1,0:T(8,128)(2,1)} collective-permute-done((bf16[128,2048]{1,0:T(8,128)(2,1)}, bf16[128,2048]{1,0:T(8,128)(2,1)}, u32[]{:S(2)}, u32[]{:S(2)}) %collective-permute-start.8) | collective-permute-done | bytes 524320 | tf_op jit(solution)/shard_map/ppermute | solution.py:49
  154.0 1.9 collective-permute-start.10
  155.9 0.8 copy-done.5
  156.7 2.8 collective-permute-start.4
  159.5 1.9 collective-permute-start.5
  161.4 2.5 collective-permute-start.6
  164.0 1.4 deal.1
  165.4 6.0 %all-to-all-start.6 = ((bf16[16,16,2048]{2,1,0:T(8,128)(2,1)}), bf16[16,16,2048]{2,1,0:T(8,128)(2,1)S(1)}, u32[]{:S(2)}, u32[]{:S(2)}) async-start(bf16[16,16,2048]{2,1,0:T(8,128)(2,1)} %deal.1), calls=%async_computation.6 | async-start | bytes 2097152 | tf_op jit(solution)/shard_map/all_to_all | solution.py:41
  171.4 3.3 %collective-permute-start.11 = (bf16[128,2048]{1,0:T(8,128)(2,1)}, bf16[128,2048]{1,0:T(8,128)(2,1)S(1)}, u32[]{:S(2)}, u32[]{:S(2)}) collective-permute-start(bf16[128,2048]{1,0:T(8,128)(2,1)} %copy-done.3), channel_id=1, source_target_pairs={{0,1},{1,2},{2,3},{3,0},{4,5},{5,6},{6,7},{7,4},{8,9},{9,10},{10,1... | collective-permute-start | bytes 1572872 | tf_op jit(solution)/shard_map/ppermute | solution.py:49
  174.7 2.2 collective-permute-done.3.refs_4_
  176.9 2.4 collective-permute-start.12
  179.3 20.1 %collective-permute-done.4.refs_5_ = bf16[256,2048]{1,0:T(8,128)(2,1)} collective-permute-done((bf16[256,2048]{1,0:T(8,128)(2,1)}, bf16[256,2048]{1,0:T(8,128)(2,1)}, u32[]{:S(2)}, u32[]{:S(2)}) %collective-permute-start.4) | collective-permute-done | bytes 1048608 | tf_op jit(solution)/shard_map/ppermute | solution.py:49
  199.5 7.9 %collective-permute-done.11.refs_14_ = bf16[128,2048]{1,0:T(8,128)(2,1)S(1)} collective-permute-done((bf16[128,2048]{1,0:T(8,128)(2,1)}, bf16[128,2048]{1,0:T(8,128)(2,1)S(1)}, u32[]{:S(2)}, u32[]{:S(2)}) %collective-permute-start.11) | collective-permute-done | bytes 524320 | tf_op jit(solution)/shard_map/ppermute | solution.py:49
  208.2 1.2 collective-permute-done.12.refs_15_
  210.1 1.0 copy-done.4
  211.2 1.0 copy-done.6
  212.2 1.0 copy-done.8
  213.2 1.0 copy-done.10
  214.3 8.8 %experts.1 = bf16[256,2048]{1,0:T(8,128)(2,1)S(1)} custom-call(bf16[256,2048]{1,0:T(8,128)(2,1)S(1)} %bitcast.26, bf16[256,2048]{1,0:T(8,128)(2,1)S(1)} %copy-done.1, bf16[256,2048]{1,0:T(8,128)(2,1)} %get-tuple-element.18.refs_1_, bf16[256,2048]{1,0:T(8,128)(2,1)} %collective-permute-done.1.refs_2_, bf16[256,2048]{1,0:T(8,128)(2,1)} %collective-permute-done.2.refs_3_, ...), custom_call_target="tpu_custom_call" | custom-call | tf_op jit(solution)/shard_map/experts/pallas_call | solution.py:388
  223.1 19.4 %all_to_all.47.back_ref = bf16[16,16,2048]{2,1,0:T(8,128)(2,1)S(1)} all-to-all(bf16[16,16,2048]{2,1,0:T(8,128)(2,1)S(1)} %bitcast.27), channel_id=1, replica_groups=mesh['z'=16,'c'=2,'yh'=2,'yl'=2,'x'=4] {'yh','yl','x'}, dimensions={0} | all-to-all | bytes 2097152 | tf_op jit(solution)/shard_map/all_to_all | solution.py:41
  242.6 1.1 collect.1
  243.7 15.8 %all-to-all-start.8 = ((bf16[32,16,256]{2,1,0:T(8,128)(2,1)}), bf16[32,16,256]{2,1,0:T(8,128)(2,1)S(1)}, u32[]{:S(2)}, u32[]{:S(2)}) async-start(bf16[32,16,256]{2,1,0:T(8,128)(2,1)} %bitcast.16), calls=%async_computation.8 | async-start | bytes 524288 | tf_op jit(solution)/shard_map/all_to_all | solution.py:41
  259.7 22.0 %all-to-all-done.8 = bf16[32,16,256]{2,1,0:T(8,128)(2,1)S(1)} async-done(((bf16[32,16,256]{2,1,0:T(8,128)(2,1)}), bf16[32,16,256]{2,1,0:T(8,128)(2,1)S(1)}, u32[]{:S(2)}, u32[]{:S(2)}) %all-to-all-start.8) | async-done | bytes 262176 | tf_op jit(solution)/shard_map/all_to_all | solution.py:41
  281.7 0.9 finish.1
  (47 shorter events, 3.1 us)
Async XLA Ops:
  0.0 93.6 %copy-start = (bf16[2048,128]{1,0:T(8,128)(2,1)S(1)}, bf16[2048,128]{1,0:T(8,128)(2,1)}, u32[]{:S(2)}) copy-start(bf16[2048,128]{1,0:T(8,128)(2,1)} %param.18) | copy-start | bytes 1572868
  2.3 13.4 %all-to-all-start = ((bf16[8,256,128]{2,1,0:T(8,128)(2,1)}), bf16[8,256,128]{2,1,0:T(8,128)(2,1)S(1)}, u32[]{:S(2)}, u32[]{:S(2)}) async-start(bf16[8,256,128]{2,1,0:T(8,128)(2,1)} %prepare_queries.1), calls=%async_computation | async-start | bytes 1048576 | tf_op jit(solution)/shard_map/all_to_all | solution.py:41
  46.9 9.1 %collective-permute-start = (bf16[512,256]{1,0:T(8,128)(2,1)S(1)}, bf16[512,256]{1,0:T(8,128)(2,1)S(1)}, u32[]{:S(2)}, u32[]{:S(2)}) collective-permute-start(bf16[512,256]{1,0:T(8,128)(2,1)S(1)} %bitcast.29), channel_id=1, source_target_pairs={{0,16},{16,0},{1,17},{17,1},{2,18},{18,2},{3,19},{19,3},{4,20},{20... | collective-permute-start | bytes 786440 | tf_op jit(solution)/shard_map/ppermute | solution.py:45
  73.7 20.0 %all-to-all-start.3 = ((bf16[16,128,256]{2,1,0:T(8,128)(2,1)}), bf16[16,128,256]{2,1,0:T(8,128)(2,1)}, u32[]{:S(2)}, u32[]{:S(2)}) async-start(bf16[16,128,256]{2,1,0:T(8,128)(2,1)} %combine.1), calls=%async_computation.3 | async-start | bytes 2097152 | tf_op jit(solution)/shard_map/all_to_all | solution.py:41
  82.1 77.4 %collective-permute-start.1 = (bf16[256,2048]{1,0:T(8,128)(2,1)}, bf16[256,2048]{1,0:T(8,128)(2,1)}, u32[]{:S(2)}, u32[]{:S(2)}) collective-permute-start(bf16[256,2048]{1,0:T(8,128)(2,1)} %get-tuple-element.17.refs_0_), channel_id=1, source_target_pairs={{0,1},{1,2},{2,3},{3,0},{4,5},{5,6},{6,7},{7,4},{8,9},{9,10},{10,1... | collective-permute-start | bytes 3145736 | tf_op jit(solution)/shard_map/ppermute | solution.py:49
  85.3 6.2 %copy-start.13 = (s32[16,2]{0,1:T(2,128)S(1)}, s32[16,2]{0,1:T(2,128)}, u32[]{:S(2)}) copy-start(s32[16,2]{0,1:T(2,128)} %param.21) | copy-start | bytes 388
  85.3 76.1 %collective-permute-start.2 = (bf16[256,2048]{1,0:T(8,128)(2,1)}, bf16[256,2048]{1,0:T(8,128)(2,1)}, u32[]{:S(2)}, u32[]{:S(2)}) collective-permute-start(bf16[256,2048]{1,0:T(8,128)(2,1)} %get-tuple-element.18.refs_1_), channel_id=1, source_target_pairs={{0,4},{4,8},{8,12},{12,0},{1,5},{5,9},{9,13},{13,1},{2,6},{6,10},{... | collective-permute-start | bytes 3145736 | tf_op jit(solution)/shard_map/ppermute | solution.py:49
  88.4 53.4 %collective-permute-start.7 = (bf16[128,2048]{1,0:T(8,128)(2,1)}, bf16[128,2048]{1,0:T(8,128)(2,1)S(1)}, u32[]{:S(2)}, u32[]{:S(2)}) collective-permute-start(bf16[128,2048]{1,0:T(8,128)(2,1)} %get-tuple-element.19.refs_8_), channel_id=1, source_target_pairs={{0,1},{1,2},{2,3},{3,0},{4,5},{5,6},{6,7},{7,4},{8,9},{9,10},{10,1... | collective-permute-start | bytes 1572872 | tf_op jit(solution)/shard_map/ppermute | solution.py:49
  93.6 35.5 %copy-start.11 = (bf16[16,2048]{1,0:T(8,128)(2,1)S(1)}, bf16[16,2048]{1,0:T(8,128)(2,1)}, u32[]{:S(2)}) copy-start(bf16[16,2048]{1,0:T(8,128)(2,1)} %residual_ref.1) | copy-start | bytes 196612
  93.6 35.5 %copy-start.12 = (f32[2048]{0:T(1024)S(1)}, f32[2048]{0:T(1024)}, u32[]{:S(2)}) copy-start(f32[2048]{0:T(1024)} %param.19) | copy-start | bytes 24580
  93.6 48.3 %copy-start.1 = (bf16[256,2048]{1,0:T(8,128)(2,1)S(1)}, bf16[256,2048]{1,0:T(8,128)(2,1)}, u32[]{:S(2)}) copy-start(bf16[256,2048]{1,0:T(8,128)(2,1)} %get-tuple-element.17.refs_0_) | copy-start | bytes 3145732
  96.0 43.4 %copy-start.2 = (bf16[128,2048]{1,0:T(8,128)(2,1)S(1)}, bf16[128,2048]{1,0:T(8,128)(2,1)}, u32[]{:S(2)}) copy-start(bf16[128,2048]{1,0:T(8,128)(2,1)} %get-tuple-element.19.refs_8_) | copy-start | bytes 1572868
  96.1 33.1 %all-to-all-start.4 = ((bf16[16,16,128]{2,1,0:T(8,128)(2,1)}), bf16[16,16,128]{2,1,0:T(8,128)(2,1)S(1)}, u32[]{:S(2)}, u32[]{:S(2)}) async-start(bf16[16,16,128]{2,1,0:T(8,128)(2,1)} %bitcast.8), calls=%async_computation.4 | async-start | bytes 131072 | tf_op jit(solution)/shard_map/all_to_all | solution.py:41
  130.2 33.8 %all-to-all-start.5 = ((bf16[32,16,256]{2,1,0:T(8,128)(2,1)}), bf16[32,16,256]{2,1,0:T(8,128)(2,1)S(1)}, u32[]{:S(2)}, u32[]{:S(2)}) async-start(bf16[32,16,256]{2,1,0:T(8,128)(2,1)} %bitcast.12), calls=%async_computation.5 | async-start | bytes 524288 | tf_op jit(solution)/shard_map/all_to_all | solution.py:41
  137.3 16.7 %collective-permute-start.8 = (bf16[128,2048]{1,0:T(8,128)(2,1)}, bf16[128,2048]{1,0:T(8,128)(2,1)}, u32[]{:S(2)}, u32[]{:S(2)}) collective-permute-start(bf16[128,2048]{1,0:T(8,128)(2,1)} %get-tuple-element.20.refs_9_), channel_id=1, source_target_pairs={{0,4},{4,8},{8,12},{12,0},{1,5},{5,9},{9,13},{13,1},{2,6},{6,10},{... | collective-permute-start | bytes 1572872 | tf_op jit(solution)/shard_map/ppermute | solution.py:49
  139.5 16.4 %collective-permute-start.9 = (bf16[128,2048]{1,0:T(8,128)(2,1)S(1)}, bf16[128,2048]{1,0:T(8,128)(2,1)S(1)}, u32[]{:S(2)}, u32[]{:S(2)}) collective-permute-start(bf16[128,2048]{1,0:T(8,128)(2,1)S(1)} %copy-done.2), channel_id=1, source_target_pairs={{0,3},{1,0},{2,1},{3,2},{4,7},{5,4},{6,5},{7,6},{8,11},{9,8},{10,9... | collective-permute-start | bytes 1572872 | tf_op jit(solution)/shard_map/ppermute | solution.py:49
  141.9 23.4 %copy-start.3 = (bf16[128,2048]{1,0:T(8,128)(2,1)}, bf16[128,2048]{1,0:T(8,128)(2,1)S(1)}, u32[]{:S(2)}) copy-start(bf16[128,2048]{1,0:T(8,128)(2,1)S(1)} %collective-permute-done.7.refs_10_) | copy-start | bytes 1572868
  141.9 35.0 %collective-permute-start.3 = (bf16[256,2048]{1,0:T(8,128)(2,1)S(1)}, bf16[256,2048]{1,0:T(8,128)(2,1)}, u32[]{:S(2)}, u32[]{:S(2)}) collective-permute-start(bf16[256,2048]{1,0:T(8,128)(2,1)S(1)} %copy-done.1), channel_id=1, source_target_pairs={{0,3},{1,0},{2,1},{3,2},{4,7},{5,4},{6,5},{7,6},{8,11},{9,8},{10,9... | collective-permute-start | bytes 3145736 | tf_op jit(solution)/shard_map/ppermute | solution.py:49
  154.0 17.4 %collective-permute-start.10 = (bf16[128,2048]{1,0:T(8,128)(2,1)}, bf16[128,2048]{1,0:T(8,128)(2,1)}, u32[]{:S(2)}, u32[]{:S(2)}) collective-permute-start(bf16[128,2048]{1,0:T(8,128)(2,1)} %get-tuple-element.20.refs_9_), channel_id=1, source_target_pairs={{0,12},{4,0},{8,4},{12,8},{1,13},{5,1},{9,5},{13,9},{2,14},{6,2},{... | collective-permute-start | bytes 1572872 | tf_op jit(solution)/shard_map/ppermute | solution.py:49
  155.9 0.8 copy-start.5
  156.7 42.8 %collective-permute-start.4 = (bf16[256,2048]{1,0:T(8,128)(2,1)}, bf16[256,2048]{1,0:T(8,128)(2,1)}, u32[]{:S(2)}, u32[]{:S(2)}) collective-permute-start(bf16[256,2048]{1,0:T(8,128)(2,1)} %get-tuple-element.18.refs_1_), channel_id=1, source_target_pairs={{0,12},{4,0},{8,4},{12,8},{1,13},{5,1},{9,5},{13,9},{2,14},{6,2},{... | collective-permute-start | bytes 3145736 | tf_op jit(solution)/shard_map/ppermute | solution.py:49
  159.5 50.6 %collective-permute-start.5 = (bf16[256,2048]{1,0:T(8,128)(2,1)}, bf16[256,2048]{1,0:T(8,128)(2,1)}, u32[]{:S(2)}, u32[]{:S(2)}) collective-permute-start(bf16[256,2048]{1,0:T(8,128)(2,1)} %collective-permute-done.1.refs_2_), channel_id=1, source_target_pairs={{0,1},{1,2},{2,3},{3,0},{4,5},{5,6},{6,7},{7,4},{8,9},{9,10},{10,1... | collective-permute-start | bytes 3145736 | tf_op jit(solution)/shard_map/ppermute | solution.py:49
  161.4 48.7 %collective-permute-start.6 = (bf16[256,2048]{1,0:T(8,128)(2,1)}, bf16[256,2048]{1,0:T(8,128)(2,1)}, u32[]{:S(2)}, u32[]{:S(2)}) collective-permute-start(bf16[256,2048]{1,0:T(8,128)(2,1)} %collective-permute-done.2.refs_3_), channel_id=1, source_target_pairs={{0,4},{4,8},{8,12},{12,0},{1,5},{5,9},{9,13},{13,1},{2,6},{6,10},{... | collective-permute-start | bytes 3145736 | tf_op jit(solution)/shard_map/ppermute | solution.py:49
  165.4 44.8 %all-to-all-start.6 = ((bf16[16,16,2048]{2,1,0:T(8,128)(2,1)}), bf16[16,16,2048]{2,1,0:T(8,128)(2,1)S(1)}, u32[]{:S(2)}, u32[]{:S(2)}) async-start(bf16[16,16,2048]{2,1,0:T(8,128)(2,1)} %deal.1), calls=%async_computation.6 | async-start | bytes 2097152 | tf_op jit(solution)/shard_map/all_to_all | solution.py:41
  171.4 36.0 %collective-permute-start.11 = (bf16[128,2048]{1,0:T(8,128)(2,1)}, bf16[128,2048]{1,0:T(8,128)(2,1)S(1)}, u32[]{:S(2)}, u32[]{:S(2)}) collective-permute-start(bf16[128,2048]{1,0:T(8,128)(2,1)} %copy-done.3), channel_id=1, source_target_pairs={{0,1},{1,2},{2,3},{3,0},{4,5},{5,6},{6,7},{7,4},{8,9},{9,10},{10,1... | collective-permute-start | bytes 1572872 | tf_op jit(solution)/shard_map/ppermute | solution.py:49
  176.9 32.4 %collective-permute-start.12 = (bf16[128,2048]{1,0:T(8,128)(2,1)}, bf16[128,2048]{1,0:T(8,128)(2,1)S(1)}, u32[]{:S(2)}, u32[]{:S(2)}) collective-permute-start(bf16[128,2048]{1,0:T(8,128)(2,1)} %collective-permute-done.8.refs_11_), channel_id=1, source_target_pairs={{0,4},{4,8},{8,12},{12,0},{1,5},{5,9},{9,13},{13,1},{2,6},{6,10},{... | collective-permute-start | bytes 1572872 | tf_op jit(solution)/shard_map/ppermute | solution.py:49
  207.4 0.8 copy-start.7
  209.3 0.8 copy-start.9
  210.1 1.0 copy-start.4
  211.2 1.0 copy-start.6
  212.2 1.0 copy-start.8
  213.2 1.0 copy-start.10
  243.7 15.8 %copy-start.14 = (f32[16,2]{0,1:T(2,128)S(1)}, f32[16,2]{0,1:T(2,128)}, u32[]{:S(2)}) copy-start(f32[16,2]{0,1:T(2,128)} %param.22) | copy-start | bytes 388
  243.7 38.0 %all-to-all-start.8 = ((bf16[32,16,256]{2,1,0:T(8,128)(2,1)}), bf16[32,16,256]{2,1,0:T(8,128)(2,1)S(1)}, u32[]{:S(2)}, u32[]{:S(2)}) async-start(bf16[32,16,256]{2,1,0:T(8,128)(2,1)} %bitcast.16), calls=%async_computation.8 | async-start | bytes 524288 | tf_op jit(solution)/shard_map/all_to_all | solution.py:41

commit v6 on v5

--- a/solution.py
+++ b/solution.py
@@ -339,55 +339,71 @@
     return outs[:2], outs[2:]
 
 
-def experts_kernel(rows_ref, *refs):
+def experts_kernel(rows_ref, own_up_ref, own_down_ref, *refs):
     pieces, (out_ref, held, acc, sems) = refs[:-4], refs[-4:]
-    pairs = len(pieces) // 4
-    ups, downs = pieces[: 2 * pairs], pieces[2 * pairs :]
-    copies = []
-    for p in range(pairs):
+    count = len(pieces) // 2
+    ups, downs = pieces[:count], pieces[count:]
+    pairs = (count + 1) // 2
+    copies = [[[] for _ in range(3)] for _ in range(pairs)]
+    for n in range(count):
+        p, i = (n + 1) // 2, (n + 1) % 2
         for j in range(3):
-            for i in range(2):
-                source = downs[2 * p + i]
-                if j < 2:
-                    source = ups[2 * p + i].at[pl.ds(j * SHARE, SHARE)]
-                copies.append(
-                    pltpu.make_async_copy(
-                        source, held.at[p, j, pl.ds(i * SHARE, SHARE)], sems.at[p, j, i]
-                    )
-                )
-    for copy in copies[:12]:
-        copy.start()
-    across = (((1,), (1,)), ((), ()))
-    for p in range(pairs):
-        gate_up = []
-        for j in range(2):
-            for copy in copies[6 * p + 2 * j : 6 * p + 2 * j + 2]:
-                copy.wait()
-            gate_up.append(
-                lax.dot_general(
-                    rows_ref[...], held[p, j], across, preferred_element_type=F32
+            source = downs[n] if j == 2 else ups[n].at[pl.ds(j * SHARE, SHARE)]
+            copies[p][j].append(
+                pltpu.make_async_copy(
+                    source, held.at[p, j, pl.ds(i * SHARE, SHARE)], sems.at[p, j, i]
                 )
             )
-        gate, upper = gate_up
-        hidden = (gate / (1.0 + jnp.exp(-gate)) * upper).astype(BF)
-        for copy in copies[6 * p + 4 : 6 * p + 6]:
+
+    def start(p):
+        for group in copies[p] if p < pairs else []:
+            for copy in group:
+                copy.start()
+
+    def wait(p, j):
+        for copy in copies[p][j]:
             copy.wait()
-        for copy in copies[6 * (p + 2) : 6 * (p + 3)]:
-            copy.start()
+
+    def against(units):
+        return lax.dot_general(
+            rows_ref[...], units, (((1,), (1,)), ((), ())), preferred_element_type=F32
+        )
+
+    def swish(gate, upper):
+        return (gate / (1.0 + jnp.exp(-gate)) * upper).astype(BF)
+
+    start(0)
+    start(1)
+    both = against(own_up_ref[...])
+    mine = swish(both[:, :SHARE], both[:, SHARE:])
+    wait(0, 0)
+    wait(0, 1)
+    gate = against(held[0, 0, SHARE:])
+    hidden = jnp.concatenate([mine, swish(gate, against(held[0, 1, SHARE:]))], axis=1)
+    wait(0, 2)
+    start(2)
+    down = jnp.concatenate([own_down_ref[...], held[0, 2, SHARE:]], axis=0)
+    acc[...] = jnp.dot(hidden, down, preferred_element_type=F32)
+    for p in range(1, pairs):
+        wait(p, 0)
+        gate = against(held[p, 0])
+        wait(p, 1)
+        hidden = swish(gate, against(held[p, 1]))
+        wait(p, 2)
+        start(p + 2)
         part = jnp.dot(hidden, held[p, 2], preferred_element_type=F32)
-        if p == 0:
-            acc[...] = part
-        elif p < pairs - 1:
+        if p < pairs - 1:
             acc[...] += part
         else:
             out_ref[...] = (acc[...] + part).astype(BF)
 
 
-def experts(rows, pieces):
-    pairs, depth = len(pieces) // 4, rows.shape[1]
+def experts(rows, ups, downs):
+    pairs, depth = len(ups) // 2, rows.shape[1]
+    pieces = [*ups[1:], *downs[1:]]
     return pl.pallas_call(
         experts_kernel,
-        in_specs=[IN_VMEM] + [IN_HBM] * len(pieces),
+        in_specs=[IN_VMEM] * 3 + [IN_HBM] * len(pieces),
         out_specs=IN_VMEM,
         out_shape=jax.ShapeDtypeStruct(rows.shape, BF),
         scratch_shapes=[
@@ -397,7 +413,7 @@
         ],
         compiler_params=grant(EXPERT_GRANT),
         name="experts",
-    )(rows, *pieces)
+    )(rows, ups[0], downs[0], *pieces)
 
 
 def local(
@@ -437,7 +453,7 @@
         left = [ring(p, axis, 1) for p, axis in zip(packs, axes)]
         right = [ring(p, axis, -1) for p, axis in zip(packs, axes)]
         last = [ring(p, axis, 1) for p, axis in zip(left, axes)]
-        pieces += [*packs, *left, *right, *last]
+        pieces.append([*packs, *left, *right, *last])
 
     parts = attend(q8, kv_mine, kv_other)
     parts = exchange(parts, GROUP)
@@ -471,7 +487,7 @@
     arrived = exchange(sent.reshape(blocks), ("z", "c"))
 
     rows = exchange(deal(arrived.reshape(sent.shape)), TP)
-    partial = experts(rows.reshape(-1, depth), pieces)
+    partial = experts(rows.reshape(-1, depth), *pieces)
     back = exchange(partial.reshape(rows.shape), TP)
     returned = exchange(collect(back).reshape(blocks), ("z", "c"))
     return finish(mixed, returned.reshape(sent.shape), route_weights, picks)

time: 284 us -> 285 us (level)
  no operation moved by 1% of the time
where the time goes in v6:
time: 285 us; the launch traced here: 284 us
  waiting for transfers between devices  98.9 us (35%)
  starting transfers between devices  82.8 us (29%)
  blocking collectives  63.8 us (22%)
  Pallas kernels  27.4 us (10%)
  local copies, waits for them, and re-layouts  6.81 us (2%)
    all_to_all x3, blocking collectives, exchange(): return lax.all_to_all(blocks, axis, split_axis=0, concat_axis=0, tiled=True)  63.8 us
    all_to_all x6, waiting for transfers between devices, exchange(): return lax.all_to_all(blocks, axis, split_axis=0, concat_axis=0, tiled=True)  56.4 us
    all_to_all x6, starting transfers between devices, exchange(): return lax.all_to_all(blocks, axis, split_axis=0, concat_axis=0, tiled=True)  44 us
    ppermute x12, waiting for transfers between devices, ring(): return lax.ppermute(value, axis, [(i, (i + step) % 4) for i in range(4)])  41.3 us
    ppermute x12, starting transfers between devices, ring(): return lax.ppermute(value, axis, [(i, (i + step) % 4) for i in range(4)])  30.9 us
    pallas_call x1, Pallas kernels, experts(): pl.pallas_call(experts_kernel, in_specs=[IN_VMEM] * 3 + [IN_HBM] * len(pi...  9.84 us
    ppermute x1, starting transfers between devices, swap_cores(): return lax.ppermute(value, 'c', [(0, 1), (1, 0)])  7.91 us
    unnamed x31, local copies, waits for them, and re-layouts  6.64 us
  transfers between devices with their start and end apart: 19, of which 10 were waited for; matrix products, arithmetic and copies ran while one was open for 1% of the time, Pallas kernels for 3%

profile of v6, /device:TPU:1, one launch (start us, length us, event | category | flops | bytes accessed | tf_op | source)
XLA Modules:
  0.0 283.6 jit_solution(111762739505633468)
XLA Ops:
  0.0 2.3 prepare_queries.1
  2.3 5.9 %all-to-all-start = ((bf16[8,256,128]{2,1,0:T(8,128)(2,1)}), bf16[8,256,128]{2,1,0:T(8,128)(2,1)S(1)}, u32[]{:S(2)}, u32[]{:S(2)}) async-start(bf16[8,256,128]{2,1,0:T(8,128)(2,1)} %prepare_queries.1), calls=%async_computation | async-start | bytes 1048576 | tf_op jit(solution)/shard_map/all_to_all | solution.py:41
  8.8 2.3 prepare_keys.1
  11.1 4.7 %all-to-all-done.q_ref = bf16[8,256,128]{2,1,0:T(8,128)(2,1)S(1)} async-done(((bf16[8,256,128]{2,1,0:T(8,128)(2,1)}), bf16[8,256,128]{2,1,0:T(8,128)(2,1)S(1)}, u32[]{:S(2)}, u32[]{:S(2)}) %all-to-all-start) | async-done | bytes 524320 | tf_op jit(solution)/shard_map/all_to_all | solution.py:41
  15.7 31.2 %all_to_all.45 = bf16[16,32,256]{2,1,0:T(8,128)(2,1)S(1)} all-to-all(bf16[16,32,256]{2,1,0:T(8,128)(2,1)} %prepare_keys.1), channel_id=1, replica_groups=mesh['z'=16,'c'=2,'yh'=2,'yl'=2,'x'=4] {'z'}, dimensions={0} | all-to-all | bytes 524288 | tf_op jit(solution)/shard_map/all_to_all | solution.py:41
  46.9 7.9 %collective-permute-start = (bf16[512,256]{1,0:T(8,128)(2,1)S(1)}, bf16[512,256]{1,0:T(8,128)(2,1)S(1)}, u32[]{:S(2)}, u32[]{:S(2)}) collective-permute-start(bf16[512,256]{1,0:T(8,128)(2,1)S(1)} %bitcast.29), channel_id=1, source_target_pairs={{0,16},{16,0},{1,17},{17,1},{2,18},{18,2},{3,19},{19,3},{4,20},{20... | collective-permute-start | bytes 786440 | tf_op jit(solution)/shard_map/ppermute | solution.py:45
  54.8 1.1 collective-permute-done.other_ref
  55.9 3.3 %attend.1 = bf16[8,144,256]{2,1,0:T(8,128)(2,1)S(1)} custom-call(bf16[8,256,128]{2,1,0:T(8,128)(2,1)S(1)} %all-to-all-done.q_ref, bf16[512,256]{1,0:T(8,128)(2,1)S(1)} %bitcast.30, bf16[512,256]{1,0:T(8,128)(2,1)S(1)} %collective-permute-done.other_ref), custom_call_target="tpu_custom_call" | custom-call | tf_op jit(solution)/shard_map/attend/pallas_call | solution.py:152
  59.3 13.2 %all_to_all.46.parts_ref = bf16[8,144,256]{2,1,0:T(8,128)(2,1)S(1)} all-to-all(bf16[8,144,256]{2,1,0:T(8,128)(2,1)S(1)} %attend.1), channel_id=1, replica_groups=mesh['z'=16,'c'=2,'yh'=2,'yl'=2,'x'=4] {'yl','x'}, dimensions={0} | all-to-all | bytes 1179648 | tf_op jit(solution)/shard_map/all_to_all | solution.py:41
  72.4 1.2 combine.1
  73.7 4.5 %all-to-all-start.3 = ((bf16[16,128,256]{2,1,0:T(8,128)(2,1)}), bf16[16,128,256]{2,1,0:T(8,128)(2,1)}, u32[]{:S(2)}, u32[]{:S(2)}) async-start(bf16[16,128,256]{2,1,0:T(8,128)(2,1)} %combine.1), calls=%async_computation.3 | async-start | bytes 2097152 | tf_op jit(solution)/shard_map/all_to_all | solution.py:41
  78.2 4.0 %pack.1 = (bf16[256,2048]{1,0:T(8,128)(2,1)}, bf16[256,2048]{1,0:T(8,128)(2,1)}, bf16[128,2048]{1,0:T(8,128)(2,1)}, bf16[128,2048]{1,0:T(8,128)(2,1)}) custom-call(bf16[1,2048,256]{2,1,0:T(8,128)(2,1)} %gate_ref.1, bf16[1,2048,256]{2,1,0:T(8,128)(2,1)} %up_ref.1, bf16[1,256,2048]{2,1,0:T(8,128)(2,1)} %down_ref.1), custom_call_target="tpu_custom_call" | custom-call | tf_op jit(solution)/shard_map/pack/pallas_call | solution.py:331
  82.1 3.2 %collective-permute-start.1 = (bf16[256,2048]{1,0:T(8,128)(2,1)}, bf16[256,2048]{1,0:T(8,128)(2,1)}, u32[]{:S(2)}, u32[]{:S(2)}) collective-permute-start(bf16[256,2048]{1,0:T(8,128)(2,1)} %get-tuple-element.17.own_up_ref), channel_id=1, source_target_pairs={{0,1},{1,2},{2,3},{3,0},{4,5},{5,6},{6,7},{7,4},{8,9},{9,10},{10,1... | collective-permute-start | bytes 3145736 | tf_op jit(solution)/shard_map/ppermute | solution.py:49
  85.3 3.1 %collective-permute-start.2 = (bf16[256,2048]{1,0:T(8,128)(2,1)}, bf16[256,2048]{1,0:T(8,128)(2,1)}, u32[]{:S(2)}, u32[]{:S(2)}) collective-permute-start(bf16[256,2048]{1,0:T(8,128)(2,1)} %get-tuple-element.19.refs_0_), channel_id=1, source_target_pairs={{0,4},{4,8},{8,12},{12,0},{1,5},{5,9},{9,13},{13,1},{2,6},{6,10},{... | collective-permute-start | bytes 3145736 | tf_op jit(solution)/shard_map/ppermute | solution.py:49
  88.4 3.1 %collective-permute-start.7 = (bf16[128,2048]{1,0:T(8,128)(2,1)}, bf16[128,2048]{1,0:T(8,128)(2,1)S(1)}, u32[]{:S(2)}, u32[]{:S(2)}) collective-permute-start(bf16[128,2048]{1,0:T(8,128)(2,1)} %get-tuple-element.18.own_down_ref), channel_id=1, source_target_pairs={{0,1},{1,2},{2,3},{3,0},{4,5},{5,6},{6,7},{7,4},{8,9},{9,10},{10,1... | collective-permute-start | bytes 1572872 | tf_op jit(solution)/shard_map/ppermute | solution.py:49
  92.0 1.6 all-to-all-done.3
  93.6 2.4 convolution_convert_fusion
  96.1 4.7 %all-to-all-start.4 = ((bf16[16,16,128]{2,1,0:T(8,128)(2,1)}), bf16[16,16,128]{2,1,0:T(8,128)(2,1)S(1)}, u32[]{:S(2)}, u32[]{:S(2)}) async-start(bf16[16,16,128]{2,1,0:T(8,128)(2,1)} %bitcast.8), calls=%async_computation.4 | async-start | bytes 131072 | tf_op jit(solution)/shard_map/all_to_all | solution.py:41
  101.0 28.2 %all-to-all-done.4.projected_ref = bf16[16,16,128]{2,1,0:T(8,128)(2,1)S(1)} async-done(((bf16[16,16,128]{2,1,0:T(8,128)(2,1)}), bf16[16,16,128]{2,1,0:T(8,128)(2,1)S(1)}, u32[]{:S(2)}, u32[]{:S(2)}) %all-to-all-start.4) | async-done | bytes 65568 | tf_op jit(solution)/shard_map/all_to_all | solution.py:41
  129.2 1.0 mix.1
  130.2 7.1 %all-to-all-start.5 = ((bf16[32,16,256]{2,1,0:T(8,128)(2,1)}), bf16[32,16,256]{2,1,0:T(8,128)(2,1)S(1)}, u32[]{:S(2)}, u32[]{:S(2)}) async-start(bf16[32,16,256]{2,1,0:T(8,128)(2,1)} %bitcast.12), calls=%async_computation.5 | async-start | bytes 524288 | tf_op jit(solution)/shard_map/all_to_all | solution.py:41
  137.3 2.2 collective-permute-start.8
  139.5 2.4 collective-permute-start.9
  141.9 2.2 collective-permute-start.3
  144.1 9.8 %collective-permute-done.8.refs_9_ = bf16[128,2048]{1,0:T(8,128)(2,1)} collective-permute-done((bf16[128,2048]{1,0:T(8,128)(2,1)}, bf16[128,2048]{1,0:T(8,128)(2,1)}, u32[]{:S(2)}, u32[]{:S(2)}) %collective-permute-start.8) | collective-permute-done | bytes 524320 | tf_op jit(solution)/shard_map/ppermute | solution.py:49
  154.0 1.9 collective-permute-start.10
  155.9 0.8 copy-done.5
  156.7 2.8 collective-permute-start.4
  159.5 1.9 collective-permute-start.5
  161.4 2.5 collective-permute-start.6
  164.0 1.4 deal.1
  165.4 6.0 %all-to-all-start.6 = ((bf16[16,16,2048]{2,1,0:T(8,128)(2,1)}), bf16[16,16,2048]{2,1,0:T(8,128)(2,1)S(1)}, u32[]{:S(2)}, u32[]{:S(2)}) async-start(bf16[16,16,2048]{2,1,0:T(8,128)(2,1)} %deal.1), calls=%async_computation.6 | async-start | bytes 2097152 | tf_op jit(solution)/shard_map/all_to_all | solution.py:41
  171.4 3.3 %collective-permute-start.11 = (bf16[128,2048]{1,0:T(8,128)(2,1)}, bf16[128,2048]{1,0:T(8,128)(2,1)S(1)}, u32[]{:S(2)}, u32[]{:S(2)}) collective-permute-start(bf16[128,2048]{1,0:T(8,128)(2,1)} %copy-done.3), channel_id=1, source_target_pairs={{0,1},{1,2},{2,3},{3,0},{4,5},{5,6},{6,7},{7,4},{8,9},{9,10},{10,1... | collective-permute-start | bytes 1572872 | tf_op jit(solution)/shard_map/ppermute | solution.py:49
  174.7 2.2 collective-permute-done.3.refs_3_
  176.9 2.4 collective-permute-start.12
  179.3 20.1 %collective-permute-done.4.refs_4_ = bf16[256,2048]{1,0:T(8,128)(2,1)} collective-permute-done((bf16[256,2048]{1,0:T(8,128)(2,1)}, bf16[256,2048]{1,0:T(8,128)(2,1)}, u32[]{:S(2)}, u32[]{:S(2)}) %collective-permute-start.4) | collective-permute-done | bytes 1048608 | tf_op jit(solution)/shard_map/ppermute | solution.py:49
  199.5 7.9 %collective-permute-done.11.refs_12_ = bf16[128,2048]{1,0:T(8,128)(2,1)S(1)} collective-permute-done((bf16[128,2048]{1,0:T(8,128)(2,1)}, bf16[128,2048]{1,0:T(8,128)(2,1)S(1)}, u32[]{:S(2)}, u32[]{:S(2)}) %collective-permute-start.11) | collective-permute-done | bytes 524320 | tf_op jit(solution)/shard_map/ppermute | solution.py:49
  208.2 1.2 collective-permute-done.12.refs_13_
  210.1 1.0 copy-done.4
  211.2 1.0 copy-done.6
  212.2 1.0 copy-done.8
  213.2 1.0 copy-done.10
  214.3 9.8 %experts.1 = bf16[256,2048]{1,0:T(8,128)(2,1)S(1)} custom-call(bf16[256,2048]{1,0:T(8,128)(2,1)S(1)} %bitcast.26, bf16[256,2048]{1,0:T(8,128)(2,1)S(1)} %copy-done.1, bf16[128,2048]{1,0:T(8,128)(2,1)S(1)} %copy-done.2, bf16[256,2048]{1,0:T(8,128)(2,1)} %get-tuple-element.19.refs_0_, bf16[256,2048]{1,0:T(8,128)(2,1)} %collective-permute-done.1.refs_1_, ...), custom_call_target="tpu_custom_call" | custom-call | tf_op jit(solution)/shard_map/experts/pallas_call | solution.py:404
  224.1 19.4 %all_to_all.47.back_ref = bf16[16,16,2048]{2,1,0:T(8,128)(2,1)S(1)} all-to-all(bf16[16,16,2048]{2,1,0:T(8,128)(2,1)S(1)} %bitcast.27), channel_id=1, replica_groups=mesh['z'=16,'c'=2,'yh'=2,'yl'=2,'x'=4] {'yh','yl','x'}, dimensions={0} | all-to-all | bytes 2097152 | tf_op jit(solution)/shard_map/all_to_all | solution.py:41
  243.6 1.1 collect.1
  244.7 15.8 %all-to-all-start.8 = ((bf16[32,16,256]{2,1,0:T(8,128)(2,1)}), bf16[32,16,256]{2,1,0:T(8,128)(2,1)S(1)}, u32[]{:S(2)}, u32[]{:S(2)}) async-start(bf16[32,16,256]{2,1,0:T(8,128)(2,1)} %bitcast.16), calls=%async_computation.8 | async-start | bytes 524288 | tf_op jit(solution)/shard_map/all_to_all | solution.py:41
  260.7 22.0 %all-to-all-done.8 = bf16[32,16,256]{2,1,0:T(8,128)(2,1)S(1)} async-done(((bf16[32,16,256]{2,1,0:T(8,128)(2,1)}), bf16[32,16,256]{2,1,0:T(8,128)(2,1)S(1)}, u32[]{:S(2)}, u32[]{:S(2)}) %all-to-all-start.8) | async-done | bytes 262176 | tf_op jit(solution)/shard_map/all_to_all | solution.py:41
  282.7 0.9 finish.1
  (47 shorter events, 3.1 us)
Async XLA Ops:
  0.0 93.6 %copy-start = (bf16[2048,128]{1,0:T(8,128)(2,1)S(1)}, bf16[2048,128]{1,0:T(8,128)(2,1)}, u32[]{:S(2)}) copy-start(bf16[2048,128]{1,0:T(8,128)(2,1)} %param.18) | copy-start | bytes 1572868
  2.3 13.4 %all-to-all-start = ((bf16[8,256,128]{2,1,0:T(8,128)(2,1)}), bf16[8,256,128]{2,1,0:T(8,128)(2,1)S(1)}, u32[]{:S(2)}, u32[]{:S(2)}) async-start(bf16[8,256,128]{2,1,0:T(8,128)(2,1)} %prepare_queries.1), calls=%async_computation | async-start | bytes 1048576 | tf_op jit(solution)/shard_map/all_to_all | solution.py:41
  46.9 9.1 %collective-permute-start = (bf16[512,256]{1,0:T(8,128)(2,1)S(1)}, bf16[512,256]{1,0:T(8,128)(2,1)S(1)}, u32[]{:S(2)}, u32[]{:S(2)}) collective-permute-start(bf16[512,256]{1,0:T(8,128)(2,1)S(1)} %bitcast.29), channel_id=1, source_target_pairs={{0,16},{16,0},{1,17},{17,1},{2,18},{18,2},{3,19},{19,3},{4,20},{20... | collective-permute-start | bytes 786440 | tf_op jit(solution)/shard_map/ppermute | solution.py:45
  73.7 20.0 %all-to-all-start.3 = ((bf16[16,128,256]{2,1,0:T(8,128)(2,1)}), bf16[16,128,256]{2,1,0:T(8,128)(2,1)}, u32[]{:S(2)}, u32[]{:S(2)}) async-start(bf16[16,128,256]{2,1,0:T(8,128)(2,1)} %combine.1), calls=%async_computation.3 | async-start | bytes 2097152 | tf_op jit(solution)/shard_map/all_to_all | solution.py:41
  82.1 77.4 %collective-permute-start.1 = (bf16[256,2048]{1,0:T(8,128)(2,1)}, bf16[256,2048]{1,0:T(8,128)(2,1)}, u32[]{:S(2)}, u32[]{:S(2)}) collective-permute-start(bf16[256,2048]{1,0:T(8,128)(2,1)} %get-tuple-element.17.own_up_ref), channel_id=1, source_target_pairs={{0,1},{1,2},{2,3},{3,0},{4,5},{5,6},{6,7},{7,4},{8,9},{9,10},{10,1... | collective-permute-start | bytes 3145736 | tf_op jit(solution)/shard_map/ppermute | solution.py:49
  85.3 6.2 %copy-start.13 = (s32[16,2]{0,1:T(2,128)S(1)}, s32[16,2]{0,1:T(2,128)}, u32[]{:S(2)}) copy-start(s32[16,2]{0,1:T(2,128)} %param.21) | copy-start | bytes 388
  85.3 76.1 %collective-permute-start.2 = (bf16[256,2048]{1,0:T(8,128)(2,1)}, bf16[256,2048]{1,0:T(8,128)(2,1)}, u32[]{:S(2)}, u32[]{:S(2)}) collective-permute-start(bf16[256,2048]{1,0:T(8,128)(2,1)} %get-tuple-element.19.refs_0_), channel_id=1, source_target_pairs={{0,4},{4,8},{8,12},{12,0},{1,5},{5,9},{9,13},{13,1},{2,6},{6,10},{... | collective-permute-start | bytes 3145736 | tf_op jit(solution)/shard_map/ppermute | solution.py:49
  88.4 53.4 %collective-permute-start.7 = (bf16[128,2048]{1,0:T(8,128)(2,1)}, bf16[128,2048]{1,0:T(8,128)(2,1)S(1)}, u32[]{:S(2)}, u32[]{:S(2)}) collective-permute-start(bf16[128,2048]{1,0:T(8,128)(2,1)} %get-tuple-element.18.own_down_ref), channel_id=1, source_target_pairs={{0,1},{1,2},{2,3},{3,0},{4,5},{5,6},{6,7},{7,4},{8,9},{9,10},{10,1... | collective-permute-start | bytes 1572872 | tf_op jit(solution)/shard_map/ppermute | solution.py:49
  93.6 35.5 %copy-start.11 = (bf16[16,2048]{1,0:T(8,128)(2,1)S(1)}, bf16[16,2048]{1,0:T(8,128)(2,1)}, u32[]{:S(2)}) copy-start(bf16[16,2048]{1,0:T(8,128)(2,1)} %residual_ref.1) | copy-start | bytes 196612
  93.6 35.5 %copy-start.12 = (f32[2048]{0:T(1024)S(1)}, f32[2048]{0:T(1024)}, u32[]{:S(2)}) copy-start(f32[2048]{0:T(1024)} %param.19) | copy-start | bytes 24580
  93.6 48.3 %copy-start.1 = (bf16[256,2048]{1,0:T(8,128)(2,1)S(1)}, bf16[256,2048]{1,0:T(8,128)(2,1)}, u32[]{:S(2)}) copy-start(bf16[256,2048]{1,0:T(8,128)(2,1)} %get-tuple-element.17.own_up_ref) | copy-start | bytes 3145732
  96.0 43.4 %copy-start.2 = (bf16[128,2048]{1,0:T(8,128)(2,1)S(1)}, bf16[128,2048]{1,0:T(8,128)(2,1)}, u32[]{:S(2)}) copy-start(bf16[128,2048]{1,0:T(8,128)(2,1)} %get-tuple-element.18.own_down_ref) | copy-start | bytes 1572868
  96.1 33.1 %all-to-all-start.4 = ((bf16[16,16,128]{2,1,0:T(8,128)(2,1)}), bf16[16,16,128]{2,1,0:T(8,128)(2,1)S(1)}, u32[]{:S(2)}, u32[]{:S(2)}) async-start(bf16[16,16,128]{2,1,0:T(8,128)(2,1)} %bitcast.8), calls=%async_computation.4 | async-start | bytes 131072 | tf_op jit(solution)/shard_map/all_to_all | solution.py:41
  130.2 33.8 %all-to-all-start.5 = ((bf16[32,16,256]{2,1,0:T(8,128)(2,1)}), bf16[32,16,256]{2,1,0:T(8,128)(2,1)S(1)}, u32[]{:S(2)}, u32[]{:S(2)}) async-start(bf16[32,16,256]{2,1,0:T(8,128)(2,1)} %bitcast.12), calls=%async_computation.5 | async-start | bytes 524288 | tf_op jit(solution)/shard_map/all_to_all | solution.py:41
  137.3 16.7 %collective-permute-start.8 = (bf16[128,2048]{1,0:T(8,128)(2,1)}, bf16[128,2048]{1,0:T(8,128)(2,1)}, u32[]{:S(2)}, u32[]{:S(2)}) collective-permute-start(bf16[128,2048]{1,0:T(8,128)(2,1)} %get-tuple-element.20.refs_7_), channel_id=1, source_target_pairs={{0,4},{4,8},{8,12},{12,0},{1,5},{5,9},{9,13},{13,1},{2,6},{6,10},{... | collective-permute-start | bytes 1572872 | tf_op jit(solution)/shard_map/ppermute | solution.py:49
  139.5 16.4 %collective-permute-start.9 = (bf16[128,2048]{1,0:T(8,128)(2,1)S(1)}, bf16[128,2048]{1,0:T(8,128)(2,1)S(1)}, u32[]{:S(2)}, u32[]{:S(2)}) collective-permute-start(bf16[128,2048]{1,0:T(8,128)(2,1)S(1)} %copy-done.2), channel_id=1, source_target_pairs={{0,3},{1,0},{2,1},{3,2},{4,7},{5,4},{6,5},{7,6},{8,11},{9,8},{10,9... | collective-permute-start | bytes 1572872 | tf_op jit(solution)/shard_map/ppermute | solution.py:49
  141.9 23.4 %copy-start.3 = (bf16[128,2048]{1,0:T(8,128)(2,1)}, bf16[128,2048]{1,0:T(8,128)(2,1)S(1)}, u32[]{:S(2)}) copy-start(bf16[128,2048]{1,0:T(8,128)(2,1)S(1)} %collective-permute-done.7.refs_8_) | copy-start | bytes 1572868
  141.9 35.0 %collective-permute-start.3 = (bf16[256,2048]{1,0:T(8,128)(2,1)S(1)}, bf16[256,2048]{1,0:T(8,128)(2,1)}, u32[]{:S(2)}, u32[]{:S(2)}) collective-permute-start(bf16[256,2048]{1,0:T(8,128)(2,1)S(1)} %copy-done.1), channel_id=1, source_target_pairs={{0,3},{1,0},{2,1},{3,2},{4,7},{5,4},{6,5},{7,6},{8,11},{9,8},{10,9... | collective-permute-start | bytes 3145736 | tf_op jit(solution)/shard_map/ppermute | solution.py:49
  154.0 17.4 %collective-permute-start.10 = (bf16[128,2048]{1,0:T(8,128)(2,1)}, bf16[128,2048]{1,0:T(8,128)(2,1)}, u32[]{:S(2)}, u32[]{:S(2)}) collective-permute-start(bf16[128,2048]{1,0:T(8,128)(2,1)} %get-tuple-element.20.refs_7_), channel_id=1, source_target_pairs={{0,12},{4,0},{8,4},{12,8},{1,13},{5,1},{9,5},{13,9},{2,14},{6,2},{... | collective-permute-start | bytes 1572872 | tf_op jit(solution)/shard_map/ppermute | solution.py:49
  155.9 0.8 copy-start.5
  156.7 42.8 %collective-permute-start.4 = (bf16[256,2048]{1,0:T(8,128)(2,1)}, bf16[256,2048]{1,0:T(8,128)(2,1)}, u32[]{:S(2)}, u32[]{:S(2)}) collective-permute-start(bf16[256,2048]{1,0:T(8,128)(2,1)} %get-tuple-element.19.refs_0_), channel_id=1, source_target_pairs={{0,12},{4,0},{8,4},{12,8},{1,13},{5,1},{9,5},{13,9},{2,14},{6,2},{... | collective-permute-start | bytes 3145736 | tf_op jit(solution)/shard_map/ppermute | solution.py:49
  159.5 50.6 %collective-permute-start.5 = (bf16[256,2048]{1,0:T(8,128)(2,1)}, bf16[256,2048]{1,0:T(8,128)(2,1)}, u32[]{:S(2)}, u32[]{:S(2)}) collective-permute-start(bf16[256,2048]{1,0:T(8,128)(2,1)} %collective-permute-done.1.refs_1_), channel_id=1, source_target_pairs={{0,1},{1,2},{2,3},{3,0},{4,5},{5,6},{6,7},{7,4},{8,9},{9,10},{10,1... | collective-permute-start | bytes 3145736 | tf_op jit(solution)/shard_map/ppermute | solution.py:49
  161.4 48.7 %collective-permute-start.6 = (bf16[256,2048]{1,0:T(8,128)(2,1)}, bf16[256,2048]{1,0:T(8,128)(2,1)}, u32[]{:S(2)}, u32[]{:S(2)}) collective-permute-start(bf16[256,2048]{1,0:T(8,128)(2,1)} %collective-permute-done.2.refs_2_), channel_id=1, source_target_pairs={{0,4},{4,8},{8,12},{12,0},{1,5},{5,9},{9,13},{13,1},{2,6},{6,10},{... | collective-permute-start | bytes 3145736 | tf_op jit(solution)/shard_map/ppermute | solution.py:49
  165.4 44.8 %all-to-all-start.6 = ((bf16[16,16,2048]{2,1,0:T(8,128)(2,1)}), bf16[16,16,2048]{2,1,0:T(8,128)(2,1)S(1)}, u32[]{:S(2)}, u32[]{:S(2)}) async-start(bf16[16,16,2048]{2,1,0:T(8,128)(2,1)} %deal.1), calls=%async_computation.6 | async-start | bytes 2097152 | tf_op jit(solution)/shard_map/all_to_all | solution.py:41
  171.4 36.0 %collective-permute-start.11 = (bf16[128,2048]{1,0:T(8,128)(2,1)}, bf16[128,2048]{1,0:T(8,128)(2,1)S(1)}, u32[]{:S(2)}, u32[]{:S(2)}) collective-permute-start(bf16[128,2048]{1,0:T(8,128)(2,1)} %copy-done.3), channel_id=1, source_target_pairs={{0,1},{1,2},{2,3},{3,0},{4,5},{5,6},{6,7},{7,4},{8,9},{9,10},{10,1... | collective-permute-start | bytes 1572872 | tf_op jit(solution)/shard_map/ppermute | solution.py:49
  176.9 32.4 %collective-permute-start.12 = (bf16[128,2048]{1,0:T(8,128)(2,1)}, bf16[128,2048]{1,0:T(8,128)(2,1)S(1)}, u32[]{:S(2)}, u32[]{:S(2)}) collective-permute-start(bf16[128,2048]{1,0:T(8,128)(2,1)} %collective-permute-done.8.refs_9_), channel_id=1, source_target_pairs={{0,4},{4,8},{8,12},{12,0},{1,5},{5,9},{9,13},{13,1},{2,6},{6,10},{... | collective-permute-start | bytes 1572872 | tf_op jit(solution)/shard_map/ppermute | solution.py:49
  207.4 0.8 copy-start.7
  209.3 0.8 copy-start.9
  210.1 1.0 copy-start.4
  211.2 1.0 copy-start.6
  212.2 1.0 copy-start.8
  213.2 1.0 copy-start.10
  244.7 15.8 %copy-start.14 = (f32[16,2]{0,1:T(2,128)S(1)}, f32[16,2]{0,1:T(2,128)}, u32[]{:S(2)}) copy-start(f32[16,2]{0,1:T(2,128)} %param.22) | copy-start | bytes 388
  244.7 38.0 %all-to-all-start.8 = ((bf16[32,16,256]{2,1,0:T(8,128)(2,1)}), bf16[32,16,256]{2,1,0:T(8,128)(2,1)S(1)}, u32[]{:S(2)}, u32[]{:S(2)}) async-start(bf16[32,16,256]{2,1,0:T(8,128)(2,1)} %bitcast.16), calls=%async_computation.8 | async-start | bytes 524288 | tf_op jit(solution)/shard_map/all_to_all | solution.py:41

commit v7 on v5

--- a/solution.py
+++ b/solution.py
@@ -173,12 +173,23 @@
         top = jnp.maximum(top, tops[j])
     shares = [totals[j] * jnp.exp2(tops[j] - top) for j in range(count)]
     whole = sum(shares[1:], shares[0])
-    acc = jnp.zeros(out_ref.shape[1:], F32)
+    acc = jnp.zeros((width, parts_ref.shape[2]), F32)
     for j in range(count):
         acc = acc + parts_ref[j, :width, :].astype(F32) * (shares[j] / whole)
     done = acc.astype(BF)
+    part = done.shape[1] // (NYH * NYL)
+    halves = [
+        jnp.concatenate(
+            [
+                done[:, (NYL * i + k) * part : (NYL * i + k + 1) * part]
+                for i in range(NYH)
+            ],
+            axis=1,
+        )
+        for k in range(NYL)
+    ]
     for i in range(out_ref.shape[0]):
-        out_ref[i] = done
+        out_ref[i] = halves[i // NX % NYL]
 
 
 def combine(parts):
@@ -187,7 +198,7 @@
         combine_kernel,
         in_specs=[IN_VMEM],
         out_specs=IN_VMEM,
-        out_shape=jax.ShapeDtypeStruct((NT, width, parts.shape[2]), BF),
+        out_shape=jax.ShapeDtypeStruct((NT, width, parts.shape[2] // NYL), BF),
         compiler_params=grant(16),
         name="combine",
     )(parts)
@@ -207,8 +218,15 @@
 
 
 def mix_kernel(projected_ref, residual_ref, scale_ref, selector_ref, mixed_ref, sent_ref):
+    width = projected_ref.shape[2] // NYL
     projected = jnp.concatenate(
-        [projected_ref[i].astype(F32) for i in range(projected_ref.shape[0])], axis=1
+        [
+            projected_ref[NX * h + i, :, k * width : (k + 1) * width].astype(F32)
+            for h in range(NYH)
+            for k in range(NYL)
+            for i in range(NX)
+        ],
+        axis=1,
     )
     mixed = (residual_ref[...].astype(F32) + projected).astype(BF)
     mixed_ref[...] = mixed
@@ -425,6 +443,7 @@
 
     q8 = prepare_queries(queries, query_gain, start)
     q8 = exchange(q8, GROUP)
+    out_proj_other = lax.ppermute(out_proj, "yl", [(0, 1), (1, 0)])
     kv = prepare_keys(keys, values, key_gain, yl * NX + x, yh, start)
     q8, kv = lax.optimization_barrier((q8, kv))
     kv_mine = exchange(kv, "z").reshape(-1, 2 * width)
@@ -441,11 +460,18 @@
 
     parts = attend(q8, kv_mine, kv_other)
     parts = exchange(parts, GROUP)
-    attn_all = exchange(combine(parts), TP).reshape(NT * width, tok_sp)
-    columns = lax.dot_general(
-        attn_all, out_proj, (((0,), (0,)), ((), ())), preferred_element_type=F32
-    ).astype(BF)
-    projected = exchange(columns.reshape(NT, tok_dev, -1), TP)
+    attn_all = exchange(combine(parts), TP).reshape(NT * width, -1)
+
+    def project(columns):
+        return lax.dot_general(
+            attn_all, columns, (((0,), (0,)), ((), ())), preferred_element_type=F32
+        ).astype(BF)
+
+    mine, other = project(out_proj), project(out_proj_other)
+    columns = jnp.concatenate(
+        [jnp.where(yl == 0, mine, other), jnp.where(yl == 0, other, mine)], axis=1
+    )
+    projected = exchange(columns.reshape(NYH * NX, tok_dev, -1), ("yh", "x"))
 
     cap = max(2, 2 * tok_dev * top // (NZ * NC))
     tok = jnp.arange(tok_dev, dtype=jnp.int32)

time: 284 us -> 285 us (level)
  blocking collectives: 63.8 us -> 50 us
  starting transfers between devices: 82.8 us -> 90.6 us
  waiting for transfers between devices: 98.9 us -> 106 us
    all_to_all x3 -> x2, blocking collectives: 63.8 us -> 50 us  [exchange(): return lax.all_to_all(blocks, axis, split_axis=0, concat_axis=0, tiled=True)]
    all_to_all x6 -> x7, waiting for transfers between devices: 56.4 us -> 64 us  [exchange(): return lax.all_to_all(blocks, axis, split_axis=0, concat_axis=0, tiled=True)]
    all_to_all x6 -> x7, starting transfers between devices: 44 us -> 49.1 us  [exchange(): return lax.all_to_all(blocks, axis, split_axis=0, concat_axis=0, tiled=True)]
    ppermute x0 -> x1, starting transfers between devices: none -> 3.27 us  [local(): out_proj_other = lax.ppermute(out_proj, 'yl', [(0, 1), (1, 0)])]
    unnamed x31 -> x33, local copies, waits for them, and re-layouts: 6.64 us -> 6.68 us
  transfers between devices with their start and end apart: 19 -> 21, of which waited for: 10 -> 10; matrix products, arithmetic and copies ran while one was open for 1% -> 1% of each run, Pallas kernels for 3% -> 3%
where the time goes in v7:
time: 285 us; the launch traced here: 283 us
  waiting for transfers between devices  106 us (37%)
  starting transfers between devices  90.6 us (32%)
  blocking collectives  50 us (18%)
  Pallas kernels  26.9 us (9%)
  local copies, waits for them, and re-layouts  7.59 us (3%)
    all_to_all x7, waiting for transfers between devices, exchange(): return lax.all_to_all(blocks, axis, split_axis=0, concat_axis=0, tiled=True)  64 us
    all_to_all x2, blocking collectives, exchange(): return lax.all_to_all(blocks, axis, split_axis=0, concat_axis=0, tiled=True)  50 us
    all_to_all x7, starting transfers between devices, exchange(): return lax.all_to_all(blocks, axis, split_axis=0, concat_axis=0, tiled=True)  49.1 us
    ppermute x12, waiting for transfers between devices, ring(): return lax.ppermute(value, axis, [(i, (i + step) % 4) for i in range(4)])  40.7 us
    ppermute x12, starting transfers between devices, ring(): return lax.ppermute(value, axis, [(i, (i + step) % 4) for i in range(4)])  30.3 us
    pallas_call x1, Pallas kernels, experts(): pl.pallas_call(experts_kernel, in_specs=[IN_VMEM] + [IN_HBM] * len(pieces...  8.83 us
    ppermute x1, starting transfers between devices, swap_cores(): return lax.ppermute(value, 'c', [(0, 1), (1, 0)])  7.91 us
    unnamed x33, local copies, waits for them, and re-layouts  6.68 us
  transfers between devices with their start and end apart: 21, of which 10 were waited for; matrix products, arithmetic and copies ran while one was open for 1% of the time, Pallas kernels for 3%

profile of v7, /device:TPU:1, one launch (start us, length us, event | category | flops | bytes accessed | tf_op | source)
XLA Modules:
  0.0 283.4 jit_solution(6213991088925856452)
XLA Ops:
  0.0 2.3 prepare_queries.1
  2.3 5.9 %all-to-all-start = ((bf16[8,256,128]{2,1,0:T(8,128)(2,1)}), bf16[8,256,128]{2,1,0:T(8,128)(2,1)S(1)}, u32[]{:S(2)}, u32[]{:S(2)}) async-start(bf16[8,256,128]{2,1,0:T(8,128)(2,1)} %prepare_queries.1), calls=%async_computation | async-start | bytes 1048576 | tf_op jit(solution)/shard_map/all_to_all | solution.py:41
  8.8 2.3 prepare_keys.1
  11.1 4.6 %all-to-all-done.q_ref = bf16[8,256,128]{2,1,0:T(8,128)(2,1)S(1)} async-done(((bf16[8,256,128]{2,1,0:T(8,128)(2,1)}), bf16[8,256,128]{2,1,0:T(8,128)(2,1)S(1)}, u32[]{:S(2)}, u32[]{:S(2)}) %all-to-all-start) | async-done | bytes 524320 | tf_op jit(solution)/shard_map/all_to_all | solution.py:41
  15.7 31.2 %all_to_all.45 = bf16[16,32,256]{2,1,0:T(8,128)(2,1)S(1)} all-to-all(bf16[16,32,256]{2,1,0:T(8,128)(2,1)} %prepare_keys.1), channel_id=1, replica_groups=mesh['z'=16,'c'=2,'yh'=2,'yl'=2,'x'=4] {'z'}, dimensions={0} | all-to-all | bytes 524288 | tf_op jit(solution)/shard_map/all_to_all | solution.py:41
  46.8 7.9 %collective-permute-start = (bf16[512,256]{1,0:T(8,128)(2,1)S(1)}, bf16[512,256]{1,0:T(8,128)(2,1)S(1)}, u32[]{:S(2)}, u32[]{:S(2)}) collective-permute-start(bf16[512,256]{1,0:T(8,128)(2,1)S(1)} %bitcast.31), channel_id=1, source_target_pairs={{0,16},{16,0},{1,17},{17,1},{2,18},{18,2},{3,19},{19,3},{4,20},{20... | collective-permute-start | bytes 786440 | tf_op jit(solution)/shard_map/ppermute | solution.py:45
  54.8 1.1 collective-permute-done.other_ref
  55.9 4.1 %attend.1 = bf16[8,144,256]{2,1,0:T(8,128)(2,1)} custom-call(bf16[8,256,128]{2,1,0:T(8,128)(2,1)S(1)} %all-to-all-done.q_ref, bf16[512,256]{1,0:T(8,128)(2,1)S(1)} %bitcast.32, bf16[512,256]{1,0:T(8,128)(2,1)S(1)} %collective-permute-done.other_ref), custom_call_target="tpu_custom_call" | custom-call | tf_op jit(solution)/shard_map/attend/pallas_call | solution.py:152
  60.0 3.7 %all-to-all-start.2 = ((bf16[8,144,256]{2,1,0:T(8,128)(2,1)}), bf16[8,144,256]{2,1,0:T(8,128)(2,1)S(1)}, u32[]{:S(2)}, u32[]{:S(2)}) async-start(bf16[8,144,256]{2,1,0:T(8,128)(2,1)} %attend.1), calls=%async_computation.2 | async-start | bytes 1179648 | tf_op jit(solution)/shard_map/all_to_all | solution.py:41
  63.7 3.3 %collective-permute-start.1 = (bf16[2048,128]{1,0:T(8,128)(2,1)S(1)}, bf16[2048,128]{1,0:T(8,128)(2,1)S(1)}, u32[]{:S(2)}, u32[]{:S(2)}) collective-permute-start(bf16[2048,128]{1,0:T(8,128)(2,1)S(1)} %copy-done.13), channel_id=1, source_target_pairs={{0,4},{4,0},{1,5},{5,1},{2,6},{6,2},{3,7},{7,3},{8,12},{12,8},{9,1... | collective-permute-start | bytes 1572872 | tf_op jit(solution)/shard_map/ppermute | solution.py:446
  67.0 3.9 %pack.1 = (bf16[256,2048]{1,0:T(8,128)(2,1)}, bf16[256,2048]{1,0:T(8,128)(2,1)}, bf16[128,2048]{1,0:T(8,128)(2,1)}, bf16[128,2048]{1,0:T(8,128)(2,1)}) custom-call(bf16[1,2048,256]{2,1,0:T(8,128)(2,1)} %gate_ref.1, bf16[1,2048,256]{2,1,0:T(8,128)(2,1)} %up_ref.1, bf16[1,256,2048]{2,1,0:T(8,128)(2,1)} %down_ref.1), custom_call_target="tpu_custom_call" | custom-call | tf_op jit(solution)/shard_map/pack/pallas_call | solution.py:349
  70.9 3.1 %collective-permute-start.2 = (bf16[256,2048]{1,0:T(8,128)(2,1)}, bf16[256,2048]{1,0:T(8,128)(2,1)}, u32[]{:S(2)}, u32[]{:S(2)}) collective-permute-start(bf16[256,2048]{1,0:T(8,128)(2,1)} %get-tuple-element.17.refs_0_), channel_id=1, source_target_pairs={{0,1},{1,2},{2,3},{3,0},{4,5},{5,6},{6,7},{7,4},{8,9},{9,10},{10,1... | collective-permute-start | bytes 3145736 | tf_op jit(solution)/shard_map/ppermute | solution.py:49
  74.0 2.2 collective-permute-start.3
  76.2 3.1 %collective-permute-start.8 = (bf16[128,2048]{1,0:T(8,128)(2,1)}, bf16[128,2048]{1,0:T(8,128)(2,1)}, u32[]{:S(2)}, u32[]{:S(2)}) collective-permute-start(bf16[128,2048]{1,0:T(8,128)(2,1)} %get-tuple-element.19.refs_8_), channel_id=1, source_target_pairs={{0,1},{1,2},{2,3},{3,0},{4,5},{5,6},{6,7},{7,4},{8,9},{9,10},{10,1... | collective-permute-start | bytes 1572872 | tf_op jit(solution)/shard_map/ppermute | solution.py:49
  79.3 1.0 combine.1
  80.4 5.2 %all-to-all-start.3 = ((bf16[16,128,128]{2,1,0:T(8,128)(2,1)}), bf16[16,128,128]{2,1,0:T(8,128)(2,1)S(1)}, u32[]{:S(2)}, u32[]{:S(2)}) async-start(bf16[16,128,128]{2,1,0:T(8,128)(2,1)} %combine.1), calls=%async_computation.3 | async-start | bytes 1048576 | tf_op jit(solution)/shard_map/all_to_all | solution.py:41
  86.0 31.0 %all-to-all-done.3 = bf16[16,128,128]{2,1,0:T(8,128)(2,1)S(1)} async-done(((bf16[16,128,128]{2,1,0:T(8,128)(2,1)}), bf16[16,128,128]{2,1,0:T(8,128)(2,1)S(1)}, u32[]{:S(2)}, u32[]{:S(2)}) %all-to-all-start.3) | async-done | bytes 524320 | tf_op jit(solution)/shard_map/all_to_all | solution.py:41
  118.5 3.5 %all-to-all-start.4 = ((bf16[8,16,256]{2,1,0:T(8,128)(2,1)}), bf16[8,16,256]{2,1,0:T(8,128)(2,1)S(1)}, u32[]{:S(2)}, u32[]{:S(2)}) async-start(bf16[8,16,256]{2,1,0:T(8,128)(2,1)} %bitcast.8), calls=%async_computation.4 | async-start | bytes 131072 | tf_op jit(solution)/shard_map/all_to_all | solution.py:41
  122.2 6.5 %all-to-all-done.4.projected_ref = bf16[8,16,256]{2,1,0:T(8,128)(2,1)S(1)} async-done(((bf16[8,16,256]{2,1,0:T(8,128)(2,1)}), bf16[8,16,256]{2,1,0:T(8,128)(2,1)S(1)}, u32[]{:S(2)}, u32[]{:S(2)}) %all-to-all-start.4) | async-done | bytes 65568 | tf_op jit(solution)/shard_map/all_to_all | solution.py:41
  128.7 1.0 mix.1
  129.7 8.7 %all-to-all-start.5 = ((bf16[32,16,256]{2,1,0:T(8,128)(2,1)}), bf16[32,16,256]{2,1,0:T(8,128)(2,1)S(1)}, u32[]{:S(2)}, u32[]{:S(2)}) async-start(bf16[32,16,256]{2,1,0:T(8,128)(2,1)} %bitcast.12), calls=%async_computation.5 | async-start | bytes 524288 | tf_op jit(solution)/shard_map/all_to_all | solution.py:41
  138.4 2.0 collective-permute-start.9
  140.4 2.9 %collective-permute-start.10 = (bf16[128,2048]{1,0:T(8,128)(2,1)S(1)}, bf16[128,2048]{1,0:T(8,128)(2,1)S(1)}, u32[]{:S(2)}, u32[]{:S(2)}) collective-permute-start(bf16[128,2048]{1,0:T(8,128)(2,1)S(1)} %copy-done.1), channel_id=1, source_target_pairs={{0,3},{1,0},{2,1},{3,2},{4,7},{5,4},{6,5},{7,6},{8,11},{9,8},{10,9... | collective-permute-start | bytes 1572872 | tf_op jit(solution)/shard_map/ppermute | solution.py:49
  143.3 2.1 collective-permute-start.4
  145.4 9.4 %collective-permute-done.9.refs_11_ = bf16[128,2048]{1,0:T(8,128)(2,1)S(1)} collective-permute-done((bf16[128,2048]{1,0:T(8,128)(2,1)S(1)}, bf16[128,2048]{1,0:T(8,128)(2,1)S(1)}, u32[]{:S(2)}, u32[]{:S(2)}) %collective-permute-start.9) | collective-permute-done | bytes 524320 | tf_op jit(solution)/shard_map/ppermute | solution.py:49
  154.8 1.9 collective-permute-start.11
  156.7 0.8 copy-done.5
  157.5 3.1 %collective-permute-start.5 = (bf16[256,2048]{1,0:T(8,128)(2,1)}, bf16[256,2048]{1,0:T(8,128)(2,1)}, u32[]{:S(2)}, u32[]{:S(2)}) collective-permute-start(bf16[256,2048]{1,0:T(8,128)(2,1)} %get-tuple-element.18.refs_1_), channel_id=1, source_target_pairs={{0,12},{4,0},{8,4},{12,8},{1,13},{5,1},{9,5},{13,9},{2,14},{6,2},{... | collective-permute-start | bytes 3145736 | tf_op jit(solution)/shard_map/ppermute | solution.py:49
  160.6 2.4 collective-permute-start.6
  163.0 2.2 collective-permute-start.7
  165.2 1.4 deal.1
  166.6 6.4 %all-to-all-start.6 = ((bf16[16,16,2048]{2,1,0:T(8,128)(2,1)}), bf16[16,16,2048]{2,1,0:T(8,128)(2,1)S(1)}, u32[]{:S(2)}, u32[]{:S(2)}) async-start(bf16[16,16,2048]{2,1,0:T(8,128)(2,1)} %deal.1), calls=%async_computation.6 | async-start | bytes 2097152 | tf_op jit(solution)/shard_map/all_to_all | solution.py:41
  173.0 3.3 %collective-permute-start.12 = (bf16[128,2048]{1,0:T(8,128)(2,1)}, bf16[128,2048]{1,0:T(8,128)(2,1)S(1)}, u32[]{:S(2)}, u32[]{:S(2)}) collective-permute-start(bf16[128,2048]{1,0:T(8,128)(2,1)} %collective-permute-done.8.refs_10_), channel_id=1, source_target_pairs={{0,1},{1,2},{2,3},{3,0},{4,5},{5,6},{6,7},{7,4},{8,9},{9,10},{10,1... | collective-permute-start | bytes 1572872 | tf_op jit(solution)/shard_map/ppermute | solution.py:49
  176.3 1.5 collective-permute-done.4.refs_4_
  177.8 2.2 collective-permute-start.13
  180.1 19.9 %collective-permute-done.5.refs_5_ = bf16[256,2048]{1,0:T(8,128)(2,1)} collective-permute-done((bf16[256,2048]{1,0:T(8,128)(2,1)}, bf16[256,2048]{1,0:T(8,128)(2,1)}, u32[]{:S(2)}, u32[]{:S(2)}) %collective-permute-start.5) | collective-permute-done | bytes 1048608 | tf_op jit(solution)/shard_map/ppermute | solution.py:49
  199.9 8.6 %collective-permute-done.12.refs_14_ = bf16[128,2048]{1,0:T(8,128)(2,1)S(1)} collective-permute-done((bf16[128,2048]{1,0:T(8,128)(2,1)}, bf16[128,2048]{1,0:T(8,128)(2,1)S(1)}, u32[]{:S(2)}, u32[]{:S(2)}) %collective-permute-start.12) | collective-permute-done | bytes 524320 | tf_op jit(solution)/shard_map/ppermute | solution.py:49
  209.3 1.3 collective-permute-done.13.refs_15_
  211.4 1.0 copy-done.4
  212.5 1.0 copy-done.6
  213.5 1.0 copy-done.8
  214.6 1.0 copy-done.10
  215.6 8.8 %experts.1 = bf16[256,2048]{1,0:T(8,128)(2,1)S(1)} custom-call(bf16[256,2048]{1,0:T(8,128)(2,1)S(1)} %bitcast.28, bf16[256,2048]{1,0:T(8,128)(2,1)S(1)} %copy-done, bf16[256,2048]{1,0:T(8,128)(2,1)} %get-tuple-element.18.refs_1_, bf16[256,2048]{1,0:T(8,128)(2,1)} %collective-permute-done.2.refs_2_, bf16[256,2048]{1,0:T(8,128)(2,1)} %collective-permute-done.3.refs_3_, ...), custom_call_target="tpu_custom_call" | custom-call | tf_op jit(solution)/shard_map/experts/pallas_call | solution.py:406
  224.4 18.8 %all_to_all.46.back_ref = bf16[16,16,2048]{2,1,0:T(8,128)(2,1)S(1)} all-to-all(bf16[16,16,2048]{2,1,0:T(8,128)(2,1)S(1)} %bitcast.29), channel_id=1, replica_groups=mesh['z'=16,'c'=2,'yh'=2,'yl'=2,'x'=4] {'yh','yl','x'}, dimensions={0} | all-to-all | bytes 2097152 | tf_op jit(solution)/shard_map/all_to_all | solution.py:41
  243.3 1.1 collect.1
  244.4 15.8 %all-to-all-start.8 = ((bf16[32,16,256]{2,1,0:T(8,128)(2,1)}), bf16[32,16,256]{2,1,0:T(8,128)(2,1)S(1)}, u32[]{:S(2)}, u32[]{:S(2)}) async-start(bf16[32,16,256]{2,1,0:T(8,128)(2,1)} %bitcast.16), calls=%async_computation.8 | async-start | bytes 524288 | tf_op jit(solution)/shard_map/all_to_all | solution.py:41
  260.5 22.0 %all-to-all-done.8 = bf16[32,16,256]{2,1,0:T(8,128)(2,1)S(1)} async-done(((bf16[32,16,256]{2,1,0:T(8,128)(2,1)}), bf16[32,16,256]{2,1,0:T(8,128)(2,1)S(1)}, u32[]{:S(2)}, u32[]{:S(2)}) %all-to-all-start.8) | async-done | bytes 262176 | tf_op jit(solution)/shard_map/all_to_all | solution.py:41
  282.5 0.9 finish.1
  (55 shorter events, 4.6 us)
Async XLA Ops:
  2.3 13.4 %all-to-all-start = ((bf16[8,256,128]{2,1,0:T(8,128)(2,1)}), bf16[8,256,128]{2,1,0:T(8,128)(2,1)S(1)}, u32[]{:S(2)}, u32[]{:S(2)}) async-start(bf16[8,256,128]{2,1,0:T(8,128)(2,1)} %prepare_queries.1), calls=%async_computation | async-start | bytes 1048576 | tf_op jit(solution)/shard_map/all_to_all | solution.py:41
  46.8 9.1 %collective-permute-start = (bf16[512,256]{1,0:T(8,128)(2,1)S(1)}, bf16[512,256]{1,0:T(8,128)(2,1)S(1)}, u32[]{:S(2)}, u32[]{:S(2)}) collective-permute-start(bf16[512,256]{1,0:T(8,128)(2,1)S(1)} %bitcast.31), channel_id=1, source_target_pairs={{0,16},{16,0},{1,17},{17,1},{2,18},{18,2},{3,19},{19,3},{4,20},{20... | collective-permute-start | bytes 786440 | tf_op jit(solution)/shard_map/ppermute | solution.py:45
  60.0 3.7 %copy-start.13 = (bf16[2048,128]{1,0:T(8,128)(2,1)S(1)}, bf16[2048,128]{1,0:T(8,128)(2,1)}, u32[]{:S(2)}) copy-start(bf16[2048,128]{1,0:T(8,128)(2,1)} %param.18) | copy-start | bytes 1572868
  60.0 19.3 %all-to-all-start.2 = ((bf16[8,144,256]{2,1,0:T(8,128)(2,1)}), bf16[8,144,256]{2,1,0:T(8,128)(2,1)S(1)}, u32[]{:S(2)}, u32[]{:S(2)}) async-start(bf16[8,144,256]{2,1,0:T(8,128)(2,1)} %attend.1), calls=%async_computation.2 | async-start | bytes 1179648 | tf_op jit(solution)/shard_map/all_to_all | solution.py:41
  63.7 53.6 %collective-permute-start.1 = (bf16[2048,128]{1,0:T(8,128)(2,1)S(1)}, bf16[2048,128]{1,0:T(8,128)(2,1)S(1)}, u32[]{:S(2)}, u32[]{:S(2)}) collective-permute-start(bf16[2048,128]{1,0:T(8,128)(2,1)S(1)} %copy-done.13), channel_id=1, source_target_pairs={{0,4},{4,0},{1,5},{5,1},{2,6},{6,2},{3,7},{7,3},{8,12},{12,8},{9,1... | collective-permute-start | bytes 1572872 | tf_op jit(solution)/shard_map/ppermute | solution.py:446
  70.9 89.7 %collective-permute-start.2 = (bf16[256,2048]{1,0:T(8,128)(2,1)}, bf16[256,2048]{1,0:T(8,128)(2,1)}, u32[]{:S(2)}, u32[]{:S(2)}) collective-permute-start(bf16[256,2048]{1,0:T(8,128)(2,1)} %get-tuple-element.17.refs_0_), channel_id=1, source_target_pairs={{0,1},{1,2},{2,3},{3,0},{4,5},{5,6},{6,7},{7,4},{8,9},{9,10},{10,1... | collective-permute-start | bytes 3145736 | tf_op jit(solution)/shard_map/ppermute | solution.py:49
  74.0 5.3 %copy-start.14 = (s32[16,2]{0,1:T(2,128)S(1)}, s32[16,2]{0,1:T(2,128)}, u32[]{:S(2)}) copy-start(s32[16,2]{0,1:T(2,128)} %param.21) | copy-start | bytes 388
  74.0 89.0 %collective-permute-start.3 = (bf16[256,2048]{1,0:T(8,128)(2,1)}, bf16[256,2048]{1,0:T(8,128)(2,1)}, u32[]{:S(2)}, u32[]{:S(2)}) collective-permute-start(bf16[256,2048]{1,0:T(8,128)(2,1)} %get-tuple-element.18.refs_1_), channel_id=1, source_target_pairs={{0,4},{4,8},{8,12},{12,0},{1,5},{5,9},{9,13},{13,1},{2,6},{6,10},{... | collective-permute-start | bytes 3145736 | tf_op jit(solution)/shard_map/ppermute | solution.py:49
  76.2 67.1 %collective-permute-start.8 = (bf16[128,2048]{1,0:T(8,128)(2,1)}, bf16[128,2048]{1,0:T(8,128)(2,1)}, u32[]{:S(2)}, u32[]{:S(2)}) collective-permute-start(bf16[128,2048]{1,0:T(8,128)(2,1)} %get-tuple-element.19.refs_8_), channel_id=1, source_target_pairs={{0,1},{1,2},{2,3},{3,0},{4,5},{5,6},{6,7},{7,4},{8,9},{9,10},{10,1... | collective-permute-start | bytes 1572872 | tf_op jit(solution)/shard_map/ppermute | solution.py:49
  80.4 36.6 %all-to-all-start.3 = ((bf16[16,128,128]{2,1,0:T(8,128)(2,1)}), bf16[16,128,128]{2,1,0:T(8,128)(2,1)S(1)}, u32[]{:S(2)}, u32[]{:S(2)}) async-start(bf16[16,128,128]{2,1,0:T(8,128)(2,1)} %combine.1), calls=%async_computation.3 | async-start | bytes 1048576 | tf_op jit(solution)/shard_map/all_to_all | solution.py:41
  117.3 26.0 %copy-start = (bf16[256,2048]{1,0:T(8,128)(2,1)S(1)}, bf16[256,2048]{1,0:T(8,128)(2,1)}, u32[]{:S(2)}) copy-start(bf16[256,2048]{1,0:T(8,128)(2,1)} %get-tuple-element.17.refs_0_) | copy-start | bytes 3145732
  117.7 11.0 %copy-start.11 = (bf16[16,2048]{1,0:T(8,128)(2,1)S(1)}, bf16[16,2048]{1,0:T(8,128)(2,1)}, u32[]{:S(2)}) copy-start(bf16[16,2048]{1,0:T(8,128)(2,1)} %residual_ref.1) | copy-start | bytes 196612
  117.7 10.9 %copy-start.12 = (f32[2048]{0:T(1024)S(1)}, f32[2048]{0:T(1024)}, u32[]{:S(2)}) copy-start(f32[2048]{0:T(1024)} %param.19) | copy-start | bytes 24580
  118.5 19.9 %copy-start.2 = (bf16[128,2048]{1,0:T(8,128)(2,1)S(1)}, bf16[128,2048]{1,0:T(8,128)(2,1)}, u32[]{:S(2)}) copy-start(bf16[128,2048]{1,0:T(8,128)(2,1)} %get-tuple-element.20.refs_9_) | copy-start | bytes 1572868
  118.5 21.9 %copy-start.1 = (bf16[128,2048]{1,0:T(8,128)(2,1)S(1)}, bf16[128,2048]{1,0:T(8,128)(2,1)}, u32[]{:S(2)}) copy-start(bf16[128,2048]{1,0:T(8,128)(2,1)} %get-tuple-element.19.refs_8_) | copy-start | bytes 1572868
  118.5 10.2 %all-to-all-start.4 = ((bf16[8,16,256]{2,1,0:T(8,128)(2,1)}), bf16[8,16,256]{2,1,0:T(8,128)(2,1)S(1)}, u32[]{:S(2)}, u32[]{:S(2)}) async-start(bf16[8,16,256]{2,1,0:T(8,128)(2,1)} %bitcast.8), calls=%async_computation.4 | async-start | bytes 131072 | tf_op jit(solution)/shard_map/all_to_all | solution.py:41
  129.7 35.5 %all-to-all-start.5 = ((bf16[32,16,256]{2,1,0:T(8,128)(2,1)}), bf16[32,16,256]{2,1,0:T(8,128)(2,1)S(1)}, u32[]{:S(2)}, u32[]{:S(2)}) async-start(bf16[32,16,256]{2,1,0:T(8,128)(2,1)} %bitcast.12), calls=%async_computation.5 | async-start | bytes 524288 | tf_op jit(solution)/shard_map/all_to_all | solution.py:41
  138.4 16.4 %collective-permute-start.9 = (bf16[128,2048]{1,0:T(8,128)(2,1)S(1)}, bf16[128,2048]{1,0:T(8,128)(2,1)S(1)}, u32[]{:S(2)}, u32[]{:S(2)}) collective-permute-start(bf16[128,2048]{1,0:T(8,128)(2,1)S(1)} %copy-done.2), channel_id=1, source_target_pairs={{0,4},{4,8},{8,12},{12,0},{1,5},{5,9},{9,13},{13,1},{2,6},{6,10},{... | collective-permute-start | bytes 1572872 | tf_op jit(solution)/shard_map/ppermute | solution.py:49
  140.4 16.3 %collective-permute-start.10 = (bf16[128,2048]{1,0:T(8,128)(2,1)S(1)}, bf16[128,2048]{1,0:T(8,128)(2,1)S(1)}, u32[]{:S(2)}, u32[]{:S(2)}) collective-permute-start(bf16[128,2048]{1,0:T(8,128)(2,1)S(1)} %copy-done.1), channel_id=1, source_target_pairs={{0,3},{1,0},{2,1},{3,2},{4,7},{5,4},{6,5},{7,6},{8,11},{9,8},{10,9... | collective-permute-start | bytes 1572872 | tf_op jit(solution)/shard_map/ppermute | solution.py:49
  143.3 34.5 %collective-permute-start.4 = (bf16[256,2048]{1,0:T(8,128)(2,1)S(1)}, bf16[256,2048]{1,0:T(8,128)(2,1)}, u32[]{:S(2)}, u32[]{:S(2)}) collective-permute-start(bf16[256,2048]{1,0:T(8,128)(2,1)S(1)} %copy-done), channel_id=1, source_target_pairs={{0,3},{1,0},{2,1},{3,2},{4,7},{5,4},{6,5},{7,6},{8,11},{9,8},{10,9... | collective-permute-start | bytes 3145736 | tf_op jit(solution)/shard_map/ppermute | solution.py:49
  154.8 8.2 %copy-start.3 = (bf16[128,2048]{1,0:T(8,128)(2,1)}, bf16[128,2048]{1,0:T(8,128)(2,1)S(1)}, u32[]{:S(2)}) copy-start(bf16[128,2048]{1,0:T(8,128)(2,1)S(1)} %collective-permute-done.9.refs_11_) | copy-start | bytes 1572868
  154.8 18.3 %collective-permute-start.11 = (bf16[128,2048]{1,0:T(8,128)(2,1)S(1)}, bf16[128,2048]{1,0:T(8,128)(2,1)}, u32[]{:S(2)}, u32[]{:S(2)}) collective-permute-start(bf16[128,2048]{1,0:T(8,128)(2,1)S(1)} %copy-done.2), channel_id=1, source_target_pairs={{0,12},{4,0},{8,4},{12,8},{1,13},{5,1},{9,5},{13,9},{2,14},{6,2},{... | collective-permute-start | bytes 1572872 | tf_op jit(solution)/shard_map/ppermute | solution.py:49
  156.7 0.8 copy-start.5
  157.5 42.4 %collective-permute-start.5 = (bf16[256,2048]{1,0:T(8,128)(2,1)}, bf16[256,2048]{1,0:T(8,128)(2,1)}, u32[]{:S(2)}, u32[]{:S(2)}) collective-permute-start(bf16[256,2048]{1,0:T(8,128)(2,1)} %get-tuple-element.18.refs_1_), channel_id=1, source_target_pairs={{0,12},{4,0},{8,4},{12,8},{1,13},{5,1},{9,5},{13,9},{2,14},{6,2},{... | collective-permute-start | bytes 3145736 | tf_op jit(solution)/shard_map/ppermute | solution.py:49
  160.6 50.8 %collective-permute-start.6 = (bf16[256,2048]{1,0:T(8,128)(2,1)}, bf16[256,2048]{1,0:T(8,128)(2,1)}, u32[]{:S(2)}, u32[]{:S(2)}) collective-permute-start(bf16[256,2048]{1,0:T(8,128)(2,1)} %collective-permute-done.2.refs_2_), channel_id=1, source_target_pairs={{0,1},{1,2},{2,3},{3,0},{4,5},{5,6},{6,7},{7,4},{8,9},{9,10},{10,1... | collective-permute-start | bytes 3145736 | tf_op jit(solution)/shard_map/ppermute | solution.py:49
  163.0 48.4 %collective-permute-start.7 = (bf16[256,2048]{1,0:T(8,128)(2,1)}, bf16[256,2048]{1,0:T(8,128)(2,1)}, u32[]{:S(2)}, u32[]{:S(2)}) collective-permute-start(bf16[256,2048]{1,0:T(8,128)(2,1)} %collective-permute-done.3.refs_3_), channel_id=1, source_target_pairs={{0,4},{4,8},{8,12},{12,0},{1,5},{5,9},{9,13},{13,1},{2,6},{6,10},{... | collective-permute-start | bytes 3145736 | tf_op jit(solution)/shard_map/ppermute | solution.py:49
  166.6 44.8 %all-to-all-start.6 = ((bf16[16,16,2048]{2,1,0:T(8,128)(2,1)}), bf16[16,16,2048]{2,1,0:T(8,128)(2,1)S(1)}, u32[]{:S(2)}, u32[]{:S(2)}) async-start(bf16[16,16,2048]{2,1,0:T(8,128)(2,1)} %deal.1), calls=%async_computation.6 | async-start | bytes 2097152 | tf_op jit(solution)/shard_map/all_to_all | solution.py:41
  173.0 35.5 %collective-permute-start.12 = (bf16[128,2048]{1,0:T(8,128)(2,1)}, bf16[128,2048]{1,0:T(8,128)(2,1)S(1)}, u32[]{:S(2)}, u32[]{:S(2)}) collective-permute-start(bf16[128,2048]{1,0:T(8,128)(2,1)} %collective-permute-done.8.refs_10_), channel_id=1, source_target_pairs={{0,1},{1,2},{2,3},{3,0},{4,5},{5,6},{6,7},{7,4},{8,9},{9,10},{10,1... | collective-permute-start | bytes 1572872 | tf_op jit(solution)/shard_map/ppermute | solution.py:49
  177.8 32.8 %collective-permute-start.13 = (bf16[128,2048]{1,0:T(8,128)(2,1)}, bf16[128,2048]{1,0:T(8,128)(2,1)S(1)}, u32[]{:S(2)}, u32[]{:S(2)}) collective-permute-start(bf16[128,2048]{1,0:T(8,128)(2,1)} %copy-done.3), channel_id=1, source_target_pairs={{0,4},{4,8},{8,12},{12,0},{1,5},{5,9},{9,13},{13,1},{2,6},{6,10},{... | collective-permute-start | bytes 1572872 | tf_op jit(solution)/shard_map/ppermute | solution.py:49
  208.5 0.8 copy-start.7
  210.6 0.8 copy-start.9
  211.4 1.0 copy-start.4
  212.5 1.0 copy-start.6
  213.5 1.0 copy-start.8
  214.6 1.0 copy-start.10
  244.4 15.9 %copy-start.15 = (f32[16,2]{0,1:T(2,128)S(1)}, f32[16,2]{0,1:T(2,128)}, u32[]{:S(2)}) copy-start(f32[16,2]{0,1:T(2,128)} %param.22) | copy-start | bytes 388
  244.4 38.1 %all-to-all-start.8 = ((bf16[32,16,256]{2,1,0:T(8,128)(2,1)}), bf16[32,16,256]{2,1,0:T(8,128)(2,1)S(1)}, u32[]{:S(2)}, u32[]{:S(2)}) async-start(bf16[32,16,256]{2,1,0:T(8,128)(2,1)} %bitcast.16), calls=%async_computation.8 | async-start | bytes 524288 | tf_op jit(solution)/shard_map/all_to_all | solution.py:41

commit v8 on v7

--- a/solution.py
+++ b/solution.py
@@ -66,46 +66,34 @@
     return (f * jnp.cos(angle) + other * jnp.sin(angle)).astype(BF)
 
 
-def queries_kernel(start_ref, q_ref, gain_ref, out_ref):
-    q_rot = turned(q_ref[...], gain_ref[...], start_ref[0])
-    for i in range(out_ref.shape[0]):
-        out_ref[i] = q_rot
-
-
-def prepare_queries(queries, gain, start):
-    return pl.pallas_call(
-        queries_kernel,
-        in_specs=[pl.BlockSpec(memory_space=pltpu.SMEM), IN_VMEM, IN_VMEM],
-        out_specs=IN_VMEM,
-        out_shape=jax.ShapeDtypeStruct((NG, *queries.shape), BF),
-        name="prepare_queries",
-    )(start.reshape(1), queries, gain[None, :])
-
-
-def keys_kernel(at_ref, k_ref, v_ref, gain_ref, out_ref):
-    k_rot = turned(k_ref[...], gain_ref[...], at_ref[2])
+def prepare_kernel(at_ref, q_ref, k_ref, v_ref, q_gain_ref, k_gain_ref, q8_ref, kv_ref):
+    q_rot = turned(q_ref[...], q_gain_ref[...], at_ref[2])
+    for i in range(q8_ref.shape[0]):
+        q8_ref[i] = q_rot
+    k_rot = turned(k_ref[...], k_gain_ref[...], at_ref[3])
     both = jnp.concatenate([k_rot, v_ref[...]], axis=1)
-    for i in range(out_ref.shape[0]):
-        out_ref[i] = both
-
-
-def prepare_keys(keys, values, gain, block, head, start):
-    width = gain.shape[0]
-    size = keys.shape[0] // NG
-    at = jnp.stack([block, head, start + block * size]).astype(jnp.int32)
+    for i in range(kv_ref.shape[0]):
+        kv_ref[i] = both
+
+
+def prepare(queries, keys, values, query_gain, key_gain, block, head, start):
+    tokens, width = queries.shape
+    size = tokens // NG
+    at = jnp.stack([block, head, start, start + block * size]).astype(jnp.int32)
+    whole = lambda shape: pl.BlockSpec(shape, lambda i, at: (0,) * len(shape))
     part = pl.BlockSpec((size, width), lambda i, at: (at[0], at[1]))
-    out = (NZ, size, 2 * width)
-    return pl.pallas_call(
-        keys_kernel,
+    outs = ((NG, tokens, width), (NZ, size, 2 * width))
+    return pl.pallas_call(
+        prepare_kernel,
         grid_spec=pltpu.PrefetchScalarGridSpec(
             num_scalar_prefetch=1,
             grid=(1,),
-            in_specs=[part, part, pl.BlockSpec((1, width), lambda i, at: (0, 0))],
-            out_specs=pl.BlockSpec(out, lambda i, at: (0, 0, 0)),
+            in_specs=[whole((tokens, width)), part, part, whole((1, width)), whole((1, width))],
+            out_specs=[whole(shape) for shape in outs],
         ),
-        out_shape=jax.ShapeDtypeStruct(out, BF),
-        name="prepare_keys",
-    )(at, keys, values, gain[None, :])
+        out_shape=[jax.ShapeDtypeStruct(shape, BF) for shape in outs],
+        name="prepare",
+    )(at, queries, keys, values, query_gain[None, :], key_gain[None, :])
 
 
 def split3(x):
@@ -217,11 +205,17 @@
     return jnp.where(r == source_of(i), 1.0, 0.0).astype(BF)
 
 
-def mix_kernel(projected_ref, residual_ref, scale_ref, selector_ref, mixed_ref, sent_ref):
+def mix_kernel(
+    yl_ref, projected_ref, residual_ref, scale_ref, selector_ref, mixed_ref, sent_ref
+):
     width = projected_ref.shape[2] // NYL
     projected = jnp.concatenate(
         [
-            projected_ref[NX * h + i, :, k * width : (k + 1) * width].astype(F32)
+            jnp.where(
+                yl_ref[0] == k,
+                projected_ref[NX * h + i, :, :width].astype(F32),
+                projected_ref[NX * h + i, :, width:].astype(F32),
+            )
             for h in range(NYH)
             for k in range(NYL)
             for i in range(NX)
@@ -238,11 +232,11 @@
     ).astype(BF)
 
 
-def mix(projected, residual, scale, selector):
+def mix(yl, projected, residual, scale, selector):
     shape = (selector.shape[0], residual.shape[1] // FOLD)
     return pl.pallas_call(
         mix_kernel,
-        in_specs=[IN_VMEM] * 4,
+        in_specs=[pl.BlockSpec(memory_space=pltpu.SMEM)] + [IN_VMEM] * 4,
         out_specs=[IN_VMEM] * 2,
         out_shape=[
             jax.ShapeDtypeStruct(residual.shape, BF),
@@ -250,7 +244,7 @@
         ],
         compiler_params=grant(16),
         name="mix",
-    )(projected, residual, scale[None, :], selector)
+    )(yl.reshape(1).astype(jnp.int32), projected, residual, scale[None, :], selector)
 
 
 def deal_kernel(arrived_ref, out_ref):
@@ -441,10 +435,11 @@
     yh, yl, x = lax.axis_index("yh"), lax.axis_index("yl"), lax.axis_index("x")
     start = (z * NC + c) * tok_sp
 
-    q8 = prepare_queries(queries, query_gain, start)
+    q8, kv = prepare(
+        queries, keys, values, query_gain, key_gain, yl * NX + x, yh, start
+    )
     q8 = exchange(q8, GROUP)
     out_proj_other = lax.ppermute(out_proj, "yl", [(0, 1), (1, 0)])
-    kv = prepare_keys(keys, values, key_gain, yl * NX + x, yh, start)
     q8, kv = lax.optimization_barrier((q8, kv))
     kv_mine = exchange(kv, "z").reshape(-1, 2 * width)
     kv_other = swap_cores(kv_mine)
@@ -462,15 +457,10 @@
     parts = exchange(parts, GROUP)
     attn_all = exchange(combine(parts), TP).reshape(NT * width, -1)
 
-    def project(columns):
-        return lax.dot_general(
-            attn_all, columns, (((0,), (0,)), ((), ())), preferred_element_type=F32
-        ).astype(BF)
-
-    mine, other = project(out_proj), project(out_proj_other)
-    columns = jnp.concatenate(
-        [jnp.where(yl == 0, mine, other), jnp.where(yl == 0, other, mine)], axis=1
-    )
+    both_proj = jnp.concatenate([out_proj, out_proj_other], axis=1)
+    columns = lax.dot_general(
+        attn_all, both_proj, (((0,), (0,)), ((), ())), preferred_element_type=F32
+    ).astype(BF)
     projected = exchange(columns.reshape(NYH * NX, tok_dev, -1), ("yh", "x"))
 
     cap = max(2, 2 * tok_dev * top // (NZ * NC))
@@ -492,7 +482,7 @@
         picks.append(
             (same_fold & (target[:, None] == (place // FOLD)[None, :])).astype(BF)
         )
-    mixed, sent = mix(projected, residual, expert_norm_scale, sum(picks).T)
+    mixed, sent = mix(yl, projected, residual, expert_norm_scale, sum(picks).T)
     blocks = (NZ * NC, cap * FOLD, depth // FOLD)
     arrived = exchange(sent.reshape(blocks), ("z", "c"))
 

time: 285 us -> 285 us (level)
  blocking collectives: 50 us -> 61.5 us
  starting transfers between devices: 90.6 us -> 85.6 us
  waiting for transfers between devices: 106 us -> 101 us
    all_to_all x2 -> x3, blocking collectives: 50 us -> 61.5 us  [exchange(): return lax.all_to_all(blocks, axis, split_axis=0, concat_axis=0, tiled=True)]
    all_to_all x7 -> x6, starting transfers between devices: 49.1 us -> 43.1 us  [exchange(): return lax.all_to_all(blocks, axis, split_axis=0, concat_axis=0, tiled=True)]
    all_to_all x7 -> x6, waiting for transfers between devices: 64 us -> 59.5 us  [exchange(): return lax.all_to_all(blocks, axis, split_axis=0, concat_axis=0, tiled=True)]
    unnamed x33 -> x35, local copies, waits for them, and re-layouts: 6.68 us -> 6.68 us
  transfers between devices with their start and end apart: 21 -> 20, of which waited for: 10 -> 9; matrix products, arithmetic and copies ran while one was open for 1% -> 1% of each run, Pallas kernels for 3% -> 3%
where the time goes in v8:
time: 285 us; the launch traced here: 283 us
  waiting for transfers between devices  101 us (35%)
  starting transfers between devices  85.6 us (30%)
  blocking collectives  61.5 us (22%)
  Pallas kernels  25.4 us (9%)
  local copies, waits for them, and re-layouts  6.85 us (2%)
    all_to_all x3, blocking collectives, exchange(): return lax.all_to_all(blocks, axis, split_axis=0, concat_axis=0, tiled=True)  61.5 us
    all_to_all x6, waiting for transfers between devices, exchange(): return lax.all_to_all(blocks, axis, split_axis=0, concat_axis=0, tiled=True)  59.5 us
    all_to_all x6, starting transfers between devices, exchange(): return lax.all_to_all(blocks, axis, split_axis=0, concat_axis=0, tiled=True)  43.1 us
    ppermute x12, waiting for transfers between devices, ring(): return lax.ppermute(value, axis, [(i, (i + step) % 4) for i in range(4)])  40.6 us
    ppermute x12, starting transfers between devices, ring(): return lax.ppermute(value, axis, [(i, (i + step) % 4) for i in range(4)])  30.3 us
    pallas_call x1, Pallas kernels, experts(): pl.pallas_call(experts_kernel, in_specs=[IN_VMEM] + [IN_HBM] * len(pieces...  8.83 us
    ppermute x1, starting transfers between devices, swap_cores(): return lax.ppermute(value, 'c', [(0, 1), (1, 0)])  8.79 us
    unnamed x35, local copies, waits for them, and re-layouts  6.68 us
  transfers between devices with their start and end apart: 20, of which 9 were waited for; matrix products, arithmetic and copies ran while one was open for 1% of the time, Pallas kernels for 3%

profile of v8, /device:TPU:1, one launch (start us, length us, event | category | flops | bytes accessed | tf_op | source)
XLA Modules:
  0.0 283.2 jit_solution(12312720405875152241)
XLA Ops:
  0.6 3.1 %prepare.1 = (bf16[8,256,128]{2,1,0:T(8,128)(2,1)}, bf16[16,32,256]{2,1,0:T(8,128)(2,1)}) custom-call(s32[4]{0:T(128)} %pad_add_fusion.at_ref, bf16[256,128]{1,0:T(8,128)(2,1)} %q_ref.1, bf16[256,256]{1,0:T(8,128)(2,1)} %k_ref.1, bf16[256,256]{1,0:T(8,128)(2,1)} %v_ref.1, f32[1,128]{1,0:T(1,128)} %bitcast.34, f32[1,128]{1,0:T(1,128)} %bitcast.35), custom_call_target="tpu_custom_call" | custom-call | tf_op jit(solution)/shard_map/prepare/pallas_call | solution.py:86
  3.7 13.5 %all_to_all.45.q_ref = bf16[8,256,128]{2,1,0:T(8,128)(2,1)S(1)} all-to-all(bf16[8,256,128]{2,1,0:T(8,128)(2,1)} %get-tuple-element.15), channel_id=1, replica_groups=mesh['z'=16,'c'=2,'yh'=2,'yl'=2,'x'=4] {'yl','x'}, dimensions={0} | all-to-all | bytes 1048576 | tf_op jit(solution)/shard_map/all_to_all | solution.py:41
  17.2 29.1 %all_to_all.46 = bf16[16,32,256]{2,1,0:T(8,128)(2,1)S(1)} all-to-all(bf16[16,32,256]{2,1,0:T(8,128)(2,1)S(1)} %copy-done.13), channel_id=1, replica_groups=mesh['z'=16,'c'=2,'yh'=2,'yl'=2,'x'=4] {'z'}, dimensions={0} | all-to-all | bytes 524288 | tf_op jit(solution)/shard_map/all_to_all | solution.py:41
  46.3 8.8 %collective-permute-start = (bf16[512,256]{1,0:T(8,128)(2,1)S(1)}, bf16[512,256]{1,0:T(8,128)(2,1)S(1)}, u32[]{:S(2)}, u32[]{:S(2)}) collective-permute-start(bf16[512,256]{1,0:T(8,128)(2,1)S(1)} %bitcast.29), channel_id=1, source_target_pairs={{0,16},{16,0},{1,17},{17,1},{2,18},{18,2},{3,19},{19,3},{4,20},{20... | collective-permute-start | bytes 786440 | tf_op jit(solution)/shard_map/ppermute | solution.py:45
  55.1 1.1 collective-permute-done.other_ref
  56.3 4.1 %attend.1 = bf16[8,144,256]{2,1,0:T(8,128)(2,1)} custom-call(bf16[8,256,128]{2,1,0:T(8,128)(2,1)S(1)} %all_to_all.45.q_ref, bf16[512,256]{1,0:T(8,128)(2,1)S(1)} %bitcast.30, bf16[512,256]{1,0:T(8,128)(2,1)S(1)} %collective-permute-done.other_ref), custom_call_target="tpu_custom_call" | custom-call | tf_op jit(solution)/shard_map/attend/pallas_call | solution.py:140
  60.4 3.5 %all-to-all-start.2 = ((bf16[8,144,256]{2,1,0:T(8,128)(2,1)}), bf16[8,144,256]{2,1,0:T(8,128)(2,1)S(1)}, u32[]{:S(2)}, u32[]{:S(2)}) async-start(bf16[8,144,256]{2,1,0:T(8,128)(2,1)} %attend.1), calls=%async_computation.2 | async-start | bytes 1179648 | tf_op jit(solution)/shard_map/all_to_all | solution.py:41
  64.0 3.4 %collective-permute-start.1 = (bf16[2048,128]{1,0:T(8,128)(2,1)S(1)}, bf16[2048,128]{1,0:T(8,128)(2,1)S(1)}, u32[]{:S(2)}, u32[]{:S(2)}) collective-permute-start(bf16[2048,128]{1,0:T(8,128)(2,1)S(1)} %copy-done.16), channel_id=1, source_target_pairs={{0,4},{4,0},{1,5},{5,1},{2,6},{6,2},{3,7},{7,3},{8,12},{12,8},{9,1... | collective-permute-start | bytes 1572872 | tf_op jit(solution)/shard_map/ppermute | solution.py:442
  67.4 3.9 %pack.1 = (bf16[256,2048]{1,0:T(8,128)(2,1)}, bf16[256,2048]{1,0:T(8,128)(2,1)}, bf16[128,2048]{1,0:T(8,128)(2,1)}, bf16[128,2048]{1,0:T(8,128)(2,1)}) custom-call(bf16[1,2048,256]{2,1,0:T(8,128)(2,1)} %gate_ref.1, bf16[1,2048,256]{2,1,0:T(8,128)(2,1)} %up_ref.1, bf16[1,256,2048]{2,1,0:T(8,128)(2,1)} %down_ref.1), custom_call_target="tpu_custom_call" | custom-call | tf_op jit(solution)/shard_map/pack/pallas_call | solution.py:343
  71.3 3.1 %collective-permute-start.2 = (bf16[256,2048]{1,0:T(8,128)(2,1)}, bf16[256,2048]{1,0:T(8,128)(2,1)}, u32[]{:S(2)}, u32[]{:S(2)}) collective-permute-start(bf16[256,2048]{1,0:T(8,128)(2,1)} %get-tuple-element.21.refs_0_), channel_id=1, source_target_pairs={{0,1},{1,2},{2,3},{3,0},{4,5},{5,6},{6,7},{7,4},{8,9},{9,10},{10,1... | collective-permute-start | bytes 3145736 | tf_op jit(solution)/shard_map/ppermute | solution.py:49
  74.4 2.2 collective-permute-start.3
  76.5 3.1 %collective-permute-start.8 = (bf16[128,2048]{1,0:T(8,128)(2,1)}, bf16[128,2048]{1,0:T(8,128)(2,1)}, u32[]{:S(2)}, u32[]{:S(2)}) collective-permute-start(bf16[128,2048]{1,0:T(8,128)(2,1)} %get-tuple-element.23.refs_8_), channel_id=1, source_target_pairs={{0,1},{1,2},{2,3},{3,0},{4,5},{5,6},{6,7},{7,4},{8,9},{9,10},{10,1... | collective-permute-start | bytes 1572872 | tf_op jit(solution)/shard_map/ppermute | solution.py:49
  79.7 1.0 combine.1
  80.7 5.2 %all-to-all-start.3 = ((bf16[16,128,128]{2,1,0:T(8,128)(2,1)}), bf16[16,128,128]{2,1,0:T(8,128)(2,1)S(1)}, u32[]{:S(2)}, u32[]{:S(2)}) async-start(bf16[16,128,128]{2,1,0:T(8,128)(2,1)} %combine.1), calls=%async_computation.3 | async-start | bytes 1048576 | tf_op jit(solution)/shard_map/all_to_all | solution.py:41
  86.3 31.0 %all-to-all-done.3 = bf16[16,128,128]{2,1,0:T(8,128)(2,1)S(1)} async-done(((bf16[16,128,128]{2,1,0:T(8,128)(2,1)}), bf16[16,128,128]{2,1,0:T(8,128)(2,1)S(1)}, u32[]{:S(2)}, u32[]{:S(2)}) %all-to-all-start.3) | async-done | bytes 524320 | tf_op jit(solution)/shard_map/all_to_all | solution.py:41
  117.3 1.0 convolution_convert_fusion
  118.3 3.5 %all-to-all-start.4 = ((bf16[8,16,256]{2,1,0:T(8,128)(2,1)}), bf16[8,16,256]{2,1,0:T(8,128)(2,1)S(1)}, u32[]{:S(2)}, u32[]{:S(2)}) async-start(bf16[8,16,256]{2,1,0:T(8,128)(2,1)} %bitcast.9), calls=%async_computation.4 | async-start | bytes 131072 | tf_op jit(solution)/shard_map/all_to_all | solution.py:41
  122.1 6.5 %all-to-all-done.4.projected_ref = bf16[8,16,256]{2,1,0:T(8,128)(2,1)S(1)} async-done(((bf16[8,16,256]{2,1,0:T(8,128)(2,1)}), bf16[8,16,256]{2,1,0:T(8,128)(2,1)S(1)}, u32[]{:S(2)}, u32[]{:S(2)}) %all-to-all-start.4) | async-done | bytes 65568 | tf_op jit(solution)/shard_map/all_to_all | solution.py:41
  128.5 1.0 mix.1
  129.6 8.8 %all-to-all-start.5 = ((bf16[32,16,256]{2,1,0:T(8,128)(2,1)}), bf16[32,16,256]{2,1,0:T(8,128)(2,1)S(1)}, u32[]{:S(2)}, u32[]{:S(2)}) async-start(bf16[32,16,256]{2,1,0:T(8,128)(2,1)} %bitcast.13), calls=%async_computation.5 | async-start | bytes 524288 | tf_op jit(solution)/shard_map/all_to_all | solution.py:41
  138.4 2.0 collective-permute-start.9
  140.3 2.9 %collective-permute-start.10 = (bf16[128,2048]{1,0:T(8,128)(2,1)S(1)}, bf16[128,2048]{1,0:T(8,128)(2,1)S(1)}, u32[]{:S(2)}, u32[]{:S(2)}) collective-permute-start(bf16[128,2048]{1,0:T(8,128)(2,1)S(1)} %copy-done.1), channel_id=1, source_target_pairs={{0,3},{1,0},{2,1},{3,2},{4,7},{5,4},{6,5},{7,6},{8,11},{9,8},{10,9... | collective-permute-start | bytes 1572872 | tf_op jit(solution)/shard_map/ppermute | solution.py:49
  143.2 2.1 collective-permute-start.4
  145.4 9.4 %collective-permute-done.9.refs_11_ = bf16[128,2048]{1,0:T(8,128)(2,1)S(1)} collective-permute-done((bf16[128,2048]{1,0:T(8,128)(2,1)S(1)}, bf16[128,2048]{1,0:T(8,128)(2,1)S(1)}, u32[]{:S(2)}, u32[]{:S(2)}) %collective-permute-start.9) | collective-permute-done | bytes 524320 | tf_op jit(solution)/shard_map/ppermute | solution.py:49
  154.7 1.9 collective-permute-start.11
  156.6 0.8 copy-done.5
  157.5 3.1 %collective-permute-start.5 = (bf16[256,2048]{1,0:T(8,128)(2,1)}, bf16[256,2048]{1,0:T(8,128)(2,1)}, u32[]{:S(2)}, u32[]{:S(2)}) collective-permute-start(bf16[256,2048]{1,0:T(8,128)(2,1)} %get-tuple-element.22.refs_1_), channel_id=1, source_target_pairs={{0,12},{4,0},{8,4},{12,8},{1,13},{5,1},{9,5},{13,9},{2,14},{6,2},{... | collective-permute-start | bytes 3145736 | tf_op jit(solution)/shard_map/ppermute | solution.py:49
  160.6 2.4 collective-permute-start.6
  163.0 2.2 collective-permute-start.7
  165.2 1.4 deal.1
  166.6 6.4 %all-to-all-start.6 = ((bf16[16,16,2048]{2,1,0:T(8,128)(2,1)}), bf16[16,16,2048]{2,1,0:T(8,128)(2,1)S(1)}, u32[]{:S(2)}, u32[]{:S(2)}) async-start(bf16[16,16,2048]{2,1,0:T(8,128)(2,1)} %deal.1), calls=%async_computation.6 | async-start | bytes 2097152 | tf_op jit(solution)/shard_map/all_to_all | solution.py:41
  173.0 3.3 %collective-permute-start.12 = (bf16[128,2048]{1,0:T(8,128)(2,1)}, bf16[128,2048]{1,0:T(8,128)(2,1)S(1)}, u32[]{:S(2)}, u32[]{:S(2)}) collective-permute-start(bf16[128,2048]{1,0:T(8,128)(2,1)} %collective-permute-done.8.refs_10_), channel_id=1, source_target_pairs={{0,1},{1,2},{2,3},{3,0},{4,5},{5,6},{6,7},{7,4},{8,9},{9,10},{10,1... | collective-permute-start | bytes 1572872 | tf_op jit(solution)/shard_map/ppermute | solution.py:49
  176.3 1.5 collective-permute-done.4.refs_4_
  177.8 2.2 collective-permute-start.13
  180.0 19.9 %collective-permute-done.5.refs_5_ = bf16[256,2048]{1,0:T(8,128)(2,1)} collective-permute-done((bf16[256,2048]{1,0:T(8,128)(2,1)}, bf16[256,2048]{1,0:T(8,128)(2,1)}, u32[]{:S(2)}, u32[]{:S(2)}) %collective-permute-start.5) | collective-permute-done | bytes 1048608 | tf_op jit(solution)/shard_map/ppermute | solution.py:49
  199.9 8.6 %collective-permute-done.12.refs_14_ = bf16[128,2048]{1,0:T(8,128)(2,1)S(1)} collective-permute-done((bf16[128,2048]{1,0:T(8,128)(2,1)}, bf16[128,2048]{1,0:T(8,128)(2,1)S(1)}, u32[]{:S(2)}, u32[]{:S(2)}) %collective-permute-start.12) | collective-permute-done | bytes 524320 | tf_op jit(solution)/shard_map/ppermute | solution.py:49
  208.4 0.8 copy-done.7
  209.2 1.3 collective-permute-done.13.refs_15_
  211.4 1.0 copy-done.4
  212.4 1.0 copy-done.6
  213.5 1.0 copy-done.8
  214.5 1.0 copy-done.10
  215.5 8.8 %experts.1 = bf16[256,2048]{1,0:T(8,128)(2,1)S(1)} custom-call(bf16[256,2048]{1,0:T(8,128)(2,1)S(1)} %bitcast.26, bf16[256,2048]{1,0:T(8,128)(2,1)S(1)} %copy-done, bf16[256,2048]{1,0:T(8,128)(2,1)} %get-tuple-element.22.refs_1_, bf16[256,2048]{1,0:T(8,128)(2,1)} %collective-permute-done.2.refs_2_, bf16[256,2048]{1,0:T(8,128)(2,1)} %collective-permute-done.3.refs_3_, ...), custom_call_target="tpu_custom_call" | custom-call | tf_op jit(solution)/shard_map/experts/pallas_call | solution.py:400
  224.4 18.8 %all_to_all.47.back_ref = bf16[16,16,2048]{2,1,0:T(8,128)(2,1)S(1)} all-to-all(bf16[16,16,2048]{2,1,0:T(8,128)(2,1)S(1)} %bitcast.27), channel_id=1, replica_groups=mesh['z'=16,'c'=2,'yh'=2,'yl'=2,'x'=4] {'yh','yl','x'}, dimensions={0} | all-to-all | bytes 2097152 | tf_op jit(solution)/shard_map/all_to_all | solution.py:41
  243.2 1.1 collect.1
  244.3 15.7 %all-to-all-start.8 = ((bf16[32,16,256]{2,1,0:T(8,128)(2,1)}), bf16[32,16,256]{2,1,0:T(8,128)(2,1)S(1)}, u32[]{:S(2)}, u32[]{:S(2)}) async-start(bf16[32,16,256]{2,1,0:T(8,128)(2,1)} %bitcast.17), calls=%async_computation.8 | async-start | bytes 524288 | tf_op jit(solution)/shard_map/all_to_all | solution.py:41
  260.3 22.0 %all-to-all-done.8 = bf16[32,16,256]{2,1,0:T(8,128)(2,1)S(1)} async-done(((bf16[32,16,256]{2,1,0:T(8,128)(2,1)}), bf16[32,16,256]{2,1,0:T(8,128)(2,1)S(1)}, u32[]{:S(2)}, u32[]{:S(2)}) %all-to-all-start.8) | async-done | bytes 262176 | tf_op jit(solution)/shard_map/all_to_all | solution.py:41
  282.3 0.9 finish.1
  (52 shorter events, 2.3 us)
Async XLA Ops:
  3.7 13.5 %copy-start.13 = (bf16[16,32,256]{2,1,0:T(8,128)(2,1)S(1)}, bf16[16,32,256]{2,1,0:T(8,128)(2,1)}, u32[]{:S(2)}) copy-start(bf16[16,32,256]{2,1,0:T(8,128)(2,1)} %get-tuple-element.18) | copy-start | bytes 786436
  46.3 17.6 %copy-start.16 = (bf16[2048,128]{1,0:T(8,128)(2,1)S(1)}, bf16[2048,128]{1,0:T(8,128)(2,1)}, u32[]{:S(2)}) copy-start(bf16[2048,128]{1,0:T(8,128)(2,1)} %param.18) | copy-start | bytes 1572868
  46.3 9.9 %collective-permute-start = (bf16[512,256]{1,0:T(8,128)(2,1)S(1)}, bf16[512,256]{1,0:T(8,128)(2,1)S(1)}, u32[]{:S(2)}, u32[]{:S(2)}) collective-permute-start(bf16[512,256]{1,0:T(8,128)(2,1)S(1)} %bitcast.29), channel_id=1, source_target_pairs={{0,16},{16,0},{1,17},{17,1},{2,18},{18,2},{3,19},{19,3},{4,20},{20... | collective-permute-start | bytes 786440 | tf_op jit(solution)/shard_map/ppermute | solution.py:45
  60.4 19.3 %all-to-all-start.2 = ((bf16[8,144,256]{2,1,0:T(8,128)(2,1)}), bf16[8,144,256]{2,1,0:T(8,128)(2,1)S(1)}, u32[]{:S(2)}, u32[]{:S(2)}) async-start(bf16[8,144,256]{2,1,0:T(8,128)(2,1)} %attend.1), calls=%async_computation.2 | async-start | bytes 1179648 | tf_op jit(solution)/shard_map/all_to_all | solution.py:41
  63.9 15.7 %copy-start.14 = (s32[16,2]{0,1:T(2,128)S(1)}, s32[16,2]{0,1:T(2,128)}, u32[]{:S(2)}) copy-start(s32[16,2]{0,1:T(2,128)} %param.21) | copy-start | bytes 388
  64.0 22.4 %collective-permute-start.1 = (bf16[2048,128]{1,0:T(8,128)(2,1)S(1)}, bf16[2048,128]{1,0:T(8,128)(2,1)S(1)}, u32[]{:S(2)}, u32[]{:S(2)}) collective-permute-start(bf16[2048,128]{1,0:T(8,128)(2,1)S(1)} %copy-done.16), channel_id=1, source_target_pairs={{0,4},{4,0},{1,5},{5,1},{2,6},{6,2},{3,7},{7,3},{8,12},{12,8},{9,1... | collective-permute-start | bytes 1572872 | tf_op jit(solution)/shard_map/ppermute | solution.py:442
  71.3 89.3 %collective-permute-start.2 = (bf16[256,2048]{1,0:T(8,128)(2,1)}, bf16[256,2048]{1,0:T(8,128)(2,1)}, u32[]{:S(2)}, u32[]{:S(2)}) collective-permute-start(bf16[256,2048]{1,0:T(8,128)(2,1)} %get-tuple-element.21.refs_0_), channel_id=1, source_target_pairs={{0,1},{1,2},{2,3},{3,0},{4,5},{5,6},{6,7},{7,4},{8,9},{9,10},{10,1... | collective-permute-start | bytes 3145736 | tf_op jit(solution)/shard_map/ppermute | solution.py:49
  74.4 88.6 %collective-permute-start.3 = (bf16[256,2048]{1,0:T(8,128)(2,1)}, bf16[256,2048]{1,0:T(8,128)(2,1)}, u32[]{:S(2)}, u32[]{:S(2)}) collective-permute-start(bf16[256,2048]{1,0:T(8,128)(2,1)} %get-tuple-element.22.refs_1_), channel_id=1, source_target_pairs={{0,4},{4,8},{8,12},{12,0},{1,5},{5,9},{9,13},{13,1},{2,6},{6,10},{... | collective-permute-start | bytes 3145736 | tf_op jit(solution)/shard_map/ppermute | solution.py:49
  76.5 66.7 %collective-permute-start.8 = (bf16[128,2048]{1,0:T(8,128)(2,1)}, bf16[128,2048]{1,0:T(8,128)(2,1)}, u32[]{:S(2)}, u32[]{:S(2)}) collective-permute-start(bf16[128,2048]{1,0:T(8,128)(2,1)} %get-tuple-element.23.refs_8_), channel_id=1, source_target_pairs={{0,1},{1,2},{2,3},{3,0},{4,5},{5,6},{6,7},{7,4},{8,9},{9,10},{10,1... | collective-permute-start | bytes 1572872 | tf_op jit(solution)/shard_map/ppermute | solution.py:49
  80.7 36.6 %all-to-all-start.3 = ((bf16[16,128,128]{2,1,0:T(8,128)(2,1)}), bf16[16,128,128]{2,1,0:T(8,128)(2,1)S(1)}, u32[]{:S(2)}, u32[]{:S(2)}) async-start(bf16[16,128,128]{2,1,0:T(8,128)(2,1)} %combine.1), calls=%async_computation.3 | async-start | bytes 1048576 | tf_op jit(solution)/shard_map/all_to_all | solution.py:41
  117.3 11.2 %copy-start.11 = (bf16[16,2048]{1,0:T(8,128)(2,1)S(1)}, bf16[16,2048]{1,0:T(8,128)(2,1)}, u32[]{:S(2)}) copy-start(bf16[16,2048]{1,0:T(8,128)(2,1)} %residual_ref.1) | copy-start | bytes 196612
  117.3 11.2 %copy-start.12 = (f32[2048]{0:T(1024)S(1)}, f32[2048]{0:T(1024)}, u32[]{:S(2)}) copy-start(f32[2048]{0:T(1024)} %param.19) | copy-start | bytes 24580
  117.3 21.0 %copy-start.2 = (bf16[128,2048]{1,0:T(8,128)(2,1)S(1)}, bf16[128,2048]{1,0:T(8,128)(2,1)}, u32[]{:S(2)}) copy-start(bf16[128,2048]{1,0:T(8,128)(2,1)} %get-tuple-element.24.refs_9_) | copy-start | bytes 1572868
  117.3 23.0 %copy-start.1 = (bf16[128,2048]{1,0:T(8,128)(2,1)S(1)}, bf16[128,2048]{1,0:T(8,128)(2,1)}, u32[]{:S(2)}) copy-start(bf16[128,2048]{1,0:T(8,128)(2,1)} %get-tuple-element.23.refs_8_) | copy-start | bytes 1572868
  118.3 24.9 %copy-start = (bf16[256,2048]{1,0:T(8,128)(2,1)S(1)}, bf16[256,2048]{1,0:T(8,128)(2,1)}, u32[]{:S(2)}) copy-start(bf16[256,2048]{1,0:T(8,128)(2,1)} %get-tuple-element.21.refs_0_) | copy-start | bytes 3145732
  118.3 10.2 %all-to-all-start.4 = ((bf16[8,16,256]{2,1,0:T(8,128)(2,1)}), bf16[8,16,256]{2,1,0:T(8,128)(2,1)S(1)}, u32[]{:S(2)}, u32[]{:S(2)}) async-start(bf16[8,16,256]{2,1,0:T(8,128)(2,1)} %bitcast.9), calls=%async_computation.4 | async-start | bytes 131072 | tf_op jit(solution)/shard_map/all_to_all | solution.py:41
  129.6 35.6 %all-to-all-start.5 = ((bf16[32,16,256]{2,1,0:T(8,128)(2,1)}), bf16[32,16,256]{2,1,0:T(8,128)(2,1)S(1)}, u32[]{:S(2)}, u32[]{:S(2)}) async-start(bf16[32,16,256]{2,1,0:T(8,128)(2,1)} %bitcast.13), calls=%async_computation.5 | async-start | bytes 524288 | tf_op jit(solution)/shard_map/all_to_all | solution.py:41
  138.4 16.4 %collective-permute-start.9 = (bf16[128,2048]{1,0:T(8,128)(2,1)S(1)}, bf16[128,2048]{1,0:T(8,128)(2,1)S(1)}, u32[]{:S(2)}, u32[]{:S(2)}) collective-permute-start(bf16[128,2048]{1,0:T(8,128)(2,1)S(1)} %copy-done.2), channel_id=1, source_target_pairs={{0,4},{4,8},{8,12},{12,0},{1,5},{5,9},{9,13},{13,1},{2,6},{6,10},{... | collective-permute-start | bytes 1572872 | tf_op jit(solution)/shard_map/ppermute | solution.py:49
  140.3 16.3 %collective-permute-start.10 = (bf16[128,2048]{1,0:T(8,128)(2,1)S(1)}, bf16[128,2048]{1,0:T(8,128)(2,1)S(1)}, u32[]{:S(2)}, u32[]{:S(2)}) collective-permute-start(bf16[128,2048]{1,0:T(8,128)(2,1)S(1)} %copy-done.1), channel_id=1, source_target_pairs={{0,3},{1,0},{2,1},{3,2},{4,7},{5,4},{6,5},{7,6},{8,11},{9,8},{10,9... | collective-permute-start | bytes 1572872 | tf_op jit(solution)/shard_map/ppermute | solution.py:49
  143.2 34.5 %collective-permute-start.4 = (bf16[256,2048]{1,0:T(8,128)(2,1)S(1)}, bf16[256,2048]{1,0:T(8,128)(2,1)}, u32[]{:S(2)}, u32[]{:S(2)}) collective-permute-start(bf16[256,2048]{1,0:T(8,128)(2,1)S(1)} %copy-done), channel_id=1, source_target_pairs={{0,3},{1,0},{2,1},{3,2},{4,7},{5,4},{6,5},{7,6},{8,11},{9,8},{10,9... | collective-permute-start | bytes 3145736 | tf_op jit(solution)/shard_map/ppermute | solution.py:49
  154.7 8.2 %copy-start.3 = (bf16[128,2048]{1,0:T(8,128)(2,1)}, bf16[128,2048]{1,0:T(8,128)(2,1)S(1)}, u32[]{:S(2)}) copy-start(bf16[128,2048]{1,0:T(8,128)(2,1)S(1)} %collective-permute-done.9.refs_11_) | copy-start | bytes 1572868
  154.7 18.3 %collective-permute-start.11 = (bf16[128,2048]{1,0:T(8,128)(2,1)S(1)}, bf16[128,2048]{1,0:T(8,128)(2,1)}, u32[]{:S(2)}, u32[]{:S(2)}) collective-permute-start(bf16[128,2048]{1,0:T(8,128)(2,1)S(1)} %copy-done.2), channel_id=1, source_target_pairs={{0,12},{4,0},{8,4},{12,8},{1,13},{5,1},{9,5},{13,9},{2,14},{6,2},{... | collective-permute-start | bytes 1572872 | tf_op jit(solution)/shard_map/ppermute | solution.py:49
  156.6 0.8 copy-start.5
  157.5 42.4 %collective-permute-start.5 = (bf16[256,2048]{1,0:T(8,128)(2,1)}, bf16[256,2048]{1,0:T(8,128)(2,1)}, u32[]{:S(2)}, u32[]{:S(2)}) collective-permute-start(bf16[256,2048]{1,0:T(8,128)(2,1)} %get-tuple-element.22.refs_1_), channel_id=1, source_target_pairs={{0,12},{4,0},{8,4},{12,8},{1,13},{5,1},{9,5},{13,9},{2,14},{6,2},{... | collective-permute-start | bytes 3145736 | tf_op jit(solution)/shard_map/ppermute | solution.py:49
  160.6 50.8 %collective-permute-start.6 = (bf16[256,2048]{1,0:T(8,128)(2,1)}, bf16[256,2048]{1,0:T(8,128)(2,1)}, u32[]{:S(2)}, u32[]{:S(2)}) collective-permute-start(bf16[256,2048]{1,0:T(8,128)(2,1)} %collective-permute-done.2.refs_2_), channel_id=1, source_target_pairs={{0,1},{1,2},{2,3},{3,0},{4,5},{5,6},{6,7},{7,4},{8,9},{9,10},{10,1... | collective-permute-start | bytes 3145736 | tf_op jit(solution)/shard_map/ppermute | solution.py:49
  163.0 48.4 %collective-permute-start.7 = (bf16[256,2048]{1,0:T(8,128)(2,1)}, bf16[256,2048]{1,0:T(8,128)(2,1)}, u32[]{:S(2)}, u32[]{:S(2)}) collective-permute-start(bf16[256,2048]{1,0:T(8,128)(2,1)} %collective-permute-done.3.refs_3_), channel_id=1, source_target_pairs={{0,4},{4,8},{8,12},{12,0},{1,5},{5,9},{9,13},{13,1},{2,6},{6,10},{... | collective-permute-start | bytes 3145736 | tf_op jit(solution)/shard_map/ppermute | solution.py:49
  166.6 44.8 %all-to-all-start.6 = ((bf16[16,16,2048]{2,1,0:T(8,128)(2,1)}), bf16[16,16,2048]{2,1,0:T(8,128)(2,1)S(1)}, u32[]{:S(2)}, u32[]{:S(2)}) async-start(bf16[16,16,2048]{2,1,0:T(8,128)(2,1)} %deal.1), calls=%async_computation.6 | async-start | bytes 2097152 | tf_op jit(solution)/shard_map/all_to_all | solution.py:41
  173.0 35.5 %collective-permute-start.12 = (bf16[128,2048]{1,0:T(8,128)(2,1)}, bf16[128,2048]{1,0:T(8,128)(2,1)S(1)}, u32[]{:S(2)}, u32[]{:S(2)}) collective-permute-start(bf16[128,2048]{1,0:T(8,128)(2,1)} %collective-permute-done.8.refs_10_), channel_id=1, source_target_pairs={{0,1},{1,2},{2,3},{3,0},{4,5},{5,6},{6,7},{7,4},{8,9},{9,10},{10,1... | collective-permute-start | bytes 1572872 | tf_op jit(solution)/shard_map/ppermute | solution.py:49
  177.8 32.8 %collective-permute-start.13 = (bf16[128,2048]{1,0:T(8,128)(2,1)}, bf16[128,2048]{1,0:T(8,128)(2,1)S(1)}, u32[]{:S(2)}, u32[]{:S(2)}) collective-permute-start(bf16[128,2048]{1,0:T(8,128)(2,1)} %copy-done.3), channel_id=1, source_target_pairs={{0,4},{4,8},{8,12},{12,0},{1,5},{5,9},{9,13},{13,1},{2,6},{6,10},{... | collective-permute-start | bytes 1572872 | tf_op jit(solution)/shard_map/ppermute | solution.py:49
  208.4 0.8 copy-start.7
  210.6 0.8 copy-start.9
  211.4 1.0 copy-start.4
  212.4 1.0 copy-start.6
  213.5 1.0 copy-start.8
  214.5 1.0 copy-start.10
  243.2 16.8 %copy-start.15 = (f32[16,2]{0,1:T(2,128)S(1)}, f32[16,2]{0,1:T(2,128)}, u32[]{:S(2)}) copy-start(f32[16,2]{0,1:T(2,128)} %param.22) | copy-start | bytes 388
  244.3 38.0 %all-to-all-start.8 = ((bf16[32,16,256]{2,1,0:T(8,128)(2,1)}), bf16[32,16,256]{2,1,0:T(8,128)(2,1)S(1)}, u32[]{:S(2)}, u32[]{:S(2)}) async-start(bf16[32,16,256]{2,1,0:T(8,128)(2,1)} %bitcast.17), calls=%async_computation.8 | async-start | bytes 524288 | tf_op jit(solution)/shard_map/all_to_all | solution.py:41
